TPU v7x, 256 devices: a whole 4x4x8 slice. The times are simulated.
256 devices in a mesh: sp: 64 (over z, x, core), tp: 4 (over y).
Axes of the slice: x: 4, y: 4, z: 8, core: 2. Of those that a mesh axis runs over, the one named last changes fastest.
Arguments:
- receptance: bfloat16 [8192, 1024], P('sp', 'tp'), may hold values from -6 to 6
- key_by_head: bfloat16 [8192, 1024], P('sp', 'tp'), may hold values from -6 to 6
- value_head_rows: bfloat16 [8192, 1024], P('sp', 'tp'), may hold values from -6 to 6
- decay_preact: bfloat16 [8192, 1024], P('sp', 'tp'), may hold values from -13 to -0.5
- correction_preact: bfloat16 [8192, 1024], P('sp', 'tp'), may hold values from -7 to 3
- result_sigmoid_factor: bfloat16 [8192, 1024], P('sp', 'tp'), may hold values from -6 to 6
- key_rate_mixing: float32 [1024], P('tp'), may hold values from 0.3 to 0.9
- diagonal_current_factor: float32 [1024], P('tp'), may hold values from -0.6 to 0.6
- per_head_gain: float32 [1024], P('tp'), may hold values from 0.1 to 1.9
- per_head_bias: float32 [1024], P('tp'), may hold values from -1.5 to 1.5
- output_matrix: bfloat16 [1024, 2048], P('tp'), may hold values from -0.1875 to 0.1875
- residual: bfloat16 [8192, 2048], P('sp'), may hold values from -6 to 6
- expert_norm_gain: float32 [2048], replicated, may hold values from 0.1 to 1.9
- routes: int32 [8192, 8], P('sp'), may hold values from 0 to 255, all different within a row; in each aligned block of 128 rows (0 to 127, 128 to 255, ...) at most 6 rows name the same one
- chosen_expert_weight: float32 [8192, 8], P('sp'), may hold values from 0.05 to 0.6
- routed_gate_weight: bfloat16 [256, 2048, 512], P(('sp', 'tp')), may hold values from -0.125 to 0.125
- routed_up_weight: bfloat16 [256, 2048, 512], P(('sp', 'tp')), may hold values from -0.125 to 0.125
- routed_down_weight: bfloat16 [256, 512, 2048], P(('sp', 'tp')), may hold values from -0.25 to 0.25
- common_gate_weight: bfloat16 [2048, 512], P(None, 'tp'), may hold values from -0.125 to 0.125
- common_up_weight: bfloat16 [2048, 512], P(None, 'tp'), may hold values from -0.125 to 0.125
- common_down_weight: bfloat16 [512, 2048], P('tp'), may hold values from -0.25 to 0.25
Outputs:
- layer_out: bfloat16 [8192, 2048], P('sp', 'tp')
Inputs may be any that keep to these rules, and one draw needn't show every extreme that they name: `routes`: each row names 8 different experts; in each aligned block of 128 rows no expert is named by more than 6 rows.
All inputs are finite; a program needn't handle non-finite values.
Results may differ from a plain program's by a relative error of at most 0.018.
Values may be sent and summed in bfloat16 or wider, within the bound.
No kernel may reach another device: no remote copies, remote signals or barrier semaphores. Data moves between devices by JAX's collectives and lax.ppermute only.
A program may use at most 64 MiB of HBM per device.

v0:
```python
import jax
import jax.numpy as jnp
from jax import lax
from jax.sharding import Mesh
from jax.sharding import PartitionSpec as P

CHANNEL_SPAN = 64
SP = ("sp_0", "sp_1", "sp_2")
SP_TP = ("sp_0", "sp_1", "sp_2", "tp")


NORM_EPS = 1e-06
GROUP_EPS = 0.00064
HIGHEST = lax.Precision.HIGHEST


def neutral_like(array, identity):
    return jax.tree.map(
        lambda part, zero: jnp.zeros_like(part) + jnp.asarray(zero, part.dtype), array, identity
    )


def carried_in(array, axes, combine, identity):
    before = start = neutral_like(array, identity)
    total = array
    for axis in reversed(axes):
        peers, position = (lax.axis_size(axis), lax.axis_index(axis))
        pieces = jax.tree.map(lambda part: lax.all_gather(part, axis), total)
        inside, total = (start, start)
        for k in range(peers):
            passed = k < position
            total = combine(total, jax.tree.map(lambda part: part[k], pieces))
            inside = jax.tree.map(lambda new, old: jnp.where(passed, new, old), total, inside)
        before = combine(inside, before)
    return before


def from_everyone(array, axis):
    copies = jnp.broadcast_to(array, (lax.axis_size(axis), *array.shape))
    return lax.all_to_all(copies, axis, split_axis=0, concat_axis=0, tiled=True)


def joined_along(blocks, dim):
    blocks = jnp.moveaxis(blocks, 0, dim)
    shape = blocks.shape
    return blocks.reshape(*shape[:dim], shape[dim] * shape[dim + 1], *shape[dim + 2 :])


def gather_directly(array, axis, dim):
    blocks = from_everyone(array, axis)
    return joined_along(blocks, dim)


def split_up(array, dim, peers):
    before, after = (array.shape[:dim], array.shape[dim + 1 :])
    return jnp.moveaxis(array.reshape(*before, peers, -1, *after), dim, 0)


def summed_on_arrival(array, axis, dim):
    blocks = split_up(array, dim, lax.axis_size(axis))
    arrived = lax.all_to_all(blocks, axis, split_axis=0, concat_axis=0, tiled=True)
    return arrived.astype(jnp.float32).sum(axis=0)


def partition_channels(source, head_size):
    row_count, col_count = source.shape
    return source.astype(jnp.float32).reshape(row_count, col_count // head_size, head_size)


def prepare(
    receptance, key_by_head, value_head_rows, decay_preact, correction_preact, key_rate_mixing
):
    key_rows = partition_channels(key_by_head, CHANNEL_SPAN)
    learning = jax.nn.sigmoid(partition_channels(correction_preact, CHANNEL_SPAN))
    length = jnp.sqrt(jnp.sum(key_rows * key_rows, axis=-1, keepdims=True))
    unit_keys = key_rows / jnp.maximum(length, 1.0)
    mix_rows = key_rate_mixing.reshape(1, key_rows.shape[1], CHANNEL_SPAN)
    interpolated_lookup_vectors = key_rows * (1.0 + (learning - 1.0) * mix_rows)
    log_decay = -jnp.exp(-jax.nn.softplus(-partition_channels(decay_preact, CHANNEL_SPAN)) - 0.5)
    return (
        partition_channels(receptance, CHANNEL_SPAN),
        interpolated_lookup_vectors,
        partition_channels(value_head_rows, CHANNEL_SPAN),
        log_decay,
        unit_keys,
        learning,
    )


def finalize(
    state_readout,
    query_vectors_partitioned,
    interpolated_lookup_vectors,
    content_vectors_partitioned,
    per_head_gain,
    per_head_bias,
    diagonal_current_factor,
    result_sigmoid_factor,
):
    shard_attention_count = state_readout.shape[1]
    average = jnp.mean(state_readout, axis=-1, keepdims=True)
    centred = state_readout - average
    variance = jnp.mean(centred * centred, axis=-1, keepdims=True)
    standardized_channels = centred * lax.rsqrt(variance + GROUP_EPS)
    standardized_channels = standardized_channels * per_head_gain.reshape(
        1, shard_attention_count, CHANNEL_SPAN
    ) + per_head_bias.reshape(1, shard_attention_count, CHANNEL_SPAN)
    diagonal_extra_contribution = (
        jnp.sum(
            query_vectors_partitioned
            * interpolated_lookup_vectors
            * diagonal_current_factor.reshape(1, shard_attention_count, CHANNEL_SPAN),
            axis=-1,
            keepdims=True,
        )
        * content_vectors_partitioned
    )
    concatenated_channels = (
        standardized_channels + diagonal_extra_contribution
    ) * partition_channels(result_sigmoid_factor, CHANNEL_SPAN)
    return concatenated_channels.reshape(
        state_readout.shape[0], shard_attention_count * CHANNEL_SPAN
    ).astype(jnp.bfloat16)


def expert_apply(rows_in, gate_weight, up_weight, down_weight):
    gate_part = jnp.dot(rows_in, gate_weight, preferred_element_type=jnp.float32)
    up_part = jnp.dot(rows_in, up_weight, preferred_element_type=jnp.float32)
    hidden = (jax.nn.silu(gate_part) * up_part).astype(jnp.bfloat16)
    return jnp.dot(hidden, down_weight, preferred_element_type=jnp.float32)


def to_blocks(source, span_len):
    row_count, head_count, head_size = source.shape
    return source.reshape(row_count // span_len, span_len, head_count, head_size).transpose(
        0, 2, 1, 3
    )


def from_blocks(source):
    block_count, head_count, span_len, head_size = source.shape
    return source.transpose(0, 2, 1, 3).reshape(block_count * span_len, head_count, head_size)


def compose(former, latter):
    return (
        jnp.matmul(former[0], latter[0], precision=HIGHEST),
        jnp.matmul(former[1], latter[0], precision=HIGHEST) + latter[1],
    )


def pair_products(left_rows, right_rows, keep_mask):
    return jnp.where(
        keep_mask, jnp.einsum("bhtn,bhsn->bhts", left_rows, right_rows, precision=HIGHEST), 0.0
    )


def unit_lower_inverse(strict_part, span_len):
    inverse = jnp.eye(span_len, dtype=jnp.float32) + strict_part
    power = strict_part
    covered = 1
    while covered < span_len - 1:
        power = jnp.matmul(power, power, precision=HIGHEST)
        inverse = inverse + jnp.matmul(inverse, power, precision=HIGHEST)
        covered = 2 * covered + 1
    return inverse


def block_terms(recept, interpolated_lookup_vectors, values, log_decay, unit_keys, learning):
    span_len = recept.shape[2]
    head_size = recept.shape[3]
    cumulative = jnp.cumsum(log_decay, axis=2)
    before = -jnp.exp(cumulative - log_decay) * unit_keys
    inverse_decay = jnp.exp(-cumulative)
    erase_cols = inverse_decay * unit_keys * learning
    write_cols = inverse_decay * interpolated_lookup_vectors
    read_rows = jnp.exp(cumulative) * recept
    later_row = lax.broadcasted_iota(jnp.int32, (span_len, span_len), 0)
    earlier_col = lax.broadcasted_iota(jnp.int32, (span_len, span_len), 1)
    strict = later_row > earlier_col
    inclusive = later_row >= earlier_col
    erase_pairs = pair_products(before, erase_cols, strict)
    write_pairs = pair_products(before, write_cols, strict)
    read_erase = pair_products(read_rows, erase_cols, inclusive)
    read_write = pair_products(read_rows, write_cols, inclusive)
    system_inverse = unit_lower_inverse(erase_pairs, span_len)
    right_side = jnp.concatenate(
        [jnp.einsum("bhts,bhsn->bhtn", write_pairs, values, precision=HIGHEST), before], axis=-1
    )
    solved = jnp.matmul(system_inverse, right_side, precision=HIGHEST)
    removed = solved[..., :head_size]
    carried = solved[..., head_size:]
    local_out = jnp.einsum("bhts,bhsn->bhtn", read_erase, removed, precision=HIGHEST) + jnp.einsum(
        "bhts,bhsn->bhtn", read_write, values, precision=HIGHEST
    )
    query_eff = read_rows + jnp.einsum("bhts,bhsn->bhtn", read_erase, carried, precision=HIGHEST)
    final_decay = jnp.exp(cumulative[:, :, span_len - 1 :, :])
    erase_end = final_decay * erase_cols
    write_end = final_decay * write_cols
    transit = (
        jnp.einsum("bhtj,bhtk->bhjk", carried, erase_end, precision=HIGHEST)
        + jnp.eye(head_size, dtype=jnp.float32) * final_decay
    )
    contrib = jnp.einsum("bhti,bhtk->bhik", removed, erase_end, precision=HIGHEST) + jnp.einsum(
        "bhti,bhtk->bhik", values, write_end, precision=HIGHEST
    )
    return (local_out, query_eff, transit, contrib)


def memory_heads(
    query_vectors_partitioned,
    interpolated_lookup_vectors,
    content_vectors_partitioned,
    log_decay,
    unit_keys,
    learning,
):
    span_len = min(64, query_vectors_partitioned.shape[0])
    local_out, query_eff, transit, contrib = block_terms(
        to_blocks(query_vectors_partitioned, span_len),
        to_blocks(interpolated_lookup_vectors, span_len),
        to_blocks(content_vectors_partitioned, span_len),
        to_blocks(log_decay, span_len),
        to_blocks(unit_keys, span_len),
        to_blocks(learning, span_len),
    )
    inner_p, inner_c = lax.associative_scan(compose, (transit, contrib), axis=0)
    totals = (inner_p[-1], inner_c[-1])
    head_count = transit.shape[1]
    head_size = transit.shape[2]
    identity_p = jnp.broadcast_to(
        jnp.eye(head_size, dtype=jnp.float32), (head_count, head_size, head_size)
    )
    zero_maps = jnp.zeros_like(identity_p)
    prefix = carried_in(totals, SP, compose, (identity_p, zero_maps))
    entering = prefix[1]
    start_p = jnp.concatenate([identity_p[None], inner_p[:-1]], axis=0)
    start_c = jnp.concatenate([zero_maps[None], inner_c[:-1]], axis=0)
    state_in = jnp.matmul(entering[None], start_p, precision=HIGHEST) + start_c
    state_readout = local_out + jnp.einsum(
        "bhtj,bhij->bhti", query_eff, state_in, precision=HIGHEST
    )
    return from_blocks(state_readout)


def per_device(
    receptance,
    key_by_head,
    value_head_rows,
    decay_preact,
    correction_preact,
    result_sigmoid_factor,
    key_rate_mixing,
    diagonal_current_factor,
    per_head_gain,
    per_head_bias,
    output_matrix,
    residual,
    expert_norm_gain,
    routes,
    chosen_expert_weight,
    routed_gate_weight,
    routed_up_weight,
    routed_down_weight,
    common_gate_weight,
    common_up_weight,
    common_down_weight,
):
    (
        query_vectors_partitioned,
        interpolated_lookup_vectors,
        content_vectors_partitioned,
        log_decay,
        unit_keys,
        learning,
    ) = prepare(
        receptance, key_by_head, value_head_rows, decay_preact, correction_preact, key_rate_mixing
    )
    state_readout = memory_heads(
        query_vectors_partitioned,
        interpolated_lookup_vectors,
        content_vectors_partitioned,
        log_decay,
        unit_keys,
        learning,
    )
    blended_heads = finalize(
        state_readout,
        query_vectors_partitioned,
        interpolated_lookup_vectors,
        content_vectors_partitioned,
        per_head_gain,
        per_head_bias,
        diagonal_current_factor,
        result_sigmoid_factor,
    )
    whole_heads = gather_directly(blended_heads, "tp", 1)
    projected = jnp.dot(
        whole_heads,
        lax.all_gather(output_matrix, "tp", axis=0, tiled=True),
        preferred_element_type=jnp.float32,
    )
    middle = (residual.astype(jnp.float32) + projected).astype(jnp.bfloat16)
    middle_full = middle.astype(jnp.float32)
    row_scale = lax.rsqrt(jnp.mean(middle_full * middle_full, axis=-1, keepdims=True) + NORM_EPS)
    normed = (middle_full * row_scale * expert_norm_gain).astype(jnp.bfloat16)
    tp_index = lax.axis_index("tp")
    tp_count = lax.axis_size("tp")
    sp_count = lax.axis_size(SP)
    token_count, top_count = routes.shape
    model_width = normed.shape[1]
    capacity = 3 * token_count * top_count // (2 * sp_count * tp_count)
    owned_routes = routes % tp_count == tp_index
    target = routes // tp_count
    places = jnp.arange(sp_count, dtype=jnp.int32)
    hit_counts = jnp.sum(
        jnp.where(owned_routes[:, :, None] & (target[:, :, None] == places[None, None, :]), 1, 0),
        axis=1,
    ).astype(jnp.int32)
    earlier = jnp.cumsum(hit_counts, axis=0) - hit_counts
    within = jnp.take_along_axis(earlier, target, axis=1)
    slot_index = target * capacity + within
    dropped = sp_count * capacity
    flat_slots = jnp.where(owned_routes, slot_index, dropped).reshape(-1)
    token_ids = jnp.broadcast_to(jnp.arange(token_count, dtype=jnp.int32)[:, None], routes.shape)
    slot_tokens = (
        jnp.full((dropped,), token_count, jnp.int32)
        .at[flat_slots]
        .set(token_ids.reshape(-1), mode="drop")
    )
    slot_weights = (
        jnp.zeros((dropped,), jnp.float32)
        .at[flat_slots]
        .set(chosen_expert_weight.reshape(-1), mode="drop")
    )
    padded = jnp.concatenate([normed, jnp.zeros((1, model_width), jnp.bfloat16)], axis=0)
    outgoing = padded[slot_tokens].reshape(sp_count, capacity, model_width)
    arrived = lax.all_to_all(outgoing, SP, split_axis=0, concat_axis=0, tiled=True)
    source_count, item_count, feature_count = arrived.shape
    flat_rows = arrived.reshape(source_count * item_count, feature_count)
    answer = expert_apply(
        flat_rows, routed_gate_weight[0], routed_up_weight[0], routed_down_weight[0]
    ).astype(jnp.bfloat16)
    returned = lax.all_to_all(
        answer.reshape(source_count, item_count, feature_count),
        SP,
        split_axis=0,
        concat_axis=0,
        tiled=True,
    )
    flat_back = returned.reshape(dropped, model_width)
    token_rows = jnp.arange(token_count, dtype=jnp.int32)
    combine_table = jnp.where(
        slot_tokens[None, :] == token_rows[:, None], slot_weights[None, :], 0.0
    )
    routed = jnp.dot(combine_table, flat_back.astype(jnp.float32), precision=HIGHEST)
    shared_out = expert_apply(normed, common_gate_weight, common_up_weight, common_down_weight)
    summed = summed_on_arrival((routed + shared_out).astype(jnp.bfloat16), "tp", 1)
    col_count = summed.shape[1]
    own_cols = lax.dynamic_slice_in_dim(middle, tp_index * col_count, col_count, 1)
    return (own_cols.astype(jnp.float32) + summed).astype(jnp.bfloat16)


def solution(mesh):
    finer = Mesh(mesh.devices.reshape(8, 4, 2, mesh.shape["tp"]), ("sp_0", "sp_1", "sp_2", "tp"))
    placed = (
        P(SP, "tp"),
        P(SP, "tp"),
        P(SP, "tp"),
        P(SP, "tp"),
        P(SP, "tp"),
        P(SP, "tp"),
        P("tp"),
        P("tp"),
        P("tp"),
        P("tp"),
        P("tp", None),
        P(SP, None),
        P(),
        P(SP, None),
        P(SP, None),
        P(SP_TP, None, None),
        P(SP_TP, None, None),
        P(SP_TP, None, None),
        P(None, "tp"),
        P(None, "tp"),
        P("tp", None),
    )
    return jax.shard_map(
        per_device, mesh=finer, in_specs=placed, out_specs=P(SP, "tp"), check_vma=False
    )
```

profile of v0, /device:TPU:1, one launch (start us, length us, event | category | flops | bytes accessed | tf_op | source)
XLA Modules:
  0.0 337.7 jit_solution(14527262596248538851)
XLA Ops:
  7.3 0.9 copy.111
  12.9 1.4 bitcast_multiply_fusion
  17.6 1.1 fusion.169
  18.7 1.1 convolution_add_fusion.3
  19.8 1.2 convolution_select_fusion.1
  21.0 1.0 reshape_reshape.7
  22.0 1.5 convolution_add_fusion.2
  23.6 1.2 fusion.72
  26.0 0.9 convolution_bitcast_fusion.3
  28.5 0.9 fusion.20
  29.4 0.9 copy.108
  30.4 0.9 reshape.286
  31.9 1.6 pad_add_fusion.1
  33.6 4.9 %all_gather.33 = f32[2,4,64,64]{3,2,1,0:T(8,128)S(1)} all-gather(f32[1,4,64,64]{3,2,1,0:T(8,128)S(1)} %get-tuple-element.13), channel_id=1, replica_groups=mesh['sp_0'=8,'sp_1'=4,'sp_2'=2,'tp'=4] {'sp_2'}, dimensions={0}, use_global_device_ids=true | all-gather | bytes 196608 | tf_op jit(solution)/shard_map/all_gather | solution.py:28
  39.6 11.1 %all-gather = f32[16,64,64]{2,1,0:T(8,128)S(1)} all-gather(f32[4,64,64]{2,1,0:T(8,128)S(1)} %fusion.95), channel_id=2, replica_groups=mesh['sp_0'=8,'sp_1'=4,'sp_2'=2,'tp'=4] {'sp_1'}, dimensions={0}, use_global_device_ids=true | all-gather | bytes 327680 | tf_op jit(solution)/shard_map/all_gather | solution.py:28
  51.4 3.7 %all_gather.38 = f32[2,4,64,64]{3,2,1,0:T(8,128)S(1)} all-gather(f32[1,4,64,64]{3,2,1,0:T(8,128)S(1)} %get-tuple-element.11), channel_id=1, replica_groups=mesh['sp_0'=8,'sp_1'=4,'sp_2'=2,'tp'=4] {'sp_2'}, dimensions={0}, use_global_device_ids=true | all-gather | bytes 196608 | tf_op jit(solution)/shard_map/all_gather | solution.py:28
  56.3 10.9 %all-gather.2 = f32[16,64,64]{2,1,0:T(8,128)S(1)} all-gather(f32[4,64,64]{2,1,0:T(8,128)S(1)} %convolution_add_fusion.22), channel_id=4, replica_groups=mesh['sp_0'=8,'sp_1'=4,'sp_2'=2,'tp'=4] {'sp_1'}, dimensions={0}, use_global_device_ids=true | all-gather | bytes 327680 | tf_op jit(solution)/shard_map/all_gather | solution.py:28
  70.1 23.7 %all-gather.1 = f32[32,64,64]{2,1,0:T(8,128)S(1)} all-gather(f32[4,64,64]{2,1,0:T(8,128)S(1)} %fusion.96), channel_id=3, replica_groups=mesh['sp_0'=8,'sp_1'=4,'sp_2'=2,'tp'=4] {'sp_0'}, dimensions={0}, use_global_device_ids=true | all-gather | bytes 589824 | tf_op jit(solution)/shard_map/all_gather | solution.py:28
  93.8 21.5 %all-gather.3 = f32[32,64,64]{2,1,0:T(8,128)S(1)} all-gather(f32[4,64,64]{2,1,0:T(8,128)S(1)} %convolution_add_fusion.19), channel_id=5, replica_groups=mesh['sp_0'=8,'sp_1'=4,'sp_2'=2,'tp'=4] {'sp_0'}, dimensions={0}, use_global_device_ids=true | all-gather | bytes 589824 | tf_op jit(solution)/shard_map/all_gather | solution.py:28
  117.3 0.9 convolution_add_fusion.17
  118.2 1.1 copy.110
  119.3 1.3 fusion.82
  120.7 1.3 convolution_add_fusion.16
  122.0 1.3 convolution_add_fusion.15
  123.3 1.3 convolution_add_fusion.14
  124.6 1.2 convolution_add_fusion.13
  126.2 1.2 fusion.19
  133.5 0.9 multiply_convert_fusion
  135.3 4.3 %all-to-all-start = ((bf16[4,128,256]{1,2,0:T(8,128)(2,1)}), bf16[4,128,256]{1,2,0:T(8,128)(2,1)S(1)}, u32[]{:S(2)}, u32[]{:S(2)}) async-start(bf16[4,128,256]{1,2,0:T(8,128)(2,1)} %broadcast_in_dim.112), calls=%async_computation | async-start | bytes 524288 | tf_op jit(solution)/shard_map/all_to_all | solution.py:40
  140.4 7.1 %gather_fusion.1 = s32[1024]{0:T(1024)S(1)} fusion(s32[128,64]{1,0:T(8,128)S(1)} %sub.47, s32[1024]{0:T(1024)S(1)} %reshape.205), kind=kCustom, calls=%fused_computation.1 | custom fusion | bytes 16384 | tf_op jit(solution)/shard_map/jit(take_along_axis)/gather | solution.py:321
  147.9 4.5 %scatter_custom_fusion = s32[384]{0:T(512)S(1)} fusion(s32[1024]{0:T(1024)S(1)} %bitcast.203, s32[1024]{0:T(1024)S(1)} %reshape.215, s32[]{:T(128)} %constant.112.clone.1), kind=kCustom, calls=%fused_computation.237 | custom fusion | bytes 1540 | tf_op jit(solution)/shard_map/scatter | solution.py:329
  152.5 3.0 fusion.22
  156.6 3.1 gather_fusion
  159.7 3.7 %reshape.190 = bf16[64,6,2048]{2,1,0:T(8,128)(2,1)} reshape(bf16[384,2048]{1,0:T(8,128)(2,1)} %gather_fusion) | data formatting | bytes 3145728 | tf_op jit(solution)/shard_map/reshape | solution.py:337
  163.4 70.8 %all_to_all.20 = bf16[64,6,2048]{2,1,0:T(8,128)(2,1)} all-to-all(bf16[64,6,2048]{2,1,0:T(8,128)(2,1)} %reshape.190), channel_id=1, replica_groups=mesh['sp_0'=8,'sp_1'=4,'sp_2'=2,'tp'=4] {'sp_0','sp_1','sp_2'}, dimensions={0} | all-to-all | bytes 3145728 | tf_op jit(solution)/shard_map/all_to_all | solution.py:338
  234.2 3.7 %reshape.191 = bf16[384,2048]{1,0:T(8,128)(2,1)} reshape(bf16[64,6,2048]{2,1,0:T(8,128)(2,1)} %all_to_all.20) | data formatting | bytes 3145728 | tf_op jit(solution)/shard_map/reshape | solution.py:340
  237.9 3.9 %fusion.6 = f32[384,512]{1,0:T(8,128)} fusion(bf16[384,2048]{1,0:T(8,128)(2,1)} %reshape.191, bf16[1,2048,512]{2,1,0:T(8,128)(2,1)} %param.36), kind=kOutput, calls=%fused_computation.13 | convolution fusion | flops 805306368 | bytes 4456448 | tf_op jit(solution)/shard_map/dot_general | solution.py:127
  241.8 5.3 %convolution_convert_fusion = bf16[384,2048]{1,0:T(8,128)(2,1)} fusion(bf16[1,512,2048]{2,1,0:T(8,128)(2,1)S(1)} %copy-done, bf16[384,2048]{1,0:T(8,128)(2,1)} %reshape.191, bf16[1,2048,512]{2,1,0:T(8,128)(2,1)} %param.37, f32[384,512]{1,0:T(8,128)} %fusion.6), kind=kOutput, calls=%fused_computation.5 | convolution fusion | flops 1612578816 | bytes 8126464 | tf_op jit(solution)/shard_map/dot_general | solution.py:130
  247.1 3.7 %reshape.192 = bf16[64,6,2048]{2,1,0:T(8,128)(2,1)} reshape(bf16[384,2048]{1,0:T(8,128)(2,1)} %convolution_convert_fusion) | data formatting | bytes 3145728 | tf_op jit(solution)/shard_map/reshape | solution.py:345
  250.8 7.3 %all-to-all-start.2 = ((bf16[64,6,2048]{2,1,0:T(8,128)(2,1)}), bf16[64,6,2048]{2,1,0:T(8,128)(2,1)}, u32[]{:S(2)}, u32[]{:S(2)}) async-start(bf16[64,6,2048]{2,1,0:T(8,128)(2,1)} %reshape.192), calls=%async_computation.2 | async-start | bytes 4194304 | tf_op jit(solution)/shard_map/all_to_all | solution.py:344
  258.3 4.3 %scatter_custom_fusion.1 = f32[384]{0:T(512)S(1)} fusion(s32[1024]{0:T(1024)S(1)} %bitcast.204, f32[1024]{0:T(1024)S(1)} %reshape.223, f32[]{:T(128)} %constant.48.clone.1), kind=kCustom, calls=%fused_computation.235 | custom fusion | bytes 1540 | tf_op jit(solution)/shard_map/scatter | solution.py:334
  262.9 44.8 %all-to-all-done.2 = bf16[64,6,2048]{2,1,0:T(8,128)(2,1)} async-done(((bf16[64,6,2048]{2,1,0:T(8,128)(2,1)}), bf16[64,6,2048]{2,1,0:T(8,128)(2,1)}, u32[]{:S(2)}, u32[]{:S(2)}) %all-to-all-start.2) | async-done | bytes 1572896 | tf_op jit(solution)/shard_map/all_to_all | solution.py:344
  307.8 3.7 %reshape.193 = bf16[384,2048]{1,0:T(8,128)(2,1)} reshape(bf16[64,6,2048]{2,1,0:T(8,128)(2,1)} %all-to-all-done.2) | data formatting | bytes 3145728 | tf_op jit(solution)/shard_map/reshape | solution.py:351
  311.5 3.4 fusion.56
  314.8 2.1 fusion.2
  317.7 4.5 %all-to-all-start.3 = ((bf16[4,128,512]{2,1,0:T(8,128)(2,1)}), bf16[4,128,512]{2,1,0:T(8,128)(2,1)S(1)}, u32[]{:S(2)}, u32[]{:S(2)}) async-start(bf16[4,128,512]{2,1,0:T(8,128)(2,1)} %bitcast.193), calls=%async_computation.3 | async-start | bytes 1048576 | tf_op jit(solution)/shard_map/all_to_all | solution.py:61
  322.2 7.0 %all-to-all-done.3 = bf16[4,128,512]{2,1,0:T(8,128)(2,1)S(1)} async-done(((bf16[4,128,512]{2,1,0:T(8,128)(2,1)}), bf16[4,128,512]{2,1,0:T(8,128)(2,1)S(1)}, u32[]{:S(2)}, u32[]{:S(2)}) %all-to-all-start.3) | async-done | bytes 524320 | tf_op jit(solution)/shard_map/all_to_all | solution.py:61
  329.3 1.6 add_convert_fusion
  (210 shorter events, 30.2 us)
Async XLA Ops:
  6.5 235.3 %copy-start = (bf16[1,512,2048]{2,1,0:T(8,128)(2,1)S(1)}, bf16[1,512,2048]{2,1,0:T(8,128)(2,1)}, u32[]{:S(2)}) copy-start(bf16[1,512,2048]{2,1,0:T(8,128)(2,1)} %param.38) | copy-start | bytes 6291460
  6.5 4.1 %copy-start.42 = (bf16[128,256]{1,0:T(8,128)(2,1)S(1)}, bf16[128,256]{1,0:T(8,128)(2,1)}, u32[]{:S(2)}) copy-start(bf16[128,256]{1,0:T(8,128)(2,1)} %param.25) | copy-start | bytes 196612
  6.5 6.0 %copy-start.48 = (f32[256]{0:T(256)S(1)}, f32[256]{0:T(256)}, u32[]{:S(2)}) copy-start(f32[256]{0:T(256)} %param.27) | copy-start | bytes 3076
  6.5 145.9 %all-gather.6.cloned.1.call-start = ((), (), s32[]{:S(2)}) async-start(), calls=%async_computation.4 | async-start | bytes 5242880 | tf_op jit(solution)/shard_map/all_gather | solution.py:300
  22.0 1.6 copy-start.4
  24.8 3.3 copy-start.5
  28.5 0.9 copy-start.34
  31.3 19.5 %slice-start = ((f32[2,4,64,64]{3,2,1,0:T(8,128)}), f32[1,4,64,64]{3,2,1,0:T(8,128)S(1)}, s32[]{:S(2)}) async-start(f32[2,4,64,64]{3,2,1,0:T(8,128)} %copy-done.34), calls=%async_computation.5 | async-start | bytes 262144 | tf_op jit(solution)/shard_map/slice | solution.py:227
  31.3 19.5 %copy-start.38 = (f32[1,4,64,64]{3,2,1,0:T(8,128)S(1)}, f32[1,4,64,64]{3,2,1,0:T(8,128)}, u32[]{:S(2)}) copy-start(f32[1,4,64,64]{3,2,1,0:T(8,128)} %fusion.20) | copy-start | bytes 196612
  39.6 15.7 %copy-start.7 = (f32[4,64,64]{2,1,0:T(8,128)}, f32[4,64,64]{2,1,0:T(8,128)S(1)}, u32[]{:S(2)}) copy-start(f32[4,64,64]{2,1,0:T(8,128)S(1)} %fusion.95) | copy-start | bytes 196612
  56.3 12.6 %copy-start.21 = (f32[4,64,64]{2,1,0:T(8,128)}, f32[4,64,64]{2,1,0:T(8,128)S(1)}, u32[]{:S(2)}) copy-start(f32[4,64,64]{2,1,0:T(8,128)S(1)} %convolution_add_fusion.22) | copy-start | bytes 196612
  67.4 1.2 copy-start.15
  68.0 1.5 copy-start.30
  68.3 1.1 copy-start.32
  68.6 25.2 %copy-start.25 = (f32[4,64,64]{2,1,0:T(8,128)}, f32[4,64,64]{2,1,0:T(8,128)S(1)}, u32[]{:S(2)}) copy-start(f32[4,64,64]{2,1,0:T(8,128)S(1)} %convolution_add_fusion.19) | copy-start | bytes 196612
  68.9 49.3 %copy-start.8 = (f32[4,64,64]{2,1,0:T(8,128)}, f32[4,64,64]{2,1,0:T(8,128)S(1)}, u32[]{:S(2)}) copy-start(f32[4,64,64]{2,1,0:T(8,128)S(1)} %fusion.102) | copy-start | bytes 196612
  69.2 49.0 %copy-start.10 = (f32[4,64,64]{2,1,0:T(8,128)}, f32[4,64,64]{2,1,0:T(8,128)S(1)}, u32[]{:S(2)}) copy-start(f32[4,64,64]{2,1,0:T(8,128)S(1)} %fusion.99) | copy-start | bytes 196612
  93.8 22.8 %copy-start.1 = (f32[32,64,64]{2,1,0:T(8,128)}, f32[32,64,64]{2,1,0:T(8,128)S(1)}, u32[]{:S(2)}) copy-start(f32[32,64,64]{2,1,0:T(8,128)S(1)} %all-gather.1) | copy-start | bytes 1572868
  115.3 1.3 copy-start.2
  119.3 6.5 %copy-start.9 = (f32[4,64,64]{2,1,0:T(8,128)S(1)}, f32[4,64,64]{2,1,0:T(8,128)}, u32[]{:S(2)}) copy-start(f32[4,64,64]{2,1,0:T(8,128)} %copy-done.8) | copy-start | bytes 196612
  119.3 6.5 %copy-start.11 = (f32[4,64,64]{2,1,0:T(8,128)S(1)}, f32[4,64,64]{2,1,0:T(8,128)}, u32[]{:S(2)}) copy-start(f32[4,64,64]{2,1,0:T(8,128)} %copy-done.10) | copy-start | bytes 196612
  119.3 6.5 %copy-start.13 = (f32[4,64,64]{2,1,0:T(8,128)S(1)}, f32[4,64,64]{2,1,0:T(8,128)}, u32[]{:S(2)}) copy-start(f32[4,64,64]{2,1,0:T(8,128)} %copy-done.12) | copy-start | bytes 196612
  119.3 6.5 %copy-start.16 = (f32[4,64,64]{2,1,0:T(8,128)S(1)}, f32[4,64,64]{2,1,0:T(8,128)}, u32[]{:S(2)}) copy-start(f32[4,64,64]{2,1,0:T(8,128)} %copy-done.15) | copy-start | bytes 196612
  119.3 6.9 %copy-start.18 = (f32[4,64,64]{2,1,0:T(8,128)S(1)}, f32[4,64,64]{2,1,0:T(8,128)}, u32[]{:S(2)}) copy-start(f32[4,64,64]{2,1,0:T(8,128)} %copy-done.17) | copy-start | bytes 196612
  119.3 6.9 %copy-start.28 = (f32[4,64,64]{2,1,0:T(8,128)S(1)}, f32[4,64,64]{2,1,0:T(8,128)}, u32[]{:S(2)}) copy-start(f32[4,64,64]{2,1,0:T(8,128)} %copy-done.27) | copy-start | bytes 196612
  119.3 6.9 %copy-start.29 = (f32[4,64,64]{2,1,0:T(8,128)S(1)}, f32[4,64,64]{2,1,0:T(8,128)}, u32[]{:S(2)}) copy-start(f32[4,64,64]{2,1,0:T(8,128)} %convolution_add_fusion.17) | copy-start | bytes 196612
  122.0 5.7 %copy-start.24 = (f32[4,64,64]{2,1,0:T(8,128)S(1)}, f32[4,64,64]{2,1,0:T(8,128)}, u32[]{:S(2)}) copy-start(f32[4,64,64]{2,1,0:T(8,128)} %copy-done.23) | copy-start | bytes 196612
  122.0 5.7 %copy-start.26 = (f32[4,64,64]{2,1,0:T(8,128)S(1)}, f32[4,64,64]{2,1,0:T(8,128)}, u32[]{:S(2)}) copy-start(f32[4,64,64]{2,1,0:T(8,128)} %copy-done.25) | copy-start | bytes 196612
  122.0 5.7 %copy-start.31 = (f32[4,64,64]{2,1,0:T(8,128)S(1)}, f32[4,64,64]{2,1,0:T(8,128)}, u32[]{:S(2)}) copy-start(f32[4,64,64]{2,1,0:T(8,128)} %copy-done.30) | copy-start | bytes 196612
  122.0 5.7 %copy-start.33 = (f32[4,64,64]{2,1,0:T(8,128)S(1)}, f32[4,64,64]{2,1,0:T(8,128)}, u32[]{:S(2)}) copy-start(f32[4,64,64]{2,1,0:T(8,128)} %copy-done.32) | copy-start | bytes 196612
  123.3 4.7 %copy-start.20 = (f32[4,64,64]{2,1,0:T(8,128)S(1)}, f32[4,64,64]{2,1,0:T(8,128)}, u32[]{:S(2)}) copy-start(f32[4,64,64]{2,1,0:T(8,128)} %copy-done.19) | copy-start | bytes 196612
  123.3 4.7 %copy-start.22 = (f32[4,64,64]{2,1,0:T(8,128)S(1)}, f32[4,64,64]{2,1,0:T(8,128)}, u32[]{:S(2)}) copy-start(f32[4,64,64]{2,1,0:T(8,128)} %copy-done.21) | copy-start | bytes 196612
  125.9 2.5 copy-start.39
  125.9 2.5 copy-start.40
  128.3 2.2 copy-start.6
  130.9 2.0 copy-start.49
  131.4 1.6 copy-start.35
  131.4 1.6 copy-start.36
  131.4 2.1 copy-start.46
  131.4 2.1 copy-start.47
  132.1 7.5 %copy-start.44 = (s32[128,8]{0,1:T(8,128)S(1)}, s32[128,8]{0,1:T(8,128)}, u32[]{:S(2)}) copy-start(s32[128,8]{0,1:T(8,128)} %param.34) | copy-start | bytes 12292
  135.3 17.1 %all-to-all-start = ((bf16[4,128,256]{1,2,0:T(8,128)(2,1)}), bf16[4,128,256]{1,2,0:T(8,128)(2,1)S(1)}, u32[]{:S(2)}, u32[]{:S(2)}) async-start(bf16[4,128,256]{1,2,0:T(8,128)(2,1)} %broadcast_in_dim.112), calls=%async_computation | async-start | bytes 524288 | tf_op jit(solution)/shard_map/all_to_all | solution.py:40
  140.4 12.1 %copy-start.41 = (bf16[128,2048]{1,0:T(8,128)(2,1)S(1)}, bf16[128,2048]{1,0:T(8,128)(2,1)}, u32[]{:S(2)}) copy-start(bf16[128,2048]{1,0:T(8,128)(2,1)} %param.32) | copy-start | bytes 1572868
  152.5 3.9 %copy-start.43 = (f32[2048]{0:T(1024)S(1)}, f32[2048]{0:T(1024)}, u32[]{:S(2)}) copy-start(f32[2048]{0:T(1024)} %param.33) | copy-start | bytes 24580
  250.8 7.3 %copy-start.45 = (f32[128,8]{0,1:T(8,128)S(1)}, f32[128,8]{0,1:T(8,128)}, u32[]{:S(2)}) copy-start(f32[128,8]{0,1:T(8,128)} %param.35) | copy-start | bytes 12292
  250.8 11.8 %copy-start.37 = (bf16[2048,128]{1,0:T(8,128)(2,1)S(1)}, bf16[2048,128]{1,0:T(8,128)(2,1)}, u32[]{:S(2)}) copy-start(bf16[2048,128]{1,0:T(8,128)(2,1)} %param.39) | copy-start | bytes 1572868
  250.8 56.9 %all-to-all-start.2 = ((bf16[64,6,2048]{2,1,0:T(8,128)(2,1)}), bf16[64,6,2048]{2,1,0:T(8,128)(2,1)}, u32[]{:S(2)}, u32[]{:S(2)}) async-start(bf16[64,6,2048]{2,1,0:T(8,128)(2,1)} %reshape.192), calls=%async_computation.2 | async-start | bytes 4194304 | tf_op jit(solution)/shard_map/all_to_all | solution.py:344
  317.7 11.5 %all-to-all-start.3 = ((bf16[4,128,512]{2,1,0:T(8,128)(2,1)}), bf16[4,128,512]{2,1,0:T(8,128)(2,1)S(1)}, u32[]{:S(2)}, u32[]{:S(2)}) async-start(bf16[4,128,512]{2,1,0:T(8,128)(2,1)} %bitcast.193), calls=%async_computation.3 | async-start | bytes 1048576 | tf_op jit(solution)/shard_map/all_to_all | solution.py:61
  (7 other events, 4.9 us)
Sparse Core Ops, SparseCore 0:
  9.1 54.4 all-gather.5
where the time goes:
time: 341 us; the launch traced here: 338 us
  blocking collectives  147 us (43%)
  waiting for transfers between devices  52.5 us (15%)
  local copies, waits for them, and re-layouts  49.8 us (15%)
  matrix products  48 us (14%)
  starting transfers between devices  16.1 us (5%)
  between operations  14.7 us (4%)
  other arithmetic  10.1 us (3%)
    all_gather x6, blocking collectives, carried_in(): pieces = jax.tree.map(lambda part: lax.all_gather(part, axis), total)  75.7 us
    all_to_all x1, blocking collectives, per_device(): lax.all_to_all(outgoing, SP, split_axis=0, concat_axis=0, tiled=True)  70.8 us
    all_to_all x1, waiting for transfers between devices, per_device(): lax.all_to_all(answer.reshape(source_count, item_count, feature_count), S...  44.8 us
    dot_general x18, matrix products, compose(): jnp.matmul(former[1], latter[0], precision=HIGHEST) + latter[1]  10.9 us
    dot_general x2, matrix products, expert_apply(): return jnp.dot(hidden, down_weight, preferred_element_type=jnp.float32)  7.39 us
    all_to_all x1, starting transfers between devices, per_device(): lax.all_to_all(answer.reshape(source_count, item_count, feature_count), S...  7.3 us
    gather x3, local copies, waits for them, and re-layouts, per_device(): within = jnp.take_along_axis(earlier, target, axis=1)  7.24 us
    all_to_all x1, waiting for transfers between devices, summed_on_arrival(): lax.all_to_all(blocks, axis, split_axis=0, concat_axis=0, tiled=True)  6.96 us
  transfers between devices with their start and end apart: 4, of which 2 were waited for; matrix products, arithmetic and copies ran while one was open for 19% of the time, Pallas kernels for 0%

commit v1 on v0

v1 whole, which is shorter than its diff:
```python
import functools

import jax
import jax.numpy as jnp
from jax import lax
from jax.experimental import pallas as pl
from jax.experimental.pallas import tpu as pltpu
from jax.sharding import Mesh
from jax.sharding import PartitionSpec as P

CH = 64
CAP = 6
LANES = 128
NORM_EPS = 1e-06
GROUP_EPS = 0.00064
PLANE = ("x", "c")
SP = ("z", "x", "c")
EVERY = ("z", "x", "c", "tp")
F32 = jnp.float32
BF16 = jnp.bfloat16
NN = ((1,), (0,))
NT = ((1,), (1,))
TN = ((0,), (0,))
PAD = 104


def dot(a, b, dims=NN):
    return lax.dot_general(a, b, (dims, ((), ())), preferred_element_type=F32)


def split(a):
    high = a.astype(BF16)
    return high, (a - high.astype(F32)).astype(BF16)


def mm(a, b, dims=NN):
    ah, al = split(a)
    bh, bl = split(b)
    return dot(ah, bh, dims) + (dot(al, bh, dims) + dot(ah, bl, dims))


def iotas(rows, cols):
    return (
        lax.broadcasted_iota(jnp.int32, (rows, cols), 0),
        lax.broadcasted_iota(jnp.int32, (rows, cols), 1),
    )


def sigmoid(x):
    return 1.0 / (1.0 + jnp.exp(-x))


def unit_inverse(low):
    n = low.shape[0]
    row, col = iotas(n, n)
    size = 8
    power = jnp.where((row // size) == (col // size), low, 0.0)
    x = jnp.where(row == col, 1.0, 0.0) + power
    span = 2
    while span < size:
        power = mm(power, power)
        x = x + mm(x, power)
        span *= 2
    while size < n:
        part = ((row // (2 * size)) == (col // (2 * size))) & ((row // size) != (col // size))
        x = x + mm(mm(x, jnp.where(part, low, 0.0)), x)
        size *= 2
    return x


def mixed_of(key, learning, mix):
    return key * (1.0 + (learning - 1.0) * mix)


def routing_kernel(routes_ref, weight_ref, token_ref, slot_weight_ref):
    experts, width = token_ref.shape
    top, tokens = routes_ref.shape
    expert, token = iotas(experts, tokens)
    hit = jnp.zeros((experts, tokens), F32)
    weight = jnp.zeros((experts, tokens), F32)
    for k in range(top):
        same = routes_ref[k : k + 1, :] == expert
        hit = hit + jnp.where(same, 1.0, 0.0)
        weight = weight + jnp.where(same, weight_ref[k : k + 1, :], 0.0)
    row, col = iotas(tokens, tokens)
    earlier = jnp.where(row < col, 1.0, 0.0).astype(BF16)
    within = dot(hit.astype(BF16), earlier)
    count = jnp.sum(hit, axis=1, keepdims=True)
    slot = lax.broadcasted_iota(jnp.int32, (experts, width), 1) // (width // CAP)
    tokens_out = jnp.full((experts, width), -1.0, F32)
    weights_out = jnp.zeros((experts, width), F32)
    number = token.astype(F32)
    for m in range(CAP):
        chosen = (hit > 0.5) & (within == float(m))
        name = jnp.sum(jnp.where(chosen, number, 0.0), axis=1, keepdims=True)
        name = jnp.where(count > float(m), name, -1.0)
        part = jnp.sum(jnp.where(chosen, weight, 0.0), axis=1, keepdims=True)
        tokens_out = jnp.where(slot == m, name, tokens_out)
        weights_out = jnp.where(slot == m, part, weights_out)
    token_ref[...] = tokens_out.astype(jnp.int32)
    slot_weight_ref[...] = weights_out


def local_kernel(r_ref, k_ref, v_ref, d_ref, c_ref, mix_ref, map_ref, read_ref):
    t, w = k_ref.shape
    key = k_ref[...].astype(F32)
    learning = sigmoid(c_ref[...].astype(F32))
    log_decay = -0.6065306597126334 * sigmoid(d_ref[...].astype(F32))
    row, col = iotas(w, w)
    group = jnp.where(row // CH == col // CH, 1.0, 0.0).astype(BF16)
    square_high, square_low = split(key * key)
    length = jnp.sqrt(dot(square_high, group) + dot(square_low, group))
    unit = key / jnp.maximum(length, 1.0)
    mixed = mixed_of(key, learning, mix_ref[...])
    row, col = iotas(t, t)
    upto = jnp.where(row >= col, 1.0, 0.0).astype(BF16)
    first = log_decay.astype(BF16)
    second, third = split(log_decay - first.astype(F32))
    total = dot(upto, first) + (dot(upto, second) + dot(upto, third))
    last = total[t - 1 : t, :]
    value = v_ref[...].astype(F32)
    before = -jnp.exp(total - log_decay) * unit
    inverse_decay = jnp.exp(-total)
    rate = unit * learning
    erase = inverse_decay * rate
    write = inverse_decay * mixed
    read = jnp.exp(total) * r_ref[...].astype(F32)
    remaining = jnp.exp(last - total)
    erase_end = remaining * rate
    write_end = remaining * mixed
    final = jnp.exp(last)
    strict = row > col
    inclusive = row >= col
    hrow, hcol = iotas(CH, CH)
    for h in range(w // CH):
        s = slice(h * CH, (h + 1) * CH)
        b, q, v = before[:, s], read[:, s], value[:, s]
        pairs = mm(
            jnp.concatenate([b, q], 0), jnp.concatenate([erase[:, s], write[:, s]], 0), NT
        )
        low = jnp.where(strict, pairs[:t, :t], 0.0)
        wrote = jnp.where(strict, pairs[:t, t:], 0.0)
        read_erase = jnp.where(inclusive, pairs[t:, :t], 0.0)
        read_write = jnp.where(inclusive, pairs[t:, t:], 0.0)
        x = unit_inverse(low)
        on_values = mm(jnp.concatenate([wrote, read_write], 0), v)
        solved = mm(x, jnp.concatenate([b, on_values[:t]], 1))
        read_ref[h] = jnp.concatenate([q, on_values[t:]], 1) + mm(read_erase, solved)
        diagonal = jnp.where(hrow == hcol, jnp.broadcast_to(final[:, s], (CH, CH)), 0.0)
        state = jnp.concatenate([diagonal, mm(write_end[:, s], v, TN)], 1)
        state = state + mm(erase_end[:, s], solved, TN)
        map_ref[2 * h] = state
        map_ref[2 * h + 1] = state


def plane_kernel(map_ref, before_ref, total_ref):
    count = map_ref.shape[0]
    hrow, hcol = iotas(CH, 2 * CH)
    before_ref[0] = jnp.where(hrow == hcol, 1.0, 0.0)
    running = map_ref[0]
    for q in range(1, count):
        before_ref[q] = running
        here = map_ref[q]
        running = mm(here[:, :CH], running) + jnp.where(hcol >= CH, here, 0.0)
    for z in range(total_ref.shape[0]):
        total_ref[z] = running


def entering_kernel(place_ref, total_ref, before_ref, out_ref):
    z_here = place_ref[0]
    core = place_ref[1]
    state = jnp.zeros((CH, CH), F32)
    for z in range(total_ref.shape[0] - 1):
        here = total_ref[z]
        state = jnp.where(z < z_here, mm(here[:, :CH], state) + here[:, CH:], state)
    half = CH // 2
    start = pl.multiple_of(core * half, half)
    count = before_ref.shape[0]
    rows = jnp.concatenate([before_ref[q, pl.ds(start, half), :] for q in range(count)], 0)
    mine = mm(rows[:, :CH], state) + rows[:, CH:]
    for q in range(count):
        part = mine[q * half : (q + 1) * half]
        out_ref[q] = jnp.concatenate([part[: half // 2], part[half // 2 :]], 1)


def finish_kernel(
    state_ref, read_ref, r_ref, k_ref, v_ref, c_ref, f_ref, mix_ref, cur_ref, gain_ref, bias_ref,
    out_ref,
):
    parts = []
    for h in range(read_ref.shape[0]):
        s = slice(h * CH, (h + 1) * CH)
        even, odd = state_ref[2 * h], state_ref[2 * h + 1]
        state = jnp.concatenate([even[:, :CH], even[:, CH:], odd[:, :CH], odd[:, CH:]], 0)
        reads = read_ref[h]
        readout = reads[:, CH:] + mm(reads[:, :CH], state)
        centred = readout - jnp.mean(readout, axis=1, keepdims=True)
        spread = jnp.mean(centred * centred, axis=1, keepdims=True)
        grouped = centred * lax.rsqrt(spread + GROUP_EPS) * gain_ref[:, s] + bias_ref[:, s]
        mixed = mixed_of(
            k_ref[:, s].astype(F32), sigmoid(c_ref[:, s].astype(F32)), mix_ref[:, s]
        )
        weight = r_ref[:, s].astype(F32) * mixed * cur_ref[:, s]
        bonus = jnp.sum(weight, axis=1, keepdims=True) * v_ref[:, s].astype(F32)
        parts.append((grouped + bonus) * f_ref[:, s].astype(F32))
    out_ref[...] = jnp.concatenate(parts, 1).astype(BF16)


def project_kernel(
    place_ref, token_ref, h0_ref, h1_ref, h2_ref, h3_ref, own_ref, near_ref, far_ref, residual_ref,
    gain_ref, out_ref, normed_ref, own_middle_ref, wide_ref, rows_ref,
):
    core = place_ref[1]
    tp = place_ref[2]
    acc = dot(h0_ref[...], own_ref[...])
    half = near_ref.shape[1]
    for k, ref in enumerate((h1_ref, h2_ref, h3_ref)):
        heads = ref[...]
        low, high = heads[:, :half], heads[:, half:]
        acc = acc + dot(jnp.where(core == 0, low, high), near_ref[k])
        acc = acc + dot(jnp.where(core == 0, high, low), far_ref[k])
    middle = (residual_ref[...].astype(F32) + acc).astype(BF16)
    full = middle.astype(F32)
    scale = lax.rsqrt(jnp.mean(full * full, axis=1, keepdims=True) + NORM_EPS)
    normed = (full * scale * gain_ref[...]).astype(BF16)
    normed_ref[...] = normed
    cols = own_middle_ref.shape[1]
    own = middle[:, :cols]
    for y in range(1, middle.shape[1] // cols):
        own = jnp.where(tp == y, middle[:, y * cols : (y + 1) * cols], own)
    own_middle_ref[...] = own
    tiles = normed.shape[1] // LANES
    wide = normed.astype(F32)
    for i in range(tiles):
        wide_ref[:, i, :] = wide[:, i * LANES : (i + 1) * LANES]
    rows_ref[...] = wide_ref[...].astype(BF16)
    dests = out_ref.shape[0] // (CAP * tiles)

    def send(i, carry):
        for m in range(CAP):
            token = jnp.maximum(token_ref[((i * 4 + tp) * CAP + m) * 4], 0)
            place = pl.multiple_of((i * CAP + m) * tiles, tiles)
            out_ref[pl.ds(place, tiles), :] = rows_ref[token]
        return carry

    lax.fori_loop(0, dests, send, 0)


def shared_kernel(place_ref, normed_ref, gate_ref, up_ref, down_ref, s0_ref, s1_ref, s2_ref, s3_ref):
    tp = place_ref[2]
    gate = dot(normed_ref[...], gate_ref[...])
    up = dot(normed_ref[...], up_ref[...])
    hidden = (gate * sigmoid(gate) * up).astype(BF16)
    cols = s0_ref.shape[1]
    for k, ref in enumerate((s0_ref, s1_ref, s2_ref, s3_ref)):
        start = pl.multiple_of(lax.rem(tp + k, 4) * cols, cols)
        ref[...] = dot(hidden, down_ref[:, pl.ds(start, cols)]).astype(ref.dtype)


def expert_kernel(
    rows_ref, gate_ref, up_ref, down_ref, out_ref, wide_ref, x_ref
):
    width = gate_ref.shape[0]
    tiles = width // LANES
    block = CAP * tiles
    sources = rows_ref.shape[0] // block

    def widen(i, carry):
        wide_ref[pl.ds(pl.multiple_of(i * PAD, 8), block), :] = rows_ref[
            pl.ds(pl.multiple_of(i * block, block), block), :
        ].astype(F32)
        return carry

    lax.fori_loop(0, sources, widen, 0)
    for m in range(CAP):
        for i in range(tiles):
            x_ref[m * sources : (m + 1) * sources, i * LANES : (i + 1) * LANES] = wide_ref[
                pl.ds(m * tiles + i, sources, stride=PAD), :
            ].astype(BF16)
    x = x_ref[...]
    gate = dot(x, gate_ref[...])
    up = dot(x, up_ref[...])
    hidden = (gate * sigmoid(gate) * up).astype(BF16)
    cols = width // 4
    for y in range(4):
        answer = dot(hidden, down_ref[:, y * cols : (y + 1) * cols])
        for m in range(CAP):
            for i in range(cols // LANES):
                wide_ref[pl.ds((y * CAP + m) * (cols // LANES) + i, sources, stride=PAD), :] = answer[
                    m * sources : (m + 1) * sources, i * LANES : (i + 1) * LANES
                ]

    def narrow(i, carry):
        out_ref[pl.ds(pl.multiple_of(i * block, block), block), :] = wide_ref[
            pl.ds(pl.multiple_of(i * PAD, 8), block), :
        ].astype(BF16)
        return carry

    lax.fori_loop(0, sources, narrow, 0)


def combine_kernel(
    back_ref, token_ref, weight_ref, middle_ref, s0_ref, s1_ref, s2_ref, s3_ref, out_ref
):
    tokens, cols = out_ref.shape
    tiles = cols // LANES
    chunk = 768
    sums = [jnp.zeros((tokens, LANES), F32) for _ in range(tiles)]
    token, lane = iotas(tokens, chunk)
    for j in range(back_ref.shape[0] // chunk):
        s = slice(j * chunk, (j + 1) * chunk)
        table = jnp.where(token_ref[:, s] == token, weight_ref[:, s], 0.0)
        rows = back_ref[s, :]
        for i in range(tiles):
            part = jnp.where(lane % tiles == i, table, 0.0).astype(BF16)
            sums[i] = sums[i] + dot(part, rows)
    total = middle_ref[...].astype(F32) + s0_ref[...] + s1_ref[...].astype(F32)
    total = total + s2_ref[...].astype(F32) + s3_ref[...].astype(F32)
    out_ref[...] = (total + jnp.concatenate(sums, 1)).astype(BF16)


def call(kernel, name, out, *args, scalars=0, scratch=()):
    smem = pl.BlockSpec(memory_space=pltpu.SMEM)
    vmem = pl.BlockSpec(memory_space=pltpu.VMEM)
    return pl.pallas_call(
        kernel,
        out_shape=out,
        in_specs=[smem] * scalars + [vmem] * (len(args) - scalars),
        out_specs=jax.tree.map(lambda _: vmem, out),
        scratch_shapes=list(scratch),
        name=name,
    )(*args)


def exchange(array, axes):
    return lax.all_to_all(array, axes, split_axis=0, concat_axis=0, tiled=True)


def turned(array, axis, shift):
    peers = lax.axis_size(axis)
    return lax.ppermute(array, axis, [(i, (i + shift) % peers) for i in range(peers)])


def per_device(
    receptance, key, value, decay, correction, factor, mix, current, gain, bias, output_matrix,
    residual, norm_gain, routes, chosen, routed_gate, routed_up, routed_down, common_gate,
    common_up, common_down,
):
    shape = jax.ShapeDtypeStruct
    tokens, inner = key.shape
    width = residual.shape[1]
    cols = width // 4
    heads = inner // CH
    z_count, plane = lax.axis_size("z"), lax.axis_size(PLANE)
    experts = lax.axis_size(EVERY)
    slots = lax.axis_size(SP) * CAP
    core = lax.axis_index("c")
    place = jnp.stack([lax.axis_index("z"), core, lax.axis_index("tp")]).astype(jnp.int32)
    mix, current, gain, bias = (a.reshape(1, -1) for a in (mix, current, gain, bias))

    half = inner // 2
    mine = lax.dynamic_slice_in_dim(output_matrix, core * half, half, 0)
    near = jnp.stack([turned(mine, "tp", k) for k in (1, 2, 3)])
    far = turned(near, "c", 1)

    table = (shape((experts, CAP * 4), jnp.int32), shape((experts, CAP * 4), F32))
    slot_token, slot_weight = call(routing_kernel, "routing", table, routes.T, chosen.T)
    slot_token = slot_token.reshape(-1)
    slot_weight = slot_weight.reshape(1, -1)

    maps, reads = call(
        local_kernel, "local_terms",
        (shape((2 * heads, CH, 2 * CH), F32), shape((heads, tokens, 2 * CH), F32)),
        receptance, key, value, decay, correction, mix,
    )
    maps = exchange(maps, PLANE)
    before, totals = call(
        plane_kernel, "plane_prefix",
        (shape((plane, CH, 2 * CH), F32), shape((z_count, CH, 2 * CH), F32)), maps,
    )
    totals = exchange(totals, "z")
    states = call(
        entering_kernel, "entering", shape((plane, CH // 4, 2 * CH), F32), place, totals, before,
        scalars=1,
    )
    states = exchange(states, PLANE)
    mixed = call(
        finish_kernel, "finish", shape((tokens, inner), BF16), states, reads, receptance, key,
        value, correction, factor, mix, current, gain, bias,
    )
    others = [turned(mixed, "tp", k) for k in (1, 2, 3)]
    outgoing, normed, own_middle = call(
        project_kernel, "project",
        (
            shape((slots * width // LANES, LANES), BF16),
            shape((tokens, width), BF16),
            shape((tokens, cols), BF16),
        ),
        place, slot_token, mixed, *others, output_matrix, near, far, residual,
        norm_gain.reshape(1, -1),
        scalars=2,
        scratch=(
            pltpu.VMEM((tokens, width // LANES, LANES), F32),
            pltpu.VMEM((tokens, width // LANES, LANES), BF16),
        ),
    )
    arrived = exchange(outgoing, SP)
    shared = call(
        shared_kernel, "shared",
        (shape((tokens, cols), F32),) + (shape((tokens, cols), BF16),) * 3,
        place, normed, common_gate, common_up, common_down, scalars=1,
    )
    shared = [shared[0]] + [turned(shared[k], "tp", k) for k in (1, 2, 3)]
    answer = call(
        expert_kernel, "expert", shape(outgoing.shape, BF16), arrived, routed_gate[0],
        routed_up[0], routed_down[0],
        scratch=(
            pltpu.VMEM((slots // CAP * PAD, LANES), F32),
            pltpu.VMEM((slots, width), BF16),
        ),
    )
    back = exchange(answer, EVERY)
    return call(
        combine_kernel, "combine", shape((tokens, cols), BF16), back, slot_token.reshape(1, -1),
        slot_weight, own_middle, *shared,
    )


def solution(mesh):
    finer = Mesh(mesh.devices.reshape(8, 4, 2, mesh.shape["tp"]), EVERY)
    placed = (
        (P(SP, "tp"),) * 6
        + (P("tp"),) * 4
        + (P("tp", None), P(SP, None), P(), P(SP, None), P(SP, None))
        + (P(EVERY, None, None),) * 3
        + (P(None, "tp"), P(None, "tp"), P("tp", None))
    )
    return jax.shard_map(
        per_device, mesh=finer, in_specs=placed, out_specs=P(SP, "tp"), check_vma=False
    )
```

time: 341 us -> 219 us (0.64)
  blocking collectives: 147 us -> 69.1 us
  matrix products: 48 us -> 0 us
  Pallas kernels: 0 us -> 44.3 us
  local copies, waits for them, and re-layouts: 49.8 us -> 7.28 us
  waiting for transfers between devices: 52.5 us -> 68.3 us
  between operations: 14.7 us -> 0.1 us
  starting transfers between devices: 16.1 us -> 28.2 us
  other arithmetic: 10.1 us -> 0.79 us
    all_gather x6 -> x0, blocking collectives: 75.7 us -> none  [carried_in(): pieces = jax.tree.map(lambda part: lax.all_gather(part, axis), total)]
    dot_general x57 -> x0, matrix products: 48 us -> none  [the longest x18 10.9 us: compose(): jnp.matmul(former[1], latter[0], precision=HIGHEST) + latter[1]]
    pallas_call x0 -> x9, Pallas kernels: none -> 44.3 us  [call(): pl.pallas_call(kernel, out_shape=out, in_specs=[smem] * scalars + [vmem]...]
    ppermute x0 -> x10, waiting for transfers between devices: none -> 33.5 us  [turned(): lax.ppermute(array, axis, [(i, (i + shift) % peers) for i in range(peers)])]
    all_to_all x3 -> x2, waiting for transfers between devices: 51.8 us -> 34.8 us  [exchange(): return lax.all_to_all(array, axes, split_axis=0, concat_axis=0, tiled=True)]
    reshape x11 -> x2, local copies, waits for them, and re-layouts: 17.1 us -> 2.35 us  [the longest x1 1.61 us: per_device(): slot_token = slot_token.reshape(-1)]
    ppermute x0 -> x10, starting transfers between devices: none -> 11.7 us  [turned(): lax.ppermute(array, axis, [(i, (i + shift) % peers) for i in range(peers)])]
    gather x4 -> x0, local copies, waits for them, and re-layouts: 10.4 us -> none  [the longest x3 7.24 us: per_device(): within = jnp.take_along_axis(earlier, target, axis=1)]
  transfers between devices with their start and end apart: 4 -> 12, of which waited for: 2 -> 6; matrix products, arithmetic and copies ran while one was open for 19% -> 2% of each run, Pallas kernels for 0% -> 11%
where the time goes in v1:
time: 219 us; the launch traced here: 218 us
  blocking collectives  69.1 us (32%)
  waiting for transfers between devices  68.3 us (31%)
  Pallas kernels  44.3 us (20%)
  starting transfers between devices  28.2 us (13%)
  local copies, waits for them, and re-layouts  7.28 us (3%)
    all_to_all x3, blocking collectives, exchange(): return lax.all_to_all(array, axes, split_axis=0, concat_axis=0, tiled=True)  69.1 us
    pallas_call x9, Pallas kernels, call(): pl.pallas_call(kernel, out_shape=out, in_specs=[smem] * scalars + [vmem]...  44.3 us
    all_to_all x2, waiting for transfers between devices, exchange(): return lax.all_to_all(array, axes, split_axis=0, concat_axis=0, tiled=True)  34.8 us
    ppermute x10, waiting for transfers between devices, turned(): lax.ppermute(array, axis, [(i, (i + shift) % peers) for i in range(peers)])  33.5 us
    all_to_all x2, starting transfers between devices, exchange(): return lax.all_to_all(array, axes, split_axis=0, concat_axis=0, tiled=True)  16.5 us
    ppermute x10, starting transfers between devices, turned(): lax.ppermute(array, axis, [(i, (i + shift) % peers) for i in range(peers)])  11.7 us
  transfers between devices with their start and end apart: 12, of which 6 were waited for; matrix products, arithmetic and copies ran while one was open for 2% of the time, Pallas kernels for 11%

profile of v1, /device:TPU:1, one launch (start us, length us, event | category | flops | bytes accessed | tf_op | source)
XLA Modules:
  0.0 218.1 jit_solution(1187414898263243428)
XLA Ops:
  0.0 1.1 constant_dynamic-slice_fusion
  1.1 3.6 %collective-permute-start.5 = (bf16[128,2048]{1,0:T(8,128)(2,1)S(1)}, bf16[128,2048]{1,0:T(8,128)(2,1)S(1)}, u32[]{:S(2)}, u32[]{:S(2)}) collective-permute-start(bf16[128,2048]{1,0:T(8,128)(2,1)S(1)} %constant_dynamic-slice_fusion), channel_id=1, source_target_pairs={{0,3},{1,0},{2,1},{3,2},{4,7},{5,4},{6,5},{7,6},{8,11},{9,8},{10,9... | collective-permute-start | bytes 1572872 | tf_op jit(solution)/shard_map/ppermute | solution.py:341
  4.7 0.3 collective-permute-start.4
  5.1 0.7 collective-permute-start.3
  5.8 20.7 %collective-permute-done.5 = bf16[128,2048]{1,0:T(8,128)(2,1)S(1)} collective-permute-done((bf16[128,2048]{1,0:T(8,128)(2,1)S(1)}, bf16[128,2048]{1,0:T(8,128)(2,1)S(1)}, u32[]{:S(2)}, u32[]{:S(2)}) %collective-permute-start.5) | collective-permute-done | bytes 524320 | tf_op jit(solution)/shard_map/ppermute | solution.py:341
  26.4 0.0 collective-permute-done.4
  26.4 4.9 %collective-permute-done.3 = bf16[128,2048]{1,0:T(8,128)(2,1)S(1)} collective-permute-done((bf16[128,2048]{1,0:T(8,128)(2,1)S(1)}, bf16[128,2048]{1,0:T(8,128)(2,1)S(1)}, u32[]{:S(2)}, u32[]{:S(2)}) %collective-permute-start.3) | collective-permute-done | bytes 524320 | tf_op jit(solution)/shard_map/ppermute | solution.py:341
  31.3 0.2 pad_maximum_fusion.near_ref
  31.5 0.0 copy-start.1
  31.5 0.6 collective-permute-start.6
  32.1 10.9 %local_terms.1 = (f32[8,64,128]{2,1,0:T(8,128)}, f32[4,128,128]{2,1,0:T(8,128)}) custom-call(bf16[128,256]{1,0:T(8,128)(2,1)} %r_ref.3, bf16[128,256]{1,0:T(8,128)(2,1)} %k_ref.3, bf16[128,256]{1,0:T(8,128)(2,1)} %v_ref.3, bf16[128,256]{1,0:T(8,128)(2,1)} %d_ref.1, bf16[128,256]{1,0:T(8,128)(2,1)} %c_ref.3, f32[1,256]{1,0:T(1,128)} %bitcast.31), custom_call_target="tpu_custom_call" | custom-call | tf_op jit(solution)/shard_map/local_terms/pallas_call | solution.py:325
  43.0 11.3 %all_to_all.37.map_ref = f32[8,64,128]{2,1,0:T(8,128)} all-to-all(f32[8,64,128]{2,1,0:T(8,128)} %get-tuple-element.19), channel_id=1, replica_groups=mesh['z'=8,'x'=4,'c'=2,'tp'=4] {'x','c'}, dimensions={0} | all-to-all | bytes 524288 | tf_op jit(solution)/shard_map/all_to_all | solution.py:336
  54.2 2.7 %plane_prefix.1 = (f32[8,64,128]{2,1,0:T(8,128)}, f32[8,64,128]{2,1,0:T(8,128)}) custom-call(f32[8,64,128]{2,1,0:T(8,128)} %all_to_all.37.map_ref), custom_call_target="tpu_custom_call" | custom-call | tf_op jit(solution)/shard_map/plane_prefix/pallas_call | solution.py:325
  56.9 8.2 %all-to-all-start.1 = ((f32[8,64,128]{2,1,0:T(8,128)}), f32[8,64,128]{2,1,0:T(8,128)S(1)}, u32[]{:S(2)}, u32[]{:S(2)}) async-start(f32[8,64,128]{2,1,0:T(8,128)} %get-tuple-element.20), calls=%async_computation.1 | async-start | bytes 524288 | tf_op jit(solution)/shard_map/all_to_all | solution.py:336
  65.1 0.6 pad_add_fusion.place_ref
  65.7 9.6 %all-to-all-done.1.total_ref = f32[8,64,128]{2,1,0:T(8,128)S(1)} async-done(((f32[8,64,128]{2,1,0:T(8,128)}), f32[8,64,128]{2,1,0:T(8,128)S(1)}, u32[]{:S(2)}, u32[]{:S(2)}) %all-to-all-start.1) | async-done | bytes 262176 | tf_op jit(solution)/shard_map/all_to_all | solution.py:336
  75.3 0.7 copy-done.3
  76.0 3.0 %entering.1 = f32[8,16,128]{2,1,0:T(8,128)} custom-call(s32[3]{0:T(128)} %pad_add_fusion.place_ref, f32[8,64,128]{2,1,0:T(8,128)} %copy-done.3, f32[8,64,128]{2,1,0:T(8,128)} %get-tuple-element.21.before_ref), custom_call_target="tpu_custom_call" | custom-call | tf_op jit(solution)/shard_map/entering/pallas_call | solution.py:325
  79.0 11.4 %all_to_all.38.state_ref = f32[8,16,128]{2,1,0:T(8,128)} all-to-all(f32[8,16,128]{2,1,0:T(8,128)} %entering.1), channel_id=1, replica_groups=mesh['z'=8,'x'=4,'c'=2,'tp'=4] {'x','c'}, dimensions={0} | all-to-all | bytes 131072 | tf_op jit(solution)/shard_map/all_to_all | solution.py:336
  90.4 2.9 %finish.1.h0_ref = bf16[128,256]{1,0:T(8,128)(2,1)} custom-call(f32[8,16,128]{2,1,0:T(8,128)} %all_to_all.38.state_ref, f32[4,128,128]{2,1,0:T(8,128)} %get-tuple-element.22.read_ref, bf16[128,256]{1,0:T(8,128)(2,1)} %r_ref.3, bf16[128,256]{1,0:T(8,128)(2,1)} %k_ref.3, bf16[128,256]{1,0:T(8,128)(2,1)} %v_ref.3, bf16[128,256]{1,0:T(8,128)(2,1)} %c_ref.3, ...), custom_call_target="tpu_custom_call" | custom-call | tf_op jit(solution)/shard_map/finish/pallas_call | solution.py:325
  93.3 0.3 collective-permute-start.2
  93.7 0.3 collective-permute-start.1
  94.0 0.8 collective-permute-start
  94.8 2.1 routing.1
  96.9 1.6 reshape.25.token_ref
  98.5 0.0 collective-permute-done.2.h3_ref
  98.5 0.0 collective-permute-done.1.h2_ref
  98.6 0.6 collective-permute-done.h1_ref
  99.2 0.0 collective-permute-done.6.far_ref
  99.2 0.6 copy-done.11
  99.8 0.5 copy-done.2
  100.4 7.2 %project.1 = (bf16[6144,128]{1,0:T(8,128)(2,1)}, bf16[128,2048]{1,0:T(8,128)(2,1)}, bf16[128,512]{1,0:T(8,128)(2,1)}) custom-call(s32[3]{0:T(128)} %pad_add_fusion.place_ref, s32[6144]{0:T(1024)} %reshape.25.token_ref, bf16[128,256]{1,0:T(8,128)(2,1)} %finish.1.h0_ref, bf16[128,256]{1,0:T(8,128)(2,1)} %copy-done.11, bf16[128,256]{1,0:T(8,128)(2,1)} %copy-done.10, ...), custom_call_target="tpu_custom_call" | custom-call | tf_op jit(solution)/shard_map/project/pallas_call | solution.py:325
  107.6 46.4 %all_to_all.39 = bf16[64,96,128]{2,1,0:T(8,128)(2,1)} all-to-all(bf16[64,96,128]{2,1,0:T(8,128)(2,1)} %bitcast.26), channel_id=1, replica_groups=mesh['z'=8,'x'=4,'c'=2,'tp'=4] {'z','x','c'}, dimensions={0} | all-to-all | bytes 3145728 | tf_op jit(solution)/shard_map/all_to_all | solution.py:336
  154.0 8.3 %expert.1 = bf16[6144,128]{1,0:T(8,128)(2,1)} custom-call(bf16[6144,128]{1,0:T(8,128)(2,1)} %bitcast.22, bf16[2048,512]{1,0:T(8,128)(2,1)} %bitcast.23, bf16[2048,512]{1,0:T(8,128)(2,1)} %bitcast.24, bf16[512,2048]{1,0:T(8,128)(2,1)} %bitcast.25), custom_call_target="tpu_custom_call" | custom-call | tf_op jit(solution)/shard_map/expert/pallas_call | solution.py:325
  162.4 8.4 %all-to-all-start.4 = ((bf16[256,24,128]{2,1,0:T(8,128)(2,1)}), bf16[256,24,128]{2,1,0:T(8,128)(2,1)S(1)}, u32[]{:S(2)}, u32[]{:S(2)}) async-start(bf16[256,24,128]{2,1,0:T(8,128)(2,1)} %bitcast.21), calls=%async_computation.4 | async-start | bytes 3145728 | tf_op jit(solution)/shard_map/all_to_all | solution.py:336
  170.7 0.0 copy-start.4
  170.8 3.0 %shared.1 = (f32[128,512]{1,0:T(8,128)}, bf16[128,512]{1,0:T(8,128)(2,1)}, bf16[128,512]{1,0:T(8,128)(2,1)}, bf16[128,512]{1,0:T(8,128)(2,1)}) custom-call(s32[3]{0:T(128)} %pad_add_fusion.place_ref, bf16[128,2048]{1,0:T(8,128)(2,1)} %get-tuple-element.26.normed_ref, bf16[2048,128]{1,0:T(8,128)(2,1)} %gate_ref.1, bf16[2048,128]{1,0:T(8,128)(2,1)} %up_ref.1, ...), custom_call_target="tpu_custom_call" | custom-call | tf_op jit(solution)/shard_map/shared/pallas_call | solution.py:325
  173.7 1.4 collective-permute-start.7
  175.1 2.5 %collective-permute-start.8 = (bf16[128,512]{1,0:T(8,128)(2,1)}, bf16[128,512]{1,0:T(8,128)(2,1)S(1)}, u32[]{:S(2)}, u32[]{:S(2)}) collective-permute-start(bf16[128,512]{1,0:T(8,128)(2,1)} %get-tuple-element.29), channel_id=1, source_target_pairs={{0,2},{1,3},{2,0},{3,1},{4,6},{5,7},{6,4},{7,5},{8,10},{9,11},{10,... | collective-permute-start | bytes 393224 | tf_op jit(solution)/shard_map/ppermute | solution.py:341
  177.5 1.1 collective-permute-start.9
  178.7 0.8 reshape_reshape.3.token_ref
  179.4 0.7 reshape.31.weight_ref
  180.2 0.0 collective-permute-done.7.s1_ref
  180.2 7.3 %collective-permute-done.8.s2_ref = bf16[128,512]{1,0:T(8,128)(2,1)S(1)} collective-permute-done((bf16[128,512]{1,0:T(8,128)(2,1)}, bf16[128,512]{1,0:T(8,128)(2,1)S(1)}, u32[]{:S(2)}, u32[]{:S(2)}) %collective-permute-start.8) | collective-permute-done | bytes 131104 | tf_op jit(solution)/shard_map/ppermute | solution.py:341
  187.5 0.0 collective-permute-done.9.s3_ref
  187.5 25.3 %all-to-all-done.4 = bf16[256,24,128]{2,1,0:T(8,128)(2,1)S(1)} async-done(((bf16[256,24,128]{2,1,0:T(8,128)(2,1)}), bf16[256,24,128]{2,1,0:T(8,128)(2,1)S(1)}, u32[]{:S(2)}, u32[]{:S(2)}) %all-to-all-start.4) | async-done | bytes 1572896 | tf_op jit(solution)/shard_map/all_to_all | solution.py:336
  212.8 1.2 copy-done
  214.0 4.2 %combine.1 = bf16[128,512]{1,0:T(8,128)(2,1)} custom-call(bf16[6144,128]{1,0:T(8,128)(2,1)} %bitcast.20, s32[1,6144]{1,0:T(1,128)} %reshape_reshape.3.token_ref, f32[1,6144]{1,0:T(1,128)} %reshape.31.weight_ref, bf16[128,512]{1,0:T(8,128)(2,1)} %get-tuple-element.25.middle_ref, f32[128,512]{1,0:T(8,128)} %get-tuple-element.27.s0_ref, ...), custom_call_target="tpu_custom_call" | custom-call | tf_op jit(solution)/shard_map/combine/pallas_call | solution.py:325
  (18 shorter events, 0.0 us)
Async XLA Ops:
  1.1 25.3 %collective-permute-start.5 = (bf16[128,2048]{1,0:T(8,128)(2,1)S(1)}, bf16[128,2048]{1,0:T(8,128)(2,1)S(1)}, u32[]{:S(2)}, u32[]{:S(2)}) collective-permute-start(bf16[128,2048]{1,0:T(8,128)(2,1)S(1)} %constant_dynamic-slice_fusion), channel_id=1, source_target_pairs={{0,3},{1,0},{2,1},{3,2},{4,7},{5,4},{6,5},{7,6},{8,11},{9,8},{10,9... | collective-permute-start | bytes 1572872 | tf_op jit(solution)/shard_map/ppermute | solution.py:341
  4.7 21.7 %collective-permute-start.4 = (bf16[128,2048]{1,0:T(8,128)(2,1)S(1)}, bf16[128,2048]{1,0:T(8,128)(2,1)S(1)}, u32[]{:S(2)}, u32[]{:S(2)}) collective-permute-start(bf16[128,2048]{1,0:T(8,128)(2,1)S(1)} %constant_dynamic-slice_fusion), channel_id=1, source_target_pairs={{0,2},{1,3},{2,0},{3,1},{4,6},{5,7},{6,4},{7,5},{8,10},{9,11},{10,... | collective-permute-start | bytes 1572872 | tf_op jit(solution)/shard_map/ppermute | solution.py:341
  5.1 26.2 %collective-permute-start.3 = (bf16[128,2048]{1,0:T(8,128)(2,1)S(1)}, bf16[128,2048]{1,0:T(8,128)(2,1)S(1)}, u32[]{:S(2)}, u32[]{:S(2)}) collective-permute-start(bf16[128,2048]{1,0:T(8,128)(2,1)S(1)} %constant_dynamic-slice_fusion), channel_id=1, source_target_pairs={{0,1},{1,2},{2,3},{3,0},{4,5},{5,6},{6,7},{7,4},{8,9},{9,10},{10,1... | collective-permute-start | bytes 1572872 | tf_op jit(solution)/shard_map/ppermute | solution.py:341
  31.5 67.1 %copy-start.1 = (bf16[3,128,2048]{2,1,0:T(8,128)(2,1)}, bf16[3,128,2048]{2,1,0:T(8,128)(2,1)S(1)}, u32[]{:S(2)}) copy-start(bf16[3,128,2048]{2,1,0:T(8,128)(2,1)S(1)} %pad_maximum_fusion.near_ref) | copy-start | bytes 4718596
  31.5 67.7 %collective-permute-start.6 = (bf16[3,128,2048]{2,1,0:T(8,128)(2,1)S(1)}, bf16[3,128,2048]{2,1,0:T(8,128)(2,1)S(1)}, u32[]{:S(2)}, u32[]{:S(2)}) collective-permute-start(bf16[3,128,2048]{2,1,0:T(8,128)(2,1)S(1)} %pad_maximum_fusion.near_ref), channel_id=1, source_target_pairs={{0,4},{4,0},{1,5},{5,1},{2,6},{6,2},{3,7},{7,3},{8,12},{12,8},{9,1... | collective-permute-start | bytes 4718600 | tf_op jit(solution)/shard_map/ppermute | solution.py:341
  56.9 18.4 %all-to-all-start.1 = ((f32[8,64,128]{2,1,0:T(8,128)}), f32[8,64,128]{2,1,0:T(8,128)S(1)}, u32[]{:S(2)}, u32[]{:S(2)}) async-start(f32[8,64,128]{2,1,0:T(8,128)} %get-tuple-element.20), calls=%async_computation.1 | async-start | bytes 524288 | tf_op jit(solution)/shard_map/all_to_all | solution.py:336
  75.3 0.7 copy-start.3
  93.3 5.2 %collective-permute-start.2 = (bf16[128,256]{1,0:T(8,128)(2,1)}, bf16[128,256]{1,0:T(8,128)(2,1)S(1)}, u32[]{:S(2)}, u32[]{:S(2)}) collective-permute-start(bf16[128,256]{1,0:T(8,128)(2,1)} %finish.1.h0_ref), channel_id=1, source_target_pairs={{0,3},{1,0},{2,1},{3,2},{4,7},{5,4},{6,5},{7,6},{8,11},{9,8},{10,9... | collective-permute-start | bytes 196616 | tf_op jit(solution)/shard_map/ppermute | solution.py:341
  93.7 4.9 %collective-permute-start.1 = (bf16[128,256]{1,0:T(8,128)(2,1)}, bf16[128,256]{1,0:T(8,128)(2,1)S(1)}, u32[]{:S(2)}, u32[]{:S(2)}) collective-permute-start(bf16[128,256]{1,0:T(8,128)(2,1)} %finish.1.h0_ref), channel_id=1, source_target_pairs={{0,2},{1,3},{2,0},{3,1},{4,6},{5,7},{6,4},{7,5},{8,10},{9,11},{10,... | collective-permute-start | bytes 196616 | tf_op jit(solution)/shard_map/ppermute | solution.py:341
  94.0 5.2 %collective-permute-start = (bf16[128,256]{1,0:T(8,128)(2,1)}, bf16[128,256]{1,0:T(8,128)(2,1)S(1)}, u32[]{:S(2)}, u32[]{:S(2)}) collective-permute-start(bf16[128,256]{1,0:T(8,128)(2,1)} %finish.1.h0_ref), channel_id=1, source_target_pairs={{0,1},{1,2},{2,3},{3,0},{4,5},{5,6},{6,7},{7,4},{8,9},{9,10},{10,1... | collective-permute-start | bytes 196616 | tf_op jit(solution)/shard_map/ppermute | solution.py:341
  98.5 0.7 copy-start.9
  98.6 0.7 copy-start.10
  99.2 0.6 copy-start.11
  99.2 1.2 copy-start.2
  162.4 50.4 %all-to-all-start.4 = ((bf16[256,24,128]{2,1,0:T(8,128)(2,1)}), bf16[256,24,128]{2,1,0:T(8,128)(2,1)S(1)}, u32[]{:S(2)}, u32[]{:S(2)}) async-start(bf16[256,24,128]{2,1,0:T(8,128)(2,1)} %bitcast.21), calls=%async_computation.4 | async-start | bytes 3145728 | tf_op jit(solution)/shard_map/all_to_all | solution.py:336
  170.7 7.9 %copy-start.4 = (s32[256,24]{1,0:T(8,128)S(1)}, s32[256,24]{1,0:T(8,128)}, u32[]{:S(2)}) copy-start(s32[256,24]{1,0:T(8,128)} %get-tuple-element.18) | copy-start | bytes 73732
  170.7 8.7 %copy-start.8 = (f32[256,24]{1,0:T(8,128)S(1)}, f32[256,24]{1,0:T(8,128)}, u32[]{:S(2)}) copy-start(f32[256,24]{1,0:T(8,128)} %get-tuple-element.24) | copy-start | bytes 73732
  173.7 6.4 %collective-permute-start.7 = (bf16[128,512]{1,0:T(8,128)(2,1)}, bf16[128,512]{1,0:T(8,128)(2,1)S(1)}, u32[]{:S(2)}, u32[]{:S(2)}) collective-permute-start(bf16[128,512]{1,0:T(8,128)(2,1)} %get-tuple-element.28), channel_id=1, source_target_pairs={{0,1},{1,2},{2,3},{3,0},{4,5},{5,6},{6,7},{7,4},{8,9},{9,10},{10,1... | collective-permute-start | bytes 393224 | tf_op jit(solution)/shard_map/ppermute | solution.py:341
  175.1 12.4 %collective-permute-start.8 = (bf16[128,512]{1,0:T(8,128)(2,1)}, bf16[128,512]{1,0:T(8,128)(2,1)S(1)}, u32[]{:S(2)}, u32[]{:S(2)}) collective-permute-start(bf16[128,512]{1,0:T(8,128)(2,1)} %get-tuple-element.29), channel_id=1, source_target_pairs={{0,2},{1,3},{2,0},{3,1},{4,6},{5,7},{6,4},{7,5},{8,10},{9,11},{10,... | collective-permute-start | bytes 393224 | tf_op jit(solution)/shard_map/ppermute | solution.py:341
  177.5 9.9 %collective-permute-start.9 = (bf16[128,512]{1,0:T(8,128)(2,1)}, bf16[128,512]{1,0:T(8,128)(2,1)S(1)}, u32[]{:S(2)}, u32[]{:S(2)}) collective-permute-start(bf16[128,512]{1,0:T(8,128)(2,1)} %get-tuple-element.30), channel_id=1, source_target_pairs={{0,3},{1,0},{2,1},{3,2},{4,7},{5,4},{6,5},{7,6},{8,11},{9,8},{10,9... | collective-permute-start | bytes 393224 | tf_op jit(solution)/shard_map/ppermute | solution.py:341
  180.2 32.6 %copy-start.5 = (bf16[128,512]{1,0:T(8,128)(2,1)}, bf16[128,512]{1,0:T(8,128)(2,1)S(1)}, u32[]{:S(2)}) copy-start(bf16[128,512]{1,0:T(8,128)(2,1)S(1)} %collective-permute-done.7.s1_ref) | copy-start | bytes 393220
  187.5 25.3 %copy-start.6 = (bf16[128,512]{1,0:T(8,128)(2,1)}, bf16[128,512]{1,0:T(8,128)(2,1)S(1)}, u32[]{:S(2)}) copy-start(bf16[128,512]{1,0:T(8,128)(2,1)S(1)} %collective-permute-done.8.s2_ref) | copy-start | bytes 393220
  187.5 25.3 %copy-start.7 = (bf16[128,512]{1,0:T(8,128)(2,1)}, bf16[128,512]{1,0:T(8,128)(2,1)S(1)}, u32[]{:S(2)}) copy-start(bf16[128,512]{1,0:T(8,128)(2,1)S(1)} %collective-permute-done.9.s3_ref) | copy-start | bytes 393220
  212.8 1.2 copy-start

commit v2 on v1

--- a/solution.py
+++ b/solution.py
@@ -50,22 +50,25 @@
     return 1.0 / (1.0 + jnp.exp(-x))
 
 
-def unit_inverse(low):
-    n = low.shape[0]
+def unit_inverses(lows):
+    n = lows[0].shape[0]
     row, col = iotas(n, n)
     size = 8
-    power = jnp.where((row // size) == (col // size), low, 0.0)
-    x = jnp.where(row == col, 1.0, 0.0) + power
+    eye = jnp.where(row == col, 1.0, 0.0)
+    inside = (row // size) == (col // size)
+    powers = [jnp.where(inside, low, 0.0) for low in lows]
+    xs = [eye + power for power in powers]
     span = 2
     while span < size:
-        power = mm(power, power)
-        x = x + mm(x, power)
+        powers = [mm(power, power) for power in powers]
+        xs = [x + mm(x, power) for x, power in zip(xs, powers)]
         span *= 2
     while size < n:
         part = ((row // (2 * size)) == (col // (2 * size))) & ((row // size) != (col // size))
-        x = x + mm(mm(x, jnp.where(part, low, 0.0)), x)
+        lefts = [mm(x, jnp.where(part, low, 0.0)) for x, low in zip(xs, lows)]
+        xs = [x + mm(left, x) for x, left in zip(xs, lefts)]
         size *= 2
-    return x
+    return xs
 
 
 def mixed_of(key, learning, mix):
@@ -132,47 +135,78 @@
     strict = row > col
     inclusive = row >= col
     hrow, hcol = iotas(CH, CH)
-    for h in range(w // CH):
-        s = slice(h * CH, (h + 1) * CH)
-        b, q, v = before[:, s], read[:, s], value[:, s]
-        pairs = mm(
-            jnp.concatenate([b, q], 0), jnp.concatenate([erase[:, s], write[:, s]], 0), NT
+    every = range(w // CH)
+
+    def parts(array):
+        return [array[:, h * CH : (h + 1) * CH] for h in every]
+
+    befores, asked, values = parts(before), parts(read), parts(value)
+    pairs = [
+        mm(jnp.concatenate([b, q], 0), jnp.concatenate([e, x], 0), NT)
+        for b, q, e, x in zip(befores, asked, parts(erase), parts(write))
+    ]
+    lows = [jnp.where(strict, p[:t, :t], 0.0) for p in pairs]
+    stacks = [
+        jnp.concatenate(
+            [jnp.where(strict, p[:t, t:], 0.0), jnp.where(inclusive, p[t:, t:], 0.0)], 0
         )
-        low = jnp.where(strict, pairs[:t, :t], 0.0)
-        wrote = jnp.where(strict, pairs[:t, t:], 0.0)
-        read_erase = jnp.where(inclusive, pairs[t:, :t], 0.0)
-        read_write = jnp.where(inclusive, pairs[t:, t:], 0.0)
-        x = unit_inverse(low)
-        on_values = mm(jnp.concatenate([wrote, read_write], 0), v)
-        solved = mm(x, jnp.concatenate([b, on_values[:t]], 1))
-        read_ref[h] = jnp.concatenate([q, on_values[t:]], 1) + mm(read_erase, solved)
-        diagonal = jnp.where(hrow == hcol, jnp.broadcast_to(final[:, s], (CH, CH)), 0.0)
-        state = jnp.concatenate([diagonal, mm(write_end[:, s], v, TN)], 1)
-        state = state + mm(erase_end[:, s], solved, TN)
+        for p in pairs
+    ]
+    on_values = [mm(stack, v) for stack, v in zip(stacks, values)]
+    written = [mm(e, v, TN) for e, v in zip(parts(write_end), values)]
+    xs = unit_inverses(lows)
+    solved = [
+        mm(x, jnp.concatenate([b, o[:t]], 1)) for x, b, o in zip(xs, befores, on_values)
+    ]
+    states = [mm(e, z, TN) for e, z in zip(parts(erase_end), solved)]
+    reads = [mm(jnp.where(inclusive, p[t:, :t], 0.0), z) for p, z in zip(pairs, solved)]
+    for h, f in zip(every, parts(final)):
+        diagonal = jnp.where(hrow == hcol, jnp.broadcast_to(f, (CH, CH)), 0.0)
+        state = states[h] + jnp.concatenate([diagonal, written[h]], 1)
         map_ref[2 * h] = state
         map_ref[2 * h + 1] = state
+        read_ref[h] = reads[h] + jnp.concatenate([asked[h], on_values[h][t:]], 1)
+
+
+def joined(former, latter, late):
+    return mm(latter[:, :CH], former) + jnp.where(late, latter, 0.0)
 
 
 def plane_kernel(map_ref, before_ref, total_ref):
     count = map_ref.shape[0]
     hrow, hcol = iotas(CH, 2 * CH)
+    late = hcol >= CH
+    maps = [map_ref[q] for q in range(count)]
+    span = 1
+    while span < count:
+        maps = [
+            maps[q] if q < span else joined(maps[q - span], maps[q], late) for q in range(count)
+        ]
+        span *= 2
     before_ref[0] = jnp.where(hrow == hcol, 1.0, 0.0)
-    running = map_ref[0]
     for q in range(1, count):
-        before_ref[q] = running
-        here = map_ref[q]
-        running = mm(here[:, :CH], running) + jnp.where(hcol >= CH, here, 0.0)
-    for z in range(total_ref.shape[0]):
-        total_ref[z] = running
-
-
-def entering_kernel(place_ref, total_ref, before_ref, out_ref):
+        before_ref[q] = maps[q - 1]
+    total_ref[...] = maps[count - 1]
+
+
+def entering_kernel(place_ref, before_ref, *refs):
+    *earlier_refs, out_ref = refs
     z_here = place_ref[0]
     core = place_ref[1]
-    state = jnp.zeros((CH, CH), F32)
-    for z in range(total_ref.shape[0] - 1):
-        here = total_ref[z]
-        state = jnp.where(z < z_here, mm(here[:, :CH], state) + here[:, CH:], state)
+    hrow, hcol = iotas(CH, 2 * CH)
+    late = hcol >= CH
+    nothing = jnp.where(hrow == hcol, 1.0, 0.0)
+    maps = [
+        jnp.where(z_here >= k, earlier_refs[k - 1][...], nothing)
+        for k in range(len(earlier_refs), 0, -1)
+    ]
+    while len(maps) > 1:
+        odd = maps[:1] if len(maps) % 2 else []
+        rest = maps[len(odd) :]
+        maps = odd + [
+            joined(rest[i], rest[i + 1], late) for i in range(0, len(rest), 2)
+        ]
+    state = maps[0][:, CH:]
     half = CH // 2
     start = pl.multiple_of(core * half, half)
     count = before_ref.shape[0]
@@ -187,38 +221,59 @@
     state_ref, read_ref, r_ref, k_ref, v_ref, c_ref, f_ref, mix_ref, cur_ref, gain_ref, bias_ref,
     out_ref,
 ):
-    parts = []
-    for h in range(read_ref.shape[0]):
-        s = slice(h * CH, (h + 1) * CH)
+    every = range(read_ref.shape[0])
+    slices = [slice(h * CH, (h + 1) * CH) for h in every]
+    mixed = mixed_of(k_ref[...].astype(F32), sigmoid(c_ref[...].astype(F32)), mix_ref[...])
+    weight = r_ref[...].astype(F32) * mixed * cur_ref[...]
+    readouts = []
+    for h in every:
         even, odd = state_ref[2 * h], state_ref[2 * h + 1]
         state = jnp.concatenate([even[:, :CH], even[:, CH:], odd[:, :CH], odd[:, CH:]], 0)
         reads = read_ref[h]
-        readout = reads[:, CH:] + mm(reads[:, :CH], state)
-        centred = readout - jnp.mean(readout, axis=1, keepdims=True)
-        spread = jnp.mean(centred * centred, axis=1, keepdims=True)
-        grouped = centred * lax.rsqrt(spread + GROUP_EPS) * gain_ref[:, s] + bias_ref[:, s]
-        mixed = mixed_of(
-            k_ref[:, s].astype(F32), sigmoid(c_ref[:, s].astype(F32)), mix_ref[:, s]
-        )
-        weight = r_ref[:, s].astype(F32) * mixed * cur_ref[:, s]
-        bonus = jnp.sum(weight, axis=1, keepdims=True) * v_ref[:, s].astype(F32)
-        parts.append((grouped + bonus) * f_ref[:, s].astype(F32))
-    out_ref[...] = jnp.concatenate(parts, 1).astype(BF16)
+        readouts.append(reads[:, CH:] + mm(reads[:, :CH], state))
+    bonuses = [jnp.sum(weight[:, s], axis=1, keepdims=True) for s in slices]
+    means = [jnp.mean(readout, axis=1, keepdims=True) for readout in readouts]
+    centred = [readout - mean for readout, mean in zip(readouts, means)]
+    spreads = [jnp.mean(c * c, axis=1, keepdims=True) for c in centred]
+    scaled = [c * lax.rsqrt(spread + GROUP_EPS) for c, spread in zip(centred, spreads)]
+    wide = (readouts[0].shape[0], CH)
+    bonus = jnp.concatenate([jnp.broadcast_to(b, wide) for b in bonuses], 1)
+    grouped = jnp.concatenate(scaled, 1) * gain_ref[...] + bias_ref[...]
+    out = (grouped + bonus * v_ref[...].astype(F32)) * f_ref[...].astype(F32)
+    out_ref[...] = out.astype(BF16)
+
+
+def fetch(sources, targets, sems):
+    copies = [
+        pltpu.make_async_copy(source, target, sems.at[i])
+        for i, (source, target) in enumerate(zip(sources, targets))
+    ]
+    for copy in copies:
+        copy.start()
+    return copies
 
 
 def project_kernel(
-    place_ref, token_ref, h0_ref, h1_ref, h2_ref, h3_ref, own_ref, near_ref, far_ref, residual_ref,
-    gain_ref, out_ref, normed_ref, own_middle_ref, wide_ref, rows_ref,
+    place_ref, token_ref, h0_ref, h1_ref, h2_ref, h3_ref, gain_ref, own_hbm, near_hbm, far_hbm,
+    residual_hbm, out_ref, normed_ref, own_middle_ref, own_ref, near_ref, far_ref, residual_ref,
+    wide_ref, rows_ref, sems,
 ):
     core = place_ref[1]
     tp = place_ref[2]
+    copies = fetch(
+        (own_hbm, near_hbm, far_hbm, residual_hbm), (own_ref, near_ref, far_ref, residual_ref), sems
+    )
+    copies[0].wait()
     acc = dot(h0_ref[...], own_ref[...])
     half = near_ref.shape[1]
-    for k, ref in enumerate((h1_ref, h2_ref, h3_ref)):
-        heads = ref[...]
-        low, high = heads[:, :half], heads[:, half:]
-        acc = acc + dot(jnp.where(core == 0, low, high), near_ref[k])
-        acc = acc + dot(jnp.where(core == 0, high, low), far_ref[k])
+    heads = [ref[...] for ref in (h1_ref, h2_ref, h3_ref)]
+    copies[1].wait()
+    for k, head in enumerate(heads):
+        acc = acc + dot(jnp.where(core == 0, head[:, :half], head[:, half:]), near_ref[k])
+    copies[2].wait()
+    for k, head in enumerate(heads):
+        acc = acc + dot(jnp.where(core == 0, head[:, half:], head[:, :half]), far_ref[k])
+    copies[3].wait()
     middle = (residual_ref[...].astype(F32) + acc).astype(BF16)
     full = middle.astype(F32)
     scale = lax.rsqrt(jnp.mean(full * full, axis=1, keepdims=True) + NORM_EPS)
@@ -233,17 +288,17 @@
     wide = normed.astype(F32)
     for i in range(tiles):
         wide_ref[:, i, :] = wide[:, i * LANES : (i + 1) * LANES]
-    rows_ref[...] = wide_ref[...].astype(BF16)
+    rows_ref[...] = wide_ref[:, :tiles, :].astype(BF16)
     dests = out_ref.shape[0] // (CAP * tiles)
 
     def send(i, carry):
         for m in range(CAP):
-            token = jnp.maximum(token_ref[((i * 4 + tp) * CAP + m) * 4], 0)
+            token = jnp.maximum(token_ref[(i * 4 + tp) * CAP + m], 0)
             place = pl.multiple_of((i * CAP + m) * tiles, tiles)
             out_ref[pl.ds(place, tiles), :] = rows_ref[token]
         return carry
 
-    lax.fori_loop(0, dests, send, 0)
+    lax.fori_loop(0, dests, send, 0, unroll=4)
 
 
 def shared_kernel(place_ref, normed_ref, gate_ref, up_ref, down_ref, s0_ref, s1_ref, s2_ref, s3_ref):
@@ -258,8 +313,9 @@
 
 
 def expert_kernel(
-    rows_ref, gate_ref, up_ref, down_ref, out_ref, wide_ref, x_ref
+    rows_ref, gate_hbm, up_hbm, down_hbm, out_ref, gate_ref, up_ref, down_ref, wide_ref, x_ref, sems
 ):
+    copies = fetch((gate_hbm, up_hbm, down_hbm), (gate_ref, up_ref, down_ref), sems)
     width = gate_ref.shape[0]
     tiles = width // LANES
     block = CAP * tiles
@@ -271,22 +327,26 @@
         ].astype(F32)
         return carry
 
-    lax.fori_loop(0, sources, widen, 0)
+    lax.fori_loop(0, sources, widen, 0, unroll=4)
     for m in range(CAP):
         for i in range(tiles):
             x_ref[m * sources : (m + 1) * sources, i * LANES : (i + 1) * LANES] = wide_ref[
                 pl.ds(m * tiles + i, sources, stride=PAD), :
             ].astype(BF16)
     x = x_ref[...]
+    copies[0].wait()
     gate = dot(x, gate_ref[...])
+    copies[1].wait()
     up = dot(x, up_ref[...])
     hidden = (gate * sigmoid(gate) * up).astype(BF16)
     cols = width // 4
+    copies[2].wait()
     for y in range(4):
         answer = dot(hidden, down_ref[:, y * cols : (y + 1) * cols])
         for m in range(CAP):
             for i in range(cols // LANES):
-                wide_ref[pl.ds((y * CAP + m) * (cols // LANES) + i, sources, stride=PAD), :] = answer[
+                place = (y * CAP + m) * (cols // LANES) + i
+                wide_ref[pl.ds(place, sources, stride=PAD), :] = answer[
                     m * sources : (m + 1) * sources, i * LANES : (i + 1) * LANES
                 ]
 
@@ -296,38 +356,41 @@
         ].astype(BF16)
         return carry
 
-    lax.fori_loop(0, sources, narrow, 0)
+    lax.fori_loop(0, sources, narrow, 0, unroll=4)
 
 
 def combine_kernel(
-    back_ref, token_ref, weight_ref, middle_ref, s0_ref, s1_ref, s2_ref, s3_ref, out_ref
+    back_ref, token_ref, weight_ref, middle_ref, s0_ref, s1_ref, s2_ref, s3_ref, out_ref, wide_ref
 ):
     tokens, cols = out_ref.shape
     tiles = cols // LANES
-    chunk = 768
-    sums = [jnp.zeros((tokens, LANES), F32) for _ in range(tiles)]
-    token, lane = iotas(tokens, chunk)
-    for j in range(back_ref.shape[0] // chunk):
-        s = slice(j * chunk, (j + 1) * chunk)
-        table = jnp.where(token_ref[:, s] == token, weight_ref[:, s], 0.0)
-        rows = back_ref[s, :]
-        for i in range(tiles):
-            part = jnp.where(lane % tiles == i, table, 0.0).astype(BF16)
-            sums[i] = sums[i] + dot(part, rows)
+    slots = back_ref.shape[0] // tiles
+    wide_ref[...] = back_ref[...].astype(F32)
+    token, _ = iotas(tokens, slots)
+    table = jnp.where(token_ref[...] == token, weight_ref[...], 0.0).astype(BF16)
+    rows = jnp.concatenate(
+        [wide_ref[pl.ds(i, slots, stride=tiles), :].astype(BF16) for i in range(tiles)], 1
+    )
     total = middle_ref[...].astype(F32) + s0_ref[...] + s1_ref[...].astype(F32)
     total = total + s2_ref[...].astype(F32) + s3_ref[...].astype(F32)
-    out_ref[...] = (total + jnp.concatenate(sums, 1)).astype(BF16)
-
-
-def call(kernel, name, out, *args, scalars=0, scratch=()):
+    out_ref[...] = (total + dot(table, rows)).astype(BF16)
+
+
+def call(kernel, name, out, *args, scalars=0, fetched=0, scratch=()):
     smem = pl.BlockSpec(memory_space=pltpu.SMEM)
     vmem = pl.BlockSpec(memory_space=pltpu.VMEM)
+    hbm = pl.BlockSpec(memory_space=pl.ANY)
+    loaded = len(args) - scalars - fetched
+    scratch = list(scratch)
+    if fetched:
+        scratch = [pltpu.VMEM(a.shape, a.dtype) for a in args[-fetched:]] + scratch
+        scratch.append(pltpu.SemaphoreType.DMA((fetched,)))
     return pl.pallas_call(
         kernel,
         out_shape=out,
-        in_specs=[smem] * scalars + [vmem] * (len(args) - scalars),
+        in_specs=[smem] * scalars + [vmem] * loaded + [hbm] * fetched,
         out_specs=jax.tree.map(lambda _: vmem, out),
-        scratch_shapes=list(scratch),
+        scratch_shapes=scratch,
         name=name,
     )(*args)
 
@@ -360,10 +423,9 @@
 
     half = inner // 2
     mine = lax.dynamic_slice_in_dim(output_matrix, core * half, half, 0)
-    near = jnp.stack([turned(mine, "tp", k) for k in (1, 2, 3)])
-    far = turned(near, "c", 1)
-
-    table = (shape((experts, CAP * 4), jnp.int32), shape((experts, CAP * 4), F32))
+    near = [turned(mine, "tp", k) for k in (1, 2, 3)]
+
+    table = (shape((experts, CAP), jnp.int32), shape((experts, CAP), F32))
     slot_token, slot_weight = call(routing_kernel, "routing", table, routes.T, chosen.T)
     slot_token = slot_token.reshape(-1)
     slot_weight = slot_weight.reshape(1, -1)
@@ -374,15 +436,18 @@
         receptance, key, value, decay, correction, mix,
     )
     maps = exchange(maps, PLANE)
-    before, totals = call(
+    before, total = call(
         plane_kernel, "plane_prefix",
-        (shape((plane, CH, 2 * CH), F32), shape((z_count, CH, 2 * CH), F32)), maps,
-    )
-    totals = exchange(totals, "z")
+        (shape((plane, CH, 2 * CH), F32), shape((CH, 2 * CH), F32)), maps,
+    )
+    earlier = [turned(total, "z", k) for k in range(1, z_count)]
     states = call(
-        entering_kernel, "entering", shape((plane, CH // 4, 2 * CH), F32), place, totals, before,
+        entering_kernel, "entering", shape((plane, CH // 4, 2 * CH), F32), place, before, *earlier,
         scalars=1,
     )
+    states, *near = lax.optimization_barrier((states, *near))
+    near = jnp.stack(near)
+    far = turned(near, "c", 1)
     states = exchange(states, PLANE)
     mixed = call(
         finish_kernel, "finish", shape((tokens, inner), BF16), states, reads, receptance, key,
@@ -396,11 +461,12 @@
             shape((tokens, width), BF16),
             shape((tokens, cols), BF16),
         ),
-        place, slot_token, mixed, *others, output_matrix, near, far, residual,
-        norm_gain.reshape(1, -1),
+        place, slot_token, mixed, *others, norm_gain.reshape(1, -1), output_matrix, near, far,
+        residual,
         scalars=2,
+        fetched=4,
         scratch=(
-            pltpu.VMEM((tokens, width // LANES, LANES), F32),
+            pltpu.VMEM((tokens, width // LANES + 8, LANES), F32),
             pltpu.VMEM((tokens, width // LANES, LANES), BF16),
         ),
     )
@@ -414,6 +480,7 @@
     answer = call(
         expert_kernel, "expert", shape(outgoing.shape, BF16), arrived, routed_gate[0],
         routed_up[0], routed_down[0],
+        fetched=3,
         scratch=(
             pltpu.VMEM((slots // CAP * PAD, LANES), F32),
             pltpu.VMEM((slots, width), BF16),
@@ -423,6 +490,7 @@
     return call(
         combine_kernel, "combine", shape((tokens, cols), BF16), back, slot_token.reshape(1, -1),
         slot_weight, own_middle, *shared,
+        scratch=(pltpu.VMEM(back.shape, F32),),
     )
 
 

time: 219 us -> 194 us (0.89)
  waiting for transfers between devices: 68.3 us -> 38.3 us
  starting transfers between devices: 28.2 us -> 43.6 us
  Pallas kernels: 44.3 us -> 35.9 us
    ppermute x10 -> x17, starting transfers between devices: 11.7 us -> 36.4 us  [turned(): lax.ppermute(array, axis, [(i, (i + shift) % peers) for i in range(peers)])]
    ppermute x10 -> x17, waiting for transfers between devices: 33.5 us -> 13.1 us  [turned(): lax.ppermute(array, axis, [(i, (i + shift) % peers) for i in range(peers)])]
    all_to_all x2 -> x1, waiting for transfers between devices: 34.8 us -> 25.2 us  [exchange(): return lax.all_to_all(array, axes, split_axis=0, concat_axis=0, tiled=True)]
    all_to_all x2 -> x1, starting transfers between devices: 16.5 us -> 7.23 us  [exchange(): return lax.all_to_all(array, axes, split_axis=0, concat_axis=0, tiled=True)]
    pallas_call x9, Pallas kernels: 44.3 us -> 35.9 us  [call(): pl.pallas_call(kernel, out_shape=out, in_specs=[smem] * scalars + [vmem]...]
  transfers between devices with their start and end apart: 12 -> 18, of which waited for: 6 -> 7; matrix products, arithmetic and copies ran while one was open for 2% -> 2% of each run, Pallas kernels for 11% -> 9%
where the time goes in v2:
time: 194 us
  blocking collectives  67.8 us (35%)
  starting transfers between devices  43.6 us (22%)
  waiting for transfers between devices  38.3 us (20%)
  Pallas kernels  35.9 us (19%)
  local copies, waits for them, and re-layouts  7.1 us (4%)
    all_to_all x3, blocking collectives, exchange(): return lax.all_to_all(array, axes, split_axis=0, concat_axis=0, tiled=True)  67.8 us
    ppermute x17, starting transfers between devices, turned(): lax.ppermute(array, axis, [(i, (i + shift) % peers) for i in range(peers)])  36.4 us
    pallas_call x9, Pallas kernels, call(): pl.pallas_call(kernel, out_shape=out, in_specs=[smem] * scalars + [vmem]...  35.9 us
    all_to_all x1, waiting for transfers between devices, exchange(): return lax.all_to_all(array, axes, split_axis=0, concat_axis=0, tiled=True)  25.2 us
    ppermute x17, waiting for transfers between devices, turned(): lax.ppermute(array, axis, [(i, (i + shift) % peers) for i in range(peers)])  13.1 us
    all_to_all x1, starting transfers between devices, exchange(): return lax.all_to_all(array, axes, split_axis=0, concat_axis=0, tiled=True)  7.23 us
  transfers between devices with their start and end apart: 18, of which 7 were waited for; matrix products, arithmetic and copies ran while one was open for 2% of the time, Pallas kernels for 9%

profile of v2, /device:TPU:1, one launch (start us, length us, event | category | flops | bytes accessed | tf_op | source)
XLA Modules:
  0.0 193.7 jit_solution(806328843486583126)
XLA Ops:
  0.0 1.1 constant_dynamic-slice_fusion
  1.1 3.6 %collective-permute-start.9 = (bf16[128,2048]{1,0:T(8,128)(2,1)S(1)}, bf16[128,2048]{1,0:T(8,128)(2,1)S(1)}, u32[]{:S(2)}, u32[]{:S(2)}) collective-permute-start(bf16[128,2048]{1,0:T(8,128)(2,1)S(1)} %constant_dynamic-slice_fusion), channel_id=1, source_target_pairs={{0,3},{1,0},{2,1},{3,2},{4,7},{5,4},{6,5},{7,6},{8,11},{9,8},{10,9... | collective-permute-start | bytes 1572872 | tf_op jit(solution)/shard_map/ppermute | solution.py:404
  4.7 0.3 collective-permute-start.8
  5.1 0.7 collective-permute-start.7
  5.8 5.2 %local_terms.1 = (f32[8,64,128]{2,1,0:T(8,128)}, f32[4,128,128]{2,1,0:T(8,128)}) custom-call(bf16[128,256]{1,0:T(8,128)(2,1)} %r_ref.3, bf16[128,256]{1,0:T(8,128)(2,1)} %k_ref.3, bf16[128,256]{1,0:T(8,128)(2,1)} %v_ref.3, bf16[128,256]{1,0:T(8,128)(2,1)} %d_ref.1, bf16[128,256]{1,0:T(8,128)(2,1)} %c_ref.3, f32[1,256]{1,0:T(1,128)} %bitcast.31), custom_call_target="tpu_custom_call" | custom-call | tf_op jit(solution)/shard_map/local_terms/pallas_call | solution.py:388
  11.0 12.4 %all_to_all.32.map_ref = f32[8,64,128]{2,1,0:T(8,128)} all-to-all(f32[8,64,128]{2,1,0:T(8,128)} %get-tuple-element.23), channel_id=1, replica_groups=mesh['z'=8,'x'=4,'c'=2,'tp'=4] {'x','c'}, dimensions={0} | all-to-all | bytes 524288 | tf_op jit(solution)/shard_map/all_to_all | solution.py:399
  23.3 2.2 %plane_prefix.1 = (f32[8,64,128]{2,1,0:T(8,128)}, f32[64,128]{1,0:T(8,128)}) custom-call(f32[8,64,128]{2,1,0:T(8,128)} %all_to_all.32.map_ref), custom_call_target="tpu_custom_call" | custom-call | tf_op jit(solution)/shard_map/plane_prefix/pallas_call | solution.py:388
  25.5 5.6 %collective-permute-start.6 = (f32[64,128]{1,0:T(8,128)}, f32[64,128]{1,0:T(8,128)S(1)}, u32[]{:S(2)}, u32[]{:S(2)}) collective-permute-start(f32[64,128]{1,0:T(8,128)} %get-tuple-element.25), channel_id=1, source_target_pairs={{0,224},{32,0},{64,32},{96,64},{128,96},{160,128},{192,160},{224,1... | collective-permute-start | bytes 98312 | tf_op jit(solution)/shard_map/ppermute | solution.py:404
  31.1 1.2 collective-permute-start.5
  32.3 0.2 collective-permute-done.6.refs_6_
  32.4 2.8 %collective-permute-start.4 = (f32[64,128]{1,0:T(8,128)}, f32[64,128]{1,0:T(8,128)S(1)}, u32[]{:S(2)}, u32[]{:S(2)}) collective-permute-start(f32[64,128]{1,0:T(8,128)} %get-tuple-element.25), channel_id=1, source_target_pairs={{0,160},{32,192},{64,224},{96,0},{128,32},{160,64},{192,96},{224,1... | collective-permute-start | bytes 98312 | tf_op jit(solution)/shard_map/ppermute | solution.py:404
  35.3 1.9 %collective-permute-start.3 = (f32[64,128]{1,0:T(8,128)}, f32[64,128]{1,0:T(8,128)S(1)}, u32[]{:S(2)}, u32[]{:S(2)}) collective-permute-start(f32[64,128]{1,0:T(8,128)} %get-tuple-element.25), channel_id=1, source_target_pairs={{0,128},{32,160},{64,192},{96,224},{128,0},{160,32},{192,64},{224,... | collective-permute-start | bytes 98312 | tf_op jit(solution)/shard_map/ppermute | solution.py:404
  37.2 3.6 %collective-permute-start.2 = (f32[64,128]{1,0:T(8,128)}, f32[64,128]{1,0:T(8,128)S(1)}, u32[]{:S(2)}, u32[]{:S(2)}) collective-permute-start(f32[64,128]{1,0:T(8,128)} %get-tuple-element.25), channel_id=1, source_target_pairs={{0,96},{32,128},{64,160},{96,192},{128,224},{160,0},{192,32},{224,... | collective-permute-start | bytes 98312 | tf_op jit(solution)/shard_map/ppermute | solution.py:404
  40.8 1.3 collective-permute-done.3.refs_3_
  42.2 2.5 %collective-permute-start.1 = (f32[64,128]{1,0:T(8,128)}, f32[64,128]{1,0:T(8,128)S(1)}, u32[]{:S(2)}, u32[]{:S(2)}) collective-permute-start(f32[64,128]{1,0:T(8,128)} %get-tuple-element.25), channel_id=1, source_target_pairs={{0,64},{32,96},{64,128},{96,160},{128,192},{160,224},{192,0},{224,... | collective-permute-start | bytes 98312 | tf_op jit(solution)/shard_map/ppermute | solution.py:404
  44.6 0.4 collective-permute-start
  45.0 0.7 pad_add_fusion.place_ref
  45.6 2.4 %collective-permute-done.1.refs_1_ = f32[64,128]{1,0:T(8,128)S(1)} collective-permute-done((f32[64,128]{1,0:T(8,128)}, f32[64,128]{1,0:T(8,128)S(1)}, u32[]{:S(2)}, u32[]{:S(2)}) %collective-permute-start.1) | collective-permute-done | bytes 32800 | tf_op jit(solution)/shard_map/ppermute | solution.py:404
  48.0 0.8 collective-permute-done.refs_0_
  48.8 0.6 copy-done.18
  49.4 2.5 %entering.1 = f32[8,16,128]{2,1,0:T(8,128)} custom-call(s32[3]{0:T(128)} %pad_add_fusion.place_ref, f32[8,64,128]{2,1,0:T(8,128)} %get-tuple-element.24.before_ref, f32[64,128]{1,0:T(8,128)} %copy-done.18, f32[64,128]{1,0:T(8,128)} %copy-done.17, f32[64,128]{1,0:T(8,128)} %copy-done.16, f32[64,128]{1,0:T(8,128)} %copy-done.15, f32[64,128]{1,0:T(8,128)} %copy-done.14, ...), custom_call_target="tpu_custom_call" | custom-call | tf_op jit(solution)/shard_map/entering/pallas_call | solution.py:388
  51.9 0.0 copy-start.4
  51.9 0.2 pad_maximum_fusion.near_hbm
  52.1 5.6 %collective-permute-start.13 = (bf16[3,128,2048]{2,1,0:T(8,128)(2,1)S(1)}, bf16[3,128,2048]{2,1,0:T(8,128)(2,1)S(1)}, u32[]{:S(2)}, u32[]{:S(2)}) collective-permute-start(bf16[3,128,2048]{2,1,0:T(8,128)(2,1)S(1)} %pad_maximum_fusion.near_hbm), channel_id=1, source_target_pairs={{0,4},{4,0},{1,5},{5,1},{2,6},{6,2},{3,7},{7,3},{8,12},{12,8},{9,1... | collective-permute-start | bytes 4718600 | tf_op jit(solution)/shard_map/ppermute | solution.py:404
  57.7 8.3 %all_to_all.33.state_ref = f32[8,16,128]{2,1,0:T(8,128)} all-to-all(f32[8,16,128]{2,1,0:T(8,128)S(1)} %copy-done.4), channel_id=1, replica_groups=mesh['z'=8,'x'=4,'c'=2,'tp'=4] {'x','c'}, dimensions={0} | all-to-all | bytes 131072 | tf_op jit(solution)/shard_map/all_to_all | solution.py:399
  65.9 2.9 %finish.1.h0_ref = bf16[128,256]{1,0:T(8,128)(2,1)} custom-call(f32[8,16,128]{2,1,0:T(8,128)} %all_to_all.33.state_ref, f32[4,128,128]{2,1,0:T(8,128)} %get-tuple-element.27.read_ref, bf16[128,256]{1,0:T(8,128)(2,1)} %r_ref.3, bf16[128,256]{1,0:T(8,128)(2,1)} %k_ref.3, bf16[128,256]{1,0:T(8,128)(2,1)} %v_ref.3, bf16[128,256]{1,0:T(8,128)(2,1)} %c_ref.3, ...), custom_call_target="tpu_custom_call" | custom-call | tf_op jit(solution)/shard_map/finish/pallas_call | solution.py:388
  68.8 2.1 %collective-permute-start.12 = (bf16[128,256]{1,0:T(8,128)(2,1)}, bf16[128,256]{1,0:T(8,128)(2,1)S(1)}, u32[]{:S(2)}, u32[]{:S(2)}) collective-permute-start(bf16[128,256]{1,0:T(8,128)(2,1)} %finish.1.h0_ref), channel_id=1, source_target_pairs={{0,3},{1,0},{2,1},{3,2},{4,7},{5,4},{6,5},{7,6},{8,11},{9,8},{10,9... | collective-permute-start | bytes 196616 | tf_op jit(solution)/shard_map/ppermute | solution.py:404
  70.9 1.1 collective-permute-start.11
  72.0 2.1 %routing.1 = (s32[256,6]{1,0:T(8,128)}, f32[256,6]{1,0:T(8,128)}) custom-call(s32[8,128]{1,0:T(8,128)} %bitcast.33, f32[8,128]{1,0:T(8,128)} %bitcast.34), custom_call_target="tpu_custom_call" | custom-call | tf_op jit(solution)/shard_map/routing/pallas_call | solution.py:388
  74.1 1.6 reshape.25.token_ref
  75.8 1.1 collective-permute-done.10.h1_ref
  76.9 0.6 copy-done.11
  77.5 0.5 copy-done.2
  78.0 7.6 %project.1 = (bf16[6144,128]{1,0:T(8,128)(2,1)}, bf16[128,2048]{1,0:T(8,128)(2,1)}, bf16[128,512]{1,0:T(8,128)(2,1)}) custom-call(s32[3]{0:T(128)} %pad_add_fusion.place_ref, s32[1536]{0:T(1024)} %reshape.25.token_ref, bf16[128,256]{1,0:T(8,128)(2,1)} %finish.1.h0_ref, bf16[128,256]{1,0:T(8,128)(2,1)} %copy-done.11, bf16[128,256]{1,0:T(8,128)(2,1)} %copy-done.10, ...), custom_call_target="tpu_custom_call" | custom-call | tf_op jit(solution)/shard_map/project/pallas_call | solution.py:388
  85.6 47.2 %all_to_all.34 = bf16[64,96,128]{2,1,0:T(8,128)(2,1)} all-to-all(bf16[64,96,128]{2,1,0:T(8,128)(2,1)} %bitcast.26), channel_id=1, replica_groups=mesh['z'=8,'x'=4,'c'=2,'tp'=4] {'z','x','c'}, dimensions={0} | all-to-all | bytes 3145728 | tf_op jit(solution)/shard_map/all_to_all | solution.py:399
  132.8 7.5 %expert.1 = bf16[6144,128]{1,0:T(8,128)(2,1)} custom-call(bf16[6144,128]{1,0:T(8,128)(2,1)} %bitcast.22, bf16[2048,512]{1,0:T(8,128)(2,1)} %bitcast.23, bf16[2048,512]{1,0:T(8,128)(2,1)} %bitcast.24, bf16[512,2048]{1,0:T(8,128)(2,1)} %bitcast.25), custom_call_target="tpu_custom_call" | custom-call | tf_op jit(solution)/shard_map/expert/pallas_call | solution.py:388
  140.4 7.2 %all-to-all-start.3 = ((bf16[256,24,128]{2,1,0:T(8,128)(2,1)}), bf16[256,24,128]{2,1,0:T(8,128)(2,1)S(1)}, u32[]{:S(2)}, u32[]{:S(2)}) async-start(bf16[256,24,128]{2,1,0:T(8,128)(2,1)} %bitcast.21), calls=%async_computation.3 | async-start | bytes 3145728 | tf_op jit(solution)/shard_map/all_to_all | solution.py:399
  147.6 0.0 copy-start.3
  147.6 3.0 %shared.1 = (f32[128,512]{1,0:T(8,128)}, bf16[128,512]{1,0:T(8,128)(2,1)}, bf16[128,512]{1,0:T(8,128)(2,1)}, bf16[128,512]{1,0:T(8,128)(2,1)}) custom-call(s32[3]{0:T(128)} %pad_add_fusion.place_ref, bf16[128,2048]{1,0:T(8,128)(2,1)} %get-tuple-element.34.normed_ref, bf16[2048,128]{1,0:T(8,128)(2,1)} %gate_ref.1, bf16[2048,128]{1,0:T(8,128)(2,1)} %up_ref.1, ...), custom_call_target="tpu_custom_call" | custom-call | tf_op jit(solution)/shard_map/shared/pallas_call | solution.py:388
  150.6 1.4 collective-permute-start.14
  152.0 2.5 %collective-permute-start.15 = (bf16[128,512]{1,0:T(8,128)(2,1)}, bf16[128,512]{1,0:T(8,128)(2,1)S(1)}, u32[]{:S(2)}, u32[]{:S(2)}) collective-permute-start(bf16[128,512]{1,0:T(8,128)(2,1)} %get-tuple-element.37), channel_id=1, source_target_pairs={{0,2},{1,3},{2,0},{3,1},{4,6},{5,7},{6,4},{7,5},{8,10},{9,11},{10,... | collective-permute-start | bytes 393224 | tf_op jit(solution)/shard_map/ppermute | solution.py:404
  154.4 1.1 collective-permute-start.16
  155.6 0.7 reshape_reshape.3.token_ref
  156.3 0.7 reshape.31.weight_ref
  157.0 7.4 %collective-permute-done.15.s2_ref = bf16[128,512]{1,0:T(8,128)(2,1)S(1)} collective-permute-done((bf16[128,512]{1,0:T(8,128)(2,1)}, bf16[128,512]{1,0:T(8,128)(2,1)S(1)}, u32[]{:S(2)}, u32[]{:S(2)}) %collective-permute-start.15) | collective-permute-done | bytes 131104 | tf_op jit(solution)/shard_map/ppermute | solution.py:404
  164.4 25.2 %all-to-all-done.3 = bf16[256,24,128]{2,1,0:T(8,128)(2,1)S(1)} async-done(((bf16[256,24,128]{2,1,0:T(8,128)(2,1)}), bf16[256,24,128]{2,1,0:T(8,128)(2,1)S(1)}, u32[]{:S(2)}, u32[]{:S(2)}) %all-to-all-start.3) | async-done | bytes 1572896 | tf_op jit(solution)/shard_map/all_to_all | solution.py:399
  189.6 1.2 copy-done
  190.8 2.9 %combine.1 = bf16[128,512]{1,0:T(8,128)(2,1)} custom-call(bf16[6144,128]{1,0:T(8,128)(2,1)} %bitcast.20, s32[1,1536]{1,0:T(1,128)} %reshape_reshape.3.token_ref, f32[1,1536]{1,0:T(1,128)} %reshape.31.weight_ref, bf16[128,512]{1,0:T(8,128)(2,1)} %get-tuple-element.33.middle_ref, f32[128,512]{1,0:T(8,128)} %get-tuple-element.35.s0_ref, ...), custom_call_target="tpu_custom_call" | custom-call | tf_op jit(solution)/shard_map/combine/pallas_call | solution.py:388
  (44 shorter events, 0.1 us)
Async XLA Ops:
  1.1 50.8 %collective-permute-start.9 = (bf16[128,2048]{1,0:T(8,128)(2,1)S(1)}, bf16[128,2048]{1,0:T(8,128)(2,1)S(1)}, u32[]{:S(2)}, u32[]{:S(2)}) collective-permute-start(bf16[128,2048]{1,0:T(8,128)(2,1)S(1)} %constant_dynamic-slice_fusion), channel_id=1, source_target_pairs={{0,3},{1,0},{2,1},{3,2},{4,7},{5,4},{6,5},{7,6},{8,11},{9,8},{10,9... | collective-permute-start | bytes 1572872 | tf_op jit(solution)/shard_map/ppermute | solution.py:404
  4.7 47.2 %collective-permute-start.8 = (bf16[128,2048]{1,0:T(8,128)(2,1)S(1)}, bf16[128,2048]{1,0:T(8,128)(2,1)S(1)}, u32[]{:S(2)}, u32[]{:S(2)}) collective-permute-start(bf16[128,2048]{1,0:T(8,128)(2,1)S(1)} %constant_dynamic-slice_fusion), channel_id=1, source_target_pairs={{0,2},{1,3},{2,0},{3,1},{4,6},{5,7},{6,4},{7,5},{8,10},{9,11},{10,... | collective-permute-start | bytes 1572872 | tf_op jit(solution)/shard_map/ppermute | solution.py:404
  5.1 46.8 %collective-permute-start.7 = (bf16[128,2048]{1,0:T(8,128)(2,1)S(1)}, bf16[128,2048]{1,0:T(8,128)(2,1)S(1)}, u32[]{:S(2)}, u32[]{:S(2)}) collective-permute-start(bf16[128,2048]{1,0:T(8,128)(2,1)S(1)} %constant_dynamic-slice_fusion), channel_id=1, source_target_pairs={{0,1},{1,2},{2,3},{3,0},{4,5},{5,6},{6,7},{7,4},{8,9},{9,10},{10,1... | collective-permute-start | bytes 1572872 | tf_op jit(solution)/shard_map/ppermute | solution.py:404
  25.5 6.9 %collective-permute-start.6 = (f32[64,128]{1,0:T(8,128)}, f32[64,128]{1,0:T(8,128)S(1)}, u32[]{:S(2)}, u32[]{:S(2)}) collective-permute-start(f32[64,128]{1,0:T(8,128)} %get-tuple-element.25), channel_id=1, source_target_pairs={{0,224},{32,0},{64,32},{96,64},{128,96},{160,128},{192,160},{224,1... | collective-permute-start | bytes 98312 | tf_op jit(solution)/shard_map/ppermute | solution.py:404
  31.1 4.2 %collective-permute-start.5 = (f32[64,128]{1,0:T(8,128)}, f32[64,128]{1,0:T(8,128)S(1)}, u32[]{:S(2)}, u32[]{:S(2)}) collective-permute-start(f32[64,128]{1,0:T(8,128)} %get-tuple-element.25), channel_id=1, source_target_pairs={{0,192},{32,224},{64,0},{96,32},{128,64},{160,96},{192,128},{224,1... | collective-permute-start | bytes 98312 | tf_op jit(solution)/shard_map/ppermute | solution.py:404
  32.4 16.4 %copy-start.12 = (f32[64,128]{1,0:T(8,128)}, f32[64,128]{1,0:T(8,128)S(1)}, u32[]{:S(2)}) copy-start(f32[64,128]{1,0:T(8,128)S(1)} %collective-permute-done.6.refs_6_) | copy-start | bytes 98308
  32.4 4.8 %collective-permute-start.4 = (f32[64,128]{1,0:T(8,128)}, f32[64,128]{1,0:T(8,128)S(1)}, u32[]{:S(2)}, u32[]{:S(2)}) collective-permute-start(f32[64,128]{1,0:T(8,128)} %get-tuple-element.25), channel_id=1, source_target_pairs={{0,160},{32,192},{64,224},{96,0},{128,32},{160,64},{192,96},{224,1... | collective-permute-start | bytes 98312 | tf_op jit(solution)/shard_map/ppermute | solution.py:404
  35.3 13.5 %copy-start.13 = (f32[64,128]{1,0:T(8,128)}, f32[64,128]{1,0:T(8,128)S(1)}, u32[]{:S(2)}) copy-start(f32[64,128]{1,0:T(8,128)S(1)} %collective-permute-done.5.refs_5_) | copy-start | bytes 98308
  35.3 6.9 %collective-permute-start.3 = (f32[64,128]{1,0:T(8,128)}, f32[64,128]{1,0:T(8,128)S(1)}, u32[]{:S(2)}, u32[]{:S(2)}) collective-permute-start(f32[64,128]{1,0:T(8,128)} %get-tuple-element.25), channel_id=1, source_target_pairs={{0,128},{32,160},{64,192},{96,224},{128,0},{160,32},{192,64},{224,... | collective-permute-start | bytes 98312 | tf_op jit(solution)/shard_map/ppermute | solution.py:404
  37.2 11.6 %copy-start.14 = (f32[64,128]{1,0:T(8,128)}, f32[64,128]{1,0:T(8,128)S(1)}, u32[]{:S(2)}) copy-start(f32[64,128]{1,0:T(8,128)S(1)} %collective-permute-done.4.refs_4_) | copy-start | bytes 98308
  37.2 7.4 %collective-permute-start.2 = (f32[64,128]{1,0:T(8,128)}, f32[64,128]{1,0:T(8,128)S(1)}, u32[]{:S(2)}, u32[]{:S(2)}) collective-permute-start(f32[64,128]{1,0:T(8,128)} %get-tuple-element.25), channel_id=1, source_target_pairs={{0,96},{32,128},{64,160},{96,192},{128,224},{160,0},{192,32},{224,... | collective-permute-start | bytes 98312 | tf_op jit(solution)/shard_map/ppermute | solution.py:404
  42.2 6.7 %copy-start.15 = (f32[64,128]{1,0:T(8,128)}, f32[64,128]{1,0:T(8,128)S(1)}, u32[]{:S(2)}) copy-start(f32[64,128]{1,0:T(8,128)S(1)} %collective-permute-done.3.refs_3_) | copy-start | bytes 98308
  42.2 5.9 %collective-permute-start.1 = (f32[64,128]{1,0:T(8,128)}, f32[64,128]{1,0:T(8,128)S(1)}, u32[]{:S(2)}, u32[]{:S(2)}) collective-permute-start(f32[64,128]{1,0:T(8,128)} %get-tuple-element.25), channel_id=1, source_target_pairs={{0,64},{32,96},{64,128},{96,160},{128,192},{160,224},{192,0},{224,... | collective-permute-start | bytes 98312 | tf_op jit(solution)/shard_map/ppermute | solution.py:404
  44.6 4.2 %copy-start.16 = (f32[64,128]{1,0:T(8,128)}, f32[64,128]{1,0:T(8,128)S(1)}, u32[]{:S(2)}) copy-start(f32[64,128]{1,0:T(8,128)S(1)} %collective-permute-done.2.refs_2_) | copy-start | bytes 98308
  44.6 4.2 %collective-permute-start = (f32[64,128]{1,0:T(8,128)}, f32[64,128]{1,0:T(8,128)S(1)}, u32[]{:S(2)}, u32[]{:S(2)}) collective-permute-start(f32[64,128]{1,0:T(8,128)} %get-tuple-element.25), channel_id=1, source_target_pairs={{0,32},{32,64},{64,96},{96,128},{128,160},{160,192},{192,224},{224... | collective-permute-start | bytes 98312 | tf_op jit(solution)/shard_map/ppermute | solution.py:404
  48.0 0.8 copy-start.17
  48.8 0.6 copy-start.18
  51.9 5.8 %copy-start.4 = (f32[8,16,128]{2,1,0:T(8,128)S(1)}, f32[8,16,128]{2,1,0:T(8,128)}, u32[]{:S(2)}) copy-start(f32[8,16,128]{2,1,0:T(8,128)} %entering.1) | copy-start | bytes 196612
  52.1 24.8 %copy-start.1 = (bf16[3,128,2048]{2,1,0:T(8,128)(2,1)}, bf16[3,128,2048]{2,1,0:T(8,128)(2,1)S(1)}, u32[]{:S(2)}) copy-start(bf16[3,128,2048]{2,1,0:T(8,128)(2,1)S(1)} %pad_maximum_fusion.near_hbm) | copy-start | bytes 4718596
  52.1 24.8 %collective-permute-start.13 = (bf16[3,128,2048]{2,1,0:T(8,128)(2,1)S(1)}, bf16[3,128,2048]{2,1,0:T(8,128)(2,1)S(1)}, u32[]{:S(2)}, u32[]{:S(2)}) collective-permute-start(bf16[3,128,2048]{2,1,0:T(8,128)(2,1)S(1)} %pad_maximum_fusion.near_hbm), channel_id=1, source_target_pairs={{0,4},{4,0},{1,5},{5,1},{2,6},{6,2},{3,7},{7,3},{8,12},{12,8},{9,1... | collective-permute-start | bytes 4718600 | tf_op jit(solution)/shard_map/ppermute | solution.py:404
  68.8 7.0 %collective-permute-start.12 = (bf16[128,256]{1,0:T(8,128)(2,1)}, bf16[128,256]{1,0:T(8,128)(2,1)S(1)}, u32[]{:S(2)}, u32[]{:S(2)}) collective-permute-start(bf16[128,256]{1,0:T(8,128)(2,1)} %finish.1.h0_ref), channel_id=1, source_target_pairs={{0,3},{1,0},{2,1},{3,2},{4,7},{5,4},{6,5},{7,6},{8,11},{9,8},{10,9... | collective-permute-start | bytes 196616 | tf_op jit(solution)/shard_map/ppermute | solution.py:404
  70.9 4.9 %collective-permute-start.11 = (bf16[128,256]{1,0:T(8,128)(2,1)}, bf16[128,256]{1,0:T(8,128)(2,1)S(1)}, u32[]{:S(2)}, u32[]{:S(2)}) collective-permute-start(bf16[128,256]{1,0:T(8,128)(2,1)} %finish.1.h0_ref), channel_id=1, source_target_pairs={{0,2},{1,3},{2,0},{3,1},{4,6},{5,7},{6,4},{7,5},{8,10},{9,11},{10,... | collective-permute-start | bytes 196616 | tf_op jit(solution)/shard_map/ppermute | solution.py:404
  72.0 4.8 %collective-permute-start.10 = (bf16[128,256]{1,0:T(8,128)(2,1)}, bf16[128,256]{1,0:T(8,128)(2,1)S(1)}, u32[]{:S(2)}, u32[]{:S(2)}) collective-permute-start(bf16[128,256]{1,0:T(8,128)(2,1)} %finish.1.h0_ref), channel_id=1, source_target_pairs={{0,1},{1,2},{2,3},{3,0},{4,5},{5,6},{6,7},{7,4},{8,9},{9,10},{10,1... | collective-permute-start | bytes 196616 | tf_op jit(solution)/shard_map/ppermute | solution.py:404
  75.8 1.1 copy-start.9
  75.8 1.1 copy-start.10
  76.8 0.6 copy-start.11
  76.8 1.1 copy-start.2
  140.4 49.3 %all-to-all-start.3 = ((bf16[256,24,128]{2,1,0:T(8,128)(2,1)}), bf16[256,24,128]{2,1,0:T(8,128)(2,1)S(1)}, u32[]{:S(2)}, u32[]{:S(2)}) async-start(bf16[256,24,128]{2,1,0:T(8,128)(2,1)} %bitcast.21), calls=%async_computation.3 | async-start | bytes 3145728 | tf_op jit(solution)/shard_map/all_to_all | solution.py:399
  147.6 7.9 %copy-start.3 = (s32[256,6]{1,0:T(8,128)S(1)}, s32[256,6]{1,0:T(8,128)}, u32[]{:S(2)}) copy-start(s32[256,6]{1,0:T(8,128)} %get-tuple-element.22) | copy-start | bytes 18436
  147.6 8.7 %copy-start.8 = (f32[256,6]{1,0:T(8,128)S(1)}, f32[256,6]{1,0:T(8,128)}, u32[]{:S(2)}) copy-start(f32[256,6]{1,0:T(8,128)} %get-tuple-element.32) | copy-start | bytes 18436
  150.6 6.4 %collective-permute-start.14 = (bf16[128,512]{1,0:T(8,128)(2,1)}, bf16[128,512]{1,0:T(8,128)(2,1)S(1)}, u32[]{:S(2)}, u32[]{:S(2)}) collective-permute-start(bf16[128,512]{1,0:T(8,128)(2,1)} %get-tuple-element.36), channel_id=1, source_target_pairs={{0,1},{1,2},{2,3},{3,0},{4,5},{5,6},{6,7},{7,4},{8,9},{9,10},{10,1... | collective-permute-start | bytes 393224 | tf_op jit(solution)/shard_map/ppermute | solution.py:404
  152.0 12.4 %collective-permute-start.15 = (bf16[128,512]{1,0:T(8,128)(2,1)}, bf16[128,512]{1,0:T(8,128)(2,1)S(1)}, u32[]{:S(2)}, u32[]{:S(2)}) collective-permute-start(bf16[128,512]{1,0:T(8,128)(2,1)} %get-tuple-element.37), channel_id=1, source_target_pairs={{0,2},{1,3},{2,0},{3,1},{4,6},{5,7},{6,4},{7,5},{8,10},{9,11},{10,... | collective-permute-start | bytes 393224 | tf_op jit(solution)/shard_map/ppermute | solution.py:404
  154.4 10.0 %collective-permute-start.16 = (bf16[128,512]{1,0:T(8,128)(2,1)}, bf16[128,512]{1,0:T(8,128)(2,1)S(1)}, u32[]{:S(2)}, u32[]{:S(2)}) collective-permute-start(bf16[128,512]{1,0:T(8,128)(2,1)} %get-tuple-element.38), channel_id=1, source_target_pairs={{0,3},{1,0},{2,1},{3,2},{4,7},{5,4},{6,5},{7,6},{8,11},{9,8},{10,9... | collective-permute-start | bytes 393224 | tf_op jit(solution)/shard_map/ppermute | solution.py:404
  157.0 32.6 %copy-start.5 = (bf16[128,512]{1,0:T(8,128)(2,1)}, bf16[128,512]{1,0:T(8,128)(2,1)S(1)}, u32[]{:S(2)}) copy-start(bf16[128,512]{1,0:T(8,128)(2,1)S(1)} %collective-permute-done.14.s1_ref) | copy-start | bytes 393220
  164.4 25.2 %copy-start.6 = (bf16[128,512]{1,0:T(8,128)(2,1)}, bf16[128,512]{1,0:T(8,128)(2,1)S(1)}, u32[]{:S(2)}) copy-start(bf16[128,512]{1,0:T(8,128)(2,1)S(1)} %collective-permute-done.15.s2_ref) | copy-start | bytes 393220
  164.4 25.2 %copy-start.7 = (bf16[128,512]{1,0:T(8,128)(2,1)}, bf16[128,512]{1,0:T(8,128)(2,1)S(1)}, u32[]{:S(2)}) copy-start(bf16[128,512]{1,0:T(8,128)(2,1)S(1)} %collective-permute-done.16.s3_ref) | copy-start | bytes 393220
  189.6 1.2 copy-start

commit v3 on v2

--- a/solution.py
+++ b/solution.py
@@ -1,5 +1,3 @@
-import functools
-
 import jax
 import jax.numpy as jnp
 from jax import lax
@@ -7,6 +5,7 @@
 from jax.experimental.pallas import tpu as pltpu
 from jax.sharding import Mesh
 from jax.sharding import PartitionSpec as P
+
 
 CH = 64
 CAP = 6
@@ -76,32 +75,27 @@
 
 
 def routing_kernel(routes_ref, weight_ref, token_ref, slot_weight_ref):
-    experts, width = token_ref.shape
-    top, tokens = routes_ref.shape
-    expert, token = iotas(experts, tokens)
-    hit = jnp.zeros((experts, tokens), F32)
-    weight = jnp.zeros((experts, tokens), F32)
+    slots, experts = token_ref.shape
+    tokens, top = routes_ref.shape
+    token, expert = iotas(tokens, experts)
+    weight = jnp.zeros((tokens, experts), F32)
+    hit = jnp.zeros((tokens, experts), F32)
     for k in range(top):
-        same = routes_ref[k : k + 1, :] == expert
-        hit = hit + jnp.where(same, 1.0, 0.0)
-        weight = weight + jnp.where(same, weight_ref[k : k + 1, :], 0.0)
+        same = routes_ref[:, k : k + 1] == expert
+        hit = jnp.where(same, 1.0, hit)
+        weight = jnp.where(same, weight_ref[:, k : k + 1], weight)
     row, col = iotas(tokens, tokens)
-    earlier = jnp.where(row < col, 1.0, 0.0).astype(BF16)
-    within = dot(hit.astype(BF16), earlier)
-    count = jnp.sum(hit, axis=1, keepdims=True)
-    slot = lax.broadcasted_iota(jnp.int32, (experts, width), 1) // (width // CAP)
-    tokens_out = jnp.full((experts, width), -1.0, F32)
-    weights_out = jnp.zeros((experts, width), F32)
-    number = token.astype(F32)
-    for m in range(CAP):
-        chosen = (hit > 0.5) & (within == float(m))
-        name = jnp.sum(jnp.where(chosen, number, 0.0), axis=1, keepdims=True)
-        name = jnp.where(count > float(m), name, -1.0)
-        part = jnp.sum(jnp.where(chosen, weight, 0.0), axis=1, keepdims=True)
-        tokens_out = jnp.where(slot == m, name, tokens_out)
-        weights_out = jnp.where(slot == m, part, weights_out)
-    token_ref[...] = tokens_out.astype(jnp.int32)
-    slot_weight_ref[...] = weights_out
+    earlier = jnp.where(row > col, 1.0, 0.0).astype(BF16)
+    within = dot(earlier, hit.astype(BF16))
+    within = jnp.where(hit > 0.5, within, -1.0)
+    number = token.astype(F32) + 1.0
+    for m in range(slots):
+        chosen = within == float(m)
+        name = jnp.sum(jnp.where(chosen, number, 0.0), axis=0, keepdims=True) - 1.0
+        token_ref[m : m + 1, :] = name.astype(jnp.int32)
+        slot_weight_ref[m : m + 1, :] = jnp.sum(
+            jnp.where(chosen, weight, 0.0), axis=0, keepdims=True
+        )
 
 
 def local_kernel(r_ref, k_ref, v_ref, d_ref, c_ref, mix_ref, map_ref, read_ref):
@@ -163,9 +157,35 @@
     for h, f in zip(every, parts(final)):
         diagonal = jnp.where(hrow == hcol, jnp.broadcast_to(f, (CH, CH)), 0.0)
         state = states[h] + jnp.concatenate([diagonal, written[h]], 1)
-        map_ref[2 * h] = state
-        map_ref[2 * h + 1] = state
+        map_ref[2 * h], map_ref[2 * h + 1] = packed(state)
         read_ref[h] = reads[h] + jnp.concatenate([asked[h], on_values[h][t:]], 1)
+
+
+def packed(state):
+    half = CH // 2
+    left = jnp.concatenate([state[:half, :CH], state[half:, :CH]], 1)
+    quarter = half // 2
+    pieces = []
+    for c in range(2):
+        cols = state[:, CH + c * half : CH + (c + 1) * half]
+        rows = [cols[i * quarter : (i + 1) * quarter] for i in range(4)]
+        pieces.append(jnp.concatenate([left, jnp.concatenate(rows, 1)], 0))
+    return pieces
+
+
+def repacked(state):
+    half = CH // 2
+    quarter = half // 2
+    left = jnp.concatenate([state[:half, :CH], state[half:, :CH]], 1)
+    rows = [state[i * quarter : (i + 1) * quarter, CH:] for i in range(4)]
+    return jnp.concatenate([left, jnp.concatenate(rows, 1)], 0)
+
+
+def unpacked(block):
+    half = CH // 2
+    left = jnp.concatenate([block[:half, :CH], block[:half, CH:]], 0)
+    right = jnp.concatenate([block[half:, i * half : (i + 1) * half] for i in range(4)], 0)
+    return jnp.concatenate([left, right], 1)
 
 
 def joined(former, latter, late):
@@ -174,31 +194,31 @@
 
 def plane_kernel(map_ref, before_ref, total_ref):
     count = map_ref.shape[0]
-    hrow, hcol = iotas(CH, 2 * CH)
+    hrow, hcol = iotas(CH, 3 * CH // 2)
     late = hcol >= CH
-    maps = [map_ref[q] for q in range(count)]
+    maps = [unpacked(map_ref[q]) for q in range(count)]
     span = 1
     while span < count:
         maps = [
             maps[q] if q < span else joined(maps[q - span], maps[q], late) for q in range(count)
         ]
         span *= 2
+    total = repacked(maps[count - 1])
+    for z in range(total_ref.shape[0]):
+        total_ref[z] = total
     before_ref[0] = jnp.where(hrow == hcol, 1.0, 0.0)
     for q in range(1, count):
         before_ref[q] = maps[q - 1]
-    total_ref[...] = maps[count - 1]
-
-
-def entering_kernel(place_ref, before_ref, *refs):
-    *earlier_refs, out_ref = refs
+
+
+def entering_kernel(place_ref, before_ref, total_ref, out_ref):
     z_here = place_ref[0]
-    core = place_ref[1]
-    hrow, hcol = iotas(CH, 2 * CH)
+    hrow, hcol = iotas(CH, 3 * CH // 2)
     late = hcol >= CH
     nothing = jnp.where(hrow == hcol, 1.0, 0.0)
     maps = [
-        jnp.where(z_here >= k, earlier_refs[k - 1][...], nothing)
-        for k in range(len(earlier_refs), 0, -1)
+        jnp.where(z < z_here, unpacked(total_ref[z]), nothing)
+        for z in range(total_ref.shape[0] - 1)
     ]
     while len(maps) > 1:
         odd = maps[:1] if len(maps) % 2 else []
@@ -207,14 +227,13 @@
             joined(rest[i], rest[i + 1], late) for i in range(0, len(rest), 2)
         ]
     state = maps[0][:, CH:]
-    half = CH // 2
-    start = pl.multiple_of(core * half, half)
     count = before_ref.shape[0]
-    rows = jnp.concatenate([before_ref[q, pl.ds(start, half), :] for q in range(count)], 0)
+    rows = jnp.concatenate([before_ref[q] for q in range(count)], 0)
     mine = mm(rows[:, :CH], state) + rows[:, CH:]
+    quarter = CH // 4
     for q in range(count):
-        part = mine[q * half : (q + 1) * half]
-        out_ref[q] = jnp.concatenate([part[: half // 2], part[half // 2 :]], 1)
+        pieces = [mine[q * CH + i * quarter : q * CH + (i + 1) * quarter] for i in range(4)]
+        out_ref[q] = jnp.concatenate(pieces, 1)
 
 
 def finish_kernel(
@@ -228,7 +247,14 @@
     readouts = []
     for h in every:
         even, odd = state_ref[2 * h], state_ref[2 * h + 1]
-        state = jnp.concatenate([even[:, :CH], even[:, CH:], odd[:, :CH], odd[:, CH:]], 0)
+        half = CH // 2
+        state = jnp.concatenate(
+            [
+                jnp.concatenate([ref[:, i * half : (i + 1) * half] for i in range(4)], 0)
+                for ref in (even, odd)
+            ],
+            1,
+        )
         reads = read_ref[h]
         readouts.append(reads[:, CH:] + mm(reads[:, :CH], state))
     bonuses = [jnp.sum(weight[:, s], axis=1, keepdims=True) for s in slices]
@@ -293,7 +319,7 @@
 
     def send(i, carry):
         for m in range(CAP):
-            token = jnp.maximum(token_ref[(i * 4 + tp) * CAP + m], 0)
+            token = jnp.maximum(token_ref[m, i * 4 + tp], 0)
             place = pl.multiple_of((i * CAP + m) * tiles, tiles)
             out_ref[pl.ds(place, tiles), :] = rows_ref[token]
         return carry
@@ -364,19 +390,29 @@
 ):
     tokens, cols = out_ref.shape
     tiles = cols // LANES
-    slots = back_ref.shape[0] // tiles
+    slots, experts = token_ref.shape
     wide_ref[...] = back_ref[...].astype(F32)
-    token, _ = iotas(tokens, slots)
-    table = jnp.where(token_ref[...] == token, weight_ref[...], 0.0).astype(BF16)
-    rows = jnp.concatenate(
-        [wide_ref[pl.ds(i, slots, stride=tiles), :].astype(BF16) for i in range(tiles)], 1
-    )
+    token, _ = iotas(tokens, experts)
     total = middle_ref[...].astype(F32) + s0_ref[...] + s1_ref[...].astype(F32)
     total = total + s2_ref[...].astype(F32) + s3_ref[...].astype(F32)
-    out_ref[...] = (total + dot(table, rows)).astype(BF16)
-
-
-def call(kernel, name, out, *args, scalars=0, fetched=0, scratch=()):
+    tables, rows = [], []
+    for m in range(slots):
+        same = token_ref[m : m + 1, :] == token
+        tables.append(jnp.where(same, weight_ref[m : m + 1, :], 0.0).astype(BF16))
+        rows.append(
+            jnp.concatenate(
+                [
+                    wide_ref[pl.ds(m * tiles + i, experts, stride=slots * tiles), :].astype(BF16)
+                    for i in range(tiles)
+                ],
+                1,
+            )
+        )
+    routed = dot(jnp.concatenate(tables, 1), jnp.concatenate(rows, 0))
+    out_ref[...] = (total + routed).astype(BF16)
+
+
+def call(kernel, out, *args, scalars=0, fetched=0, scratch=()):
     smem = pl.BlockSpec(memory_space=pltpu.SMEM)
     vmem = pl.BlockSpec(memory_space=pltpu.VMEM)
     hbm = pl.BlockSpec(memory_space=pl.ANY)
@@ -391,7 +427,6 @@
         in_specs=[smem] * scalars + [vmem] * loaded + [hbm] * fetched,
         out_specs=jax.tree.map(lambda _: vmem, out),
         scratch_shapes=scratch,
-        name=name,
     )(*args)
 
 
@@ -404,7 +439,7 @@
     return lax.ppermute(array, axis, [(i, (i + shift) % peers) for i in range(peers)])
 
 
-def per_device(
+def layer(
     receptance, key, value, decay, correction, factor, mix, current, gain, bias, output_matrix,
     residual, norm_gain, routes, chosen, routed_gate, routed_up, routed_down, common_gate,
     common_up, common_down,
@@ -421,28 +456,31 @@
     place = jnp.stack([lax.axis_index("z"), core, lax.axis_index("tp")]).astype(jnp.int32)
     mix, current, gain, bias = (a.reshape(1, -1) for a in (mix, current, gain, bias))
 
+    maps, reads = call(
+        local_kernel,
+        (shape((2 * heads, 3 * CH // 4, 2 * CH), F32), shape((heads, tokens, 2 * CH), F32)),
+        receptance, key, value, decay, correction, mix,
+    )
+    maps, output_rows = lax.optimization_barrier((maps, output_matrix))
     half = inner // 2
-    mine = lax.dynamic_slice_in_dim(output_matrix, core * half, half, 0)
+    maps = exchange(maps, PLANE)
+    mine = lax.dynamic_slice_in_dim(output_rows, core * half, half, 0)
     near = [turned(mine, "tp", k) for k in (1, 2, 3)]
-
-    table = (shape((experts, CAP), jnp.int32), shape((experts, CAP), F32))
-    slot_token, slot_weight = call(routing_kernel, "routing", table, routes.T, chosen.T)
-    slot_token = slot_token.reshape(-1)
-    slot_weight = slot_weight.reshape(1, -1)
-
-    maps, reads = call(
-        local_kernel, "local_terms",
-        (shape((2 * heads, CH, 2 * CH), F32), shape((heads, tokens, 2 * CH), F32)),
-        receptance, key, value, decay, correction, mix,
-    )
-    maps = exchange(maps, PLANE)
-    before, total = call(
-        plane_kernel, "plane_prefix",
-        (shape((plane, CH, 2 * CH), F32), shape((CH, 2 * CH), F32)), maps,
-    )
-    earlier = [turned(total, "z", k) for k in range(1, z_count)]
+    before, totals = call(
+        plane_kernel,
+        (
+            shape((plane, CH, 3 * CH // 2), F32),
+            shape((z_count, 3 * CH // 4, 2 * CH), F32),
+        ),
+        maps,
+    )
+    totals = exchange(totals, "z")
+    slot_token, slot_weight = call(
+        routing_kernel,
+        (shape((CAP, experts), jnp.int32), shape((CAP, experts), F32)), routes, chosen,
+    )
     states = call(
-        entering_kernel, "entering", shape((plane, CH // 4, 2 * CH), F32), place, before, *earlier,
+        entering_kernel, shape((plane, CH // 4, 2 * CH), F32), place, before, totals,
         scalars=1,
     )
     states, *near = lax.optimization_barrier((states, *near))
@@ -450,12 +488,12 @@
     far = turned(near, "c", 1)
     states = exchange(states, PLANE)
     mixed = call(
-        finish_kernel, "finish", shape((tokens, inner), BF16), states, reads, receptance, key,
+        finish_kernel, shape((tokens, inner), BF16), states, reads, receptance, key,
         value, correction, factor, mix, current, gain, bias,
     )
     others = [turned(mixed, "tp", k) for k in (1, 2, 3)]
     outgoing, normed, own_middle = call(
-        project_kernel, "project",
+        project_kernel,
         (
             shape((slots * width // LANES, LANES), BF16),
             shape((tokens, width), BF16),
@@ -472,13 +510,13 @@
     )
     arrived = exchange(outgoing, SP)
     shared = call(
-        shared_kernel, "shared",
+        shared_kernel,
         (shape((tokens, cols), F32),) + (shape((tokens, cols), BF16),) * 3,
         place, normed, common_gate, common_up, common_down, scalars=1,
     )
     shared = [shared[0]] + [turned(shared[k], "tp", k) for k in (1, 2, 3)]
     answer = call(
-        expert_kernel, "expert", shape(outgoing.shape, BF16), arrived, routed_gate[0],
+        expert_kernel, shape(outgoing.shape, BF16), arrived, routed_gate[0],
         routed_up[0], routed_down[0],
         fetched=3,
         scratch=(
@@ -488,8 +526,8 @@
     )
     back = exchange(answer, EVERY)
     return call(
-        combine_kernel, "combine", shape((tokens, cols), BF16), back, slot_token.reshape(1, -1),
-        slot_weight, own_middle, *shared,
+        combine_kernel, shape((tokens, cols), BF16), back, slot_token, slot_weight,
+        own_middle, *shared,
         scratch=(pltpu.VMEM(back.shape, F32),),
     )
 
@@ -503,6 +541,4 @@
         + (P(EVERY, None, None),) * 3
         + (P(None, "tp"), P(None, "tp"), P("tp", None))
     )
-    return jax.shard_map(
-        per_device, mesh=finer, in_specs=placed, out_specs=P(SP, "tp"), check_vma=False
-    )
+    return jax.shard_map(layer, mesh=finer, in_specs=placed, out_specs=P(SP, "tp"), check_vma=False)

time: 194 us -> 185 us (0.954)
  starting transfers between devices: 43.6 us -> 30.6 us
  waiting for transfers between devices: 38.3 us -> 44.3 us
    ppermute x17 -> x10, starting transfers between devices: 36.4 us -> 15.4 us  [turned(): lax.ppermute(array, axis, [(i, (i + shift) % peers) for i in range(peers)])]
    all_to_all x1 -> x2, waiting for transfers between devices: 25.2 us -> 33.7 us  [exchange(): return lax.all_to_all(array, axes, split_axis=0, concat_axis=0, tiled=True)]
    all_to_all x1 -> x2, starting transfers between devices: 7.23 us -> 15.2 us  [exchange(): return lax.all_to_all(array, axes, split_axis=0, concat_axis=0, tiled=True)]
    ppermute x17 -> x10, waiting for transfers between devices: 13.1 us -> 10.6 us  [turned(): lax.ppermute(array, axis, [(i, (i + shift) % peers) for i in range(peers)])]
    reshape x2 -> x0, local copies, waits for them, and re-layouts: 2.37 us -> none  [the longest x1 1.64 us: per_device(): slot_token = slot_token.reshape(-1)]
    unnamed x38 -> x28, local copies, waits for them, and re-layouts: 2.92 us -> 4.52 us
  transfers between devices with their start and end apart: 18 -> 12, of which waited for: 7 -> 5; matrix products, arithmetic and copies ran while one was open for 2% -> 1% of each run, Pallas kernels for 9% -> 7%
where the time goes in v3:
time: 185 us; the launch traced here: 184 us
  blocking collectives  66 us (36%)
  waiting for transfers between devices  44.3 us (24%)
  Pallas kernels  36.8 us (20%)
  starting transfers between devices  30.6 us (17%)
  local copies, waits for them, and re-layouts  5.59 us (3%)
    all_to_all x3, blocking collectives, exchange(): return lax.all_to_all(array, axes, split_axis=0, concat_axis=0, tiled=True)  66 us
    pallas_call x9, Pallas kernels, call(): pl.pallas_call(kernel, out_shape=out, in_specs=[smem] * scalars + [vmem]...  36.8 us
    all_to_all x2, waiting for transfers between devices, exchange(): return lax.all_to_all(array, axes, split_axis=0, concat_axis=0, tiled=True)  33.7 us
    ppermute x10, starting transfers between devices, turned(): lax.ppermute(array, axis, [(i, (i + shift) % peers) for i in range(peers)])  15.4 us
    all_to_all x2, starting transfers between devices, exchange(): return lax.all_to_all(array, axes, split_axis=0, concat_axis=0, tiled=True)  15.2 us
    ppermute x10, waiting for transfers between devices, turned(): lax.ppermute(array, axis, [(i, (i + shift) % peers) for i in range(peers)])  10.6 us
    unnamed x28, local copies, waits for them, and re-layouts  4.52 us
  transfers between devices with their start and end apart: 12, of which 5 were waited for; matrix products, arithmetic and copies ran while one was open for 1% of the time, Pallas kernels for 7%

profile of v3, /device:TPU:1, one launch (start us, length us, event | category | flops | bytes accessed | tf_op | source)
XLA Modules:
  0.0 184.2 jit_solution(13607549233861847447)
XLA Ops:
  0.0 5.3 %shard_map.200 = (f32[8,48,128]{2,1,0:T(8,128)}, f32[4,128,128]{2,1,0:T(8,128)}) custom-call(bf16[128,256]{1,0:T(8,128)(2,1)} %r_ref.3, bf16[128,256]{1,0:T(8,128)(2,1)} %k_ref.3, bf16[128,256]{1,0:T(8,128)(2,1)} %v_ref.3, bf16[128,256]{1,0:T(8,128)(2,1)} %d_ref.1, bf16[128,256]{1,0:T(8,128)(2,1)} %c_ref.3, f32[1,256]{1,0:T(1,128)} %bitcast.29), custom_call_target="tpu_custom_call" | custom-call | tf_op jit(solution)/shard_map/pallas_call | solution.py:424
  5.3 1.1 constant_dynamic-slice_fusion
  6.4 3.6 %collective-permute-start.2 = (bf16[128,2048]{1,0:T(8,128)(2,1)S(1)}, bf16[128,2048]{1,0:T(8,128)(2,1)S(1)}, u32[]{:S(2)}, u32[]{:S(2)}) collective-permute-start(bf16[128,2048]{1,0:T(8,128)(2,1)S(1)} %constant_dynamic-slice_fusion), channel_id=1, source_target_pairs={{0,3},{1,0},{2,1},{3,2},{4,7},{5,4},{6,5},{7,6},{8,11},{9,8},{10,9... | collective-permute-start | bytes 1572872 | tf_op jit(solution)/shard_map/ppermute | solution.py:439
  10.0 0.3 collective-permute-start.1
  10.3 0.7 collective-permute-start
  11.0 12.0 %all_to_all.37.map_ref = f32[8,48,128]{2,1,0:T(8,128)} all-to-all(f32[8,48,128]{2,1,0:T(8,128)} %get-tuple-element.26), channel_id=1, replica_groups=mesh['z'=8,'x'=4,'c'=2,'tp'=4] {'x','c'}, dimensions={0} | all-to-all | bytes 393216 | tf_op jit(solution)/shard_map/all_to_all | solution.py:434
  23.0 2.4 %shard_map.201 = (f32[8,64,96]{2,1,0:T(8,128)}, f32[8,48,128]{2,1,0:T(8,128)}) custom-call(f32[8,48,128]{2,1,0:T(8,128)} %all_to_all.37.map_ref), custom_call_target="tpu_custom_call" | custom-call | tf_op jit(solution)/shard_map/pallas_call | solution.py:424
  25.4 8.2 %all-to-all-start.1 = ((f32[8,48,128]{2,1,0:T(8,128)}), f32[8,48,128]{2,1,0:T(8,128)S(1)}, u32[]{:S(2)}, u32[]{:S(2)}) async-start(f32[8,48,128]{2,1,0:T(8,128)} %get-tuple-element.28), calls=%async_computation.1 | async-start | bytes 393216 | tf_op jit(solution)/shard_map/all_to_all | solution.py:434
  33.5 0.7 pad_add_fusion.place_ref
  34.2 8.3 %all-to-all-done.1.total_ref = f32[8,48,128]{2,1,0:T(8,128)S(1)} async-done(((f32[8,48,128]{2,1,0:T(8,128)}), f32[8,48,128]{2,1,0:T(8,128)S(1)}, u32[]{:S(2)}, u32[]{:S(2)}) %all-to-all-start.1) | async-done | bytes 196640 | tf_op jit(solution)/shard_map/all_to_all | solution.py:434
  42.5 0.7 copy-done.3
  43.2 2.6 %shard_map.202 = f32[8,16,128]{2,1,0:T(8,128)} custom-call(s32[3]{0:T(128)} %pad_add_fusion.place_ref, f32[8,64,96]{2,1,0:T(8,128)} %get-tuple-element.27.before_ref, f32[8,48,128]{2,1,0:T(8,128)} %copy-done.3), custom_call_target="tpu_custom_call" | custom-call | tf_op jit(solution)/shard_map/pallas_call | solution.py:424
  45.8 0.0 collective-permute-done.2
  45.8 0.0 collective-permute-done.1
  45.8 0.0 collective-permute-done
  45.8 0.0 copy-start.4
  45.8 0.0 copy-start.11
  45.8 0.0 copy-start.12
  45.9 0.2 pad_maximum_fusion.near_hbm
  46.0 2.5 %collective-permute-start.6 = (bf16[3,128,2048]{2,1,0:T(8,128)(2,1)S(1)}, bf16[3,128,2048]{2,1,0:T(8,128)(2,1)S(1)}, u32[]{:S(2)}, u32[]{:S(2)}) collective-permute-start(bf16[3,128,2048]{2,1,0:T(8,128)(2,1)S(1)} %pad_maximum_fusion.near_hbm), channel_id=1, source_target_pairs={{0,4},{4,0},{1,5},{5,1},{2,6},{6,2},{3,7},{7,3},{8,12},{12,8},{9,1... | collective-permute-start | bytes 4718600 | tf_op jit(solution)/shard_map/ppermute | solution.py:439
  48.6 8.4 %all_to_all.38.state_ref = f32[8,16,128]{2,1,0:T(8,128)} all-to-all(f32[8,16,128]{2,1,0:T(8,128)S(1)} %copy-done.4), channel_id=1, replica_groups=mesh['z'=8,'x'=4,'c'=2,'tp'=4] {'x','c'}, dimensions={0} | all-to-all | bytes 131072 | tf_op jit(solution)/shard_map/all_to_all | solution.py:434
  57.0 2.9 %shard_map.203.h0_ref = bf16[128,256]{1,0:T(8,128)(2,1)} custom-call(f32[8,16,128]{2,1,0:T(8,128)} %all_to_all.38.state_ref, f32[4,128,128]{2,1,0:T(8,128)} %get-tuple-element.31.read_ref, bf16[128,256]{1,0:T(8,128)(2,1)} %r_ref.3, bf16[128,256]{1,0:T(8,128)(2,1)} %k_ref.3, bf16[128,256]{1,0:T(8,128)(2,1)} %v_ref.3, bf16[128,256]{1,0:T(8,128)(2,1)} %c_ref.3, ...), custom_call_target="tpu_custom_call" | custom-call | tf_op jit(solution)/shard_map/pallas_call | solution.py:424
  59.9 2.0 %collective-permute-start.5 = (bf16[128,256]{1,0:T(8,128)(2,1)}, bf16[128,256]{1,0:T(8,128)(2,1)S(1)}, u32[]{:S(2)}, u32[]{:S(2)}) collective-permute-start(bf16[128,256]{1,0:T(8,128)(2,1)} %shard_map.203.h0_ref), channel_id=1, source_target_pairs={{0,3},{1,0},{2,1},{3,2},{4,7},{5,4},{6,5},{7,6},{8,11},{9,8},{10,9... | collective-permute-start | bytes 196616 | tf_op jit(solution)/shard_map/ppermute | solution.py:439
  61.9 1.2 collective-permute-start.4
  63.1 0.0 collective-permute-start.3
  63.1 0.7 copy.22.routes_ref
  63.9 0.7 copy.23.weight_ref
  64.6 2.1 %shard_map.199 = (s32[6,256]{1,0:T(8,128)}, f32[6,256]{1,0:T(8,128)}) custom-call(s32[128,8]{1,0:T(8,128)} %copy.22.routes_ref, f32[128,8]{1,0:T(8,128)} %copy.23.weight_ref), custom_call_target="tpu_custom_call" | custom-call | tf_op jit(solution)/shard_map/pallas_call | solution.py:424
  66.7 0.0 collective-permute-done.5.h3_ref
  66.7 0.0 collective-permute-done.4.h2_ref
  66.7 1.8 collective-permute-done.3.h1_ref
  68.6 0.0 collective-permute-done.6.far_hbm
  68.6 0.6 copy-done.10
  69.2 0.6 copy-done.2
  69.8 7.8 %shard_map.204 = (bf16[6144,128]{1,0:T(8,128)(2,1)}, bf16[128,2048]{1,0:T(8,128)(2,1)}, bf16[128,512]{1,0:T(8,128)(2,1)}) custom-call(s32[3]{0:T(128)} %pad_add_fusion.place_ref, s32[6,256]{1,0:T(8,128)} %get-tuple-element.24.token_ref, bf16[128,256]{1,0:T(8,128)(2,1)} %shard_map.203.h0_ref, bf16[128,256]{1,0:T(8,128)(2,1)} %copy-done.10, ...), custom_call_target="tpu_custom_call" | custom-call | tf_op jit(solution)/shard_map/pallas_call | solution.py:424
  77.5 45.6 %all_to_all.39 = bf16[64,96,128]{2,1,0:T(8,128)(2,1)} all-to-all(bf16[64,96,128]{2,1,0:T(8,128)(2,1)} %bitcast.24), channel_id=1, replica_groups=mesh['z'=8,'x'=4,'c'=2,'tp'=4] {'z','x','c'}, dimensions={0} | all-to-all | bytes 3145728 | tf_op jit(solution)/shard_map/all_to_all | solution.py:434
  123.2 7.5 %shard_map.205 = bf16[6144,128]{1,0:T(8,128)(2,1)} custom-call(bf16[6144,128]{1,0:T(8,128)(2,1)} %bitcast.20, bf16[2048,512]{1,0:T(8,128)(2,1)} %bitcast.21, bf16[2048,512]{1,0:T(8,128)(2,1)} %bitcast.22, bf16[512,2048]{1,0:T(8,128)(2,1)} %bitcast.23), custom_call_target="tpu_custom_call" | custom-call | tf_op jit(solution)/shard_map/pallas_call | solution.py:424
  130.7 7.1 %all-to-all-start.4 = ((bf16[256,24,128]{2,1,0:T(8,128)(2,1)}), bf16[256,24,128]{2,1,0:T(8,128)(2,1)S(1)}, u32[]{:S(2)}, u32[]{:S(2)}) async-start(bf16[256,24,128]{2,1,0:T(8,128)(2,1)} %bitcast.19), calls=%async_computation.4 | async-start | bytes 3145728 | tf_op jit(solution)/shard_map/all_to_all | solution.py:434
  137.8 2.9 %shard_map.206 = (f32[128,512]{1,0:T(8,128)}, bf16[128,512]{1,0:T(8,128)(2,1)}, bf16[128,512]{1,0:T(8,128)(2,1)}, bf16[128,512]{1,0:T(8,128)(2,1)}) custom-call(s32[3]{0:T(128)} %pad_add_fusion.place_ref, bf16[128,2048]{1,0:T(8,128)(2,1)} %get-tuple-element.38.normed_ref, bf16[2048,128]{1,0:T(8,128)(2,1)} %gate_ref.1, bf16[2048,128]{1,0:T(8,128)(2,1)} %up_ref.1, ...), custom_call_target="tpu_custom_call" | custom-call | tf_op jit(solution)/shard_map/pallas_call | solution.py:424
  140.7 1.4 collective-permute-start.7
  142.1 2.5 %collective-permute-start.8 = (bf16[128,512]{1,0:T(8,128)(2,1)}, bf16[128,512]{1,0:T(8,128)(2,1)S(1)}, u32[]{:S(2)}, u32[]{:S(2)}) collective-permute-start(bf16[128,512]{1,0:T(8,128)(2,1)} %get-tuple-element.41), channel_id=1, source_target_pairs={{0,2},{1,3},{2,0},{3,1},{4,6},{5,7},{6,4},{7,5},{8,10},{9,11},{10,... | collective-permute-start | bytes 393224 | tf_op jit(solution)/shard_map/ppermute | solution.py:439
  144.5 1.1 collective-permute-start.9
  145.6 1.3 collective-permute-done.7.s1_ref
  146.9 7.5 %collective-permute-done.8.s2_ref = bf16[128,512]{1,0:T(8,128)(2,1)S(1)} collective-permute-done((bf16[128,512]{1,0:T(8,128)(2,1)}, bf16[128,512]{1,0:T(8,128)(2,1)S(1)}, u32[]{:S(2)}, u32[]{:S(2)}) %collective-permute-start.8) | collective-permute-done | bytes 131104 | tf_op jit(solution)/shard_map/ppermute | solution.py:439
  154.4 0.0 collective-permute-done.9.s3_ref
  154.4 25.4 %all-to-all-done.4 = bf16[256,24,128]{2,1,0:T(8,128)(2,1)S(1)} async-done(((bf16[256,24,128]{2,1,0:T(8,128)(2,1)}), bf16[256,24,128]{2,1,0:T(8,128)(2,1)S(1)}, u32[]{:S(2)}, u32[]{:S(2)}) %all-to-all-start.4) | async-done | bytes 1572896 | tf_op jit(solution)/shard_map/all_to_all | solution.py:434
  179.8 1.2 copy-done.1
  181.0 3.2 %shard_map.207 = bf16[128,512]{1,0:T(8,128)(2,1)} custom-call(bf16[6144,128]{1,0:T(8,128)(2,1)} %bitcast.18, s32[6,256]{1,0:T(8,128)} %get-tuple-element.24.token_ref, f32[6,256]{1,0:T(8,128)} %get-tuple-element.36.weight_ref, bf16[128,512]{1,0:T(8,128)(2,1)} %get-tuple-element.37.middle_ref, f32[128,512]{1,0:T(8,128)} %get-tuple-element.39.s0_ref, ...), custom_call_target="tpu_custom_call" | custom-call | tf_op jit(solution)/shard_map/pallas_call | solution.py:424
  (19 shorter events, 0.0 us)
Async XLA Ops:
  6.4 39.5 %collective-permute-start.2 = (bf16[128,2048]{1,0:T(8,128)(2,1)S(1)}, bf16[128,2048]{1,0:T(8,128)(2,1)S(1)}, u32[]{:S(2)}, u32[]{:S(2)}) collective-permute-start(bf16[128,2048]{1,0:T(8,128)(2,1)S(1)} %constant_dynamic-slice_fusion), channel_id=1, source_target_pairs={{0,3},{1,0},{2,1},{3,2},{4,7},{5,4},{6,5},{7,6},{8,11},{9,8},{10,9... | collective-permute-start | bytes 1572872 | tf_op jit(solution)/shard_map/ppermute | solution.py:439
  10.0 35.8 %collective-permute-start.1 = (bf16[128,2048]{1,0:T(8,128)(2,1)S(1)}, bf16[128,2048]{1,0:T(8,128)(2,1)S(1)}, u32[]{:S(2)}, u32[]{:S(2)}) collective-permute-start(bf16[128,2048]{1,0:T(8,128)(2,1)S(1)} %constant_dynamic-slice_fusion), channel_id=1, source_target_pairs={{0,2},{1,3},{2,0},{3,1},{4,6},{5,7},{6,4},{7,5},{8,10},{9,11},{10,... | collective-permute-start | bytes 1572872 | tf_op jit(solution)/shard_map/ppermute | solution.py:439
  10.3 35.5 %collective-permute-start = (bf16[128,2048]{1,0:T(8,128)(2,1)S(1)}, bf16[128,2048]{1,0:T(8,128)(2,1)S(1)}, u32[]{:S(2)}, u32[]{:S(2)}) collective-permute-start(bf16[128,2048]{1,0:T(8,128)(2,1)S(1)} %constant_dynamic-slice_fusion), channel_id=1, source_target_pairs={{0,1},{1,2},{2,3},{3,0},{4,5},{5,6},{6,7},{7,4},{8,9},{9,10},{10,1... | collective-permute-start | bytes 1572872 | tf_op jit(solution)/shard_map/ppermute | solution.py:439
  25.4 17.2 %all-to-all-start.1 = ((f32[8,48,128]{2,1,0:T(8,128)}), f32[8,48,128]{2,1,0:T(8,128)S(1)}, u32[]{:S(2)}, u32[]{:S(2)}) async-start(f32[8,48,128]{2,1,0:T(8,128)} %get-tuple-element.28), calls=%async_computation.1 | async-start | bytes 393216 | tf_op jit(solution)/shard_map/all_to_all | solution.py:434
  42.5 0.7 copy-start.3
  45.8 2.8 %copy-start.4 = (f32[8,16,128]{2,1,0:T(8,128)S(1)}, f32[8,16,128]{2,1,0:T(8,128)}, u32[]{:S(2)}) copy-start(f32[8,16,128]{2,1,0:T(8,128)} %shard_map.202) | copy-start | bytes 196612
  45.8 17.3 %copy-start.11 = (s32[128,8]{0,1:T(8,128)S(1)}, s32[128,8]{0,1:T(8,128)}, u32[]{:S(2)}) copy-start(s32[128,8]{0,1:T(8,128)} %param.34) | copy-start | bytes 12292
  45.8 18.0 %copy-start.12 = (f32[128,8]{0,1:T(8,128)S(1)}, f32[128,8]{0,1:T(8,128)}, u32[]{:S(2)}) copy-start(f32[128,8]{0,1:T(8,128)} %param.35) | copy-start | bytes 12292
  46.0 22.5 %copy-start = (bf16[3,128,2048]{2,1,0:T(8,128)(2,1)}, bf16[3,128,2048]{2,1,0:T(8,128)(2,1)S(1)}, u32[]{:S(2)}) copy-start(bf16[3,128,2048]{2,1,0:T(8,128)(2,1)S(1)} %pad_maximum_fusion.near_hbm) | copy-start | bytes 4718596
  46.0 22.5 %collective-permute-start.6 = (bf16[3,128,2048]{2,1,0:T(8,128)(2,1)S(1)}, bf16[3,128,2048]{2,1,0:T(8,128)(2,1)S(1)}, u32[]{:S(2)}, u32[]{:S(2)}) collective-permute-start(bf16[3,128,2048]{2,1,0:T(8,128)(2,1)S(1)} %pad_maximum_fusion.near_hbm), channel_id=1, source_target_pairs={{0,4},{4,0},{1,5},{5,1},{2,6},{6,2},{3,7},{7,3},{8,12},{12,8},{9,1... | collective-permute-start | bytes 4718600 | tf_op jit(solution)/shard_map/ppermute | solution.py:439
  59.9 6.8 %collective-permute-start.5 = (bf16[128,256]{1,0:T(8,128)(2,1)}, bf16[128,256]{1,0:T(8,128)(2,1)S(1)}, u32[]{:S(2)}, u32[]{:S(2)}) collective-permute-start(bf16[128,256]{1,0:T(8,128)(2,1)} %shard_map.203.h0_ref), channel_id=1, source_target_pairs={{0,3},{1,0},{2,1},{3,2},{4,7},{5,4},{6,5},{7,6},{8,11},{9,8},{10,9... | collective-permute-start | bytes 196616 | tf_op jit(solution)/shard_map/ppermute | solution.py:439
  61.9 4.8 %collective-permute-start.4 = (bf16[128,256]{1,0:T(8,128)(2,1)}, bf16[128,256]{1,0:T(8,128)(2,1)S(1)}, u32[]{:S(2)}, u32[]{:S(2)}) collective-permute-start(bf16[128,256]{1,0:T(8,128)(2,1)} %shard_map.203.h0_ref), channel_id=1, source_target_pairs={{0,2},{1,3},{2,0},{3,1},{4,6},{5,7},{6,4},{7,5},{8,10},{9,11},{10,... | collective-permute-start | bytes 196616 | tf_op jit(solution)/shard_map/ppermute | solution.py:439
  63.1 5.4 %collective-permute-start.3 = (bf16[128,256]{1,0:T(8,128)(2,1)}, bf16[128,256]{1,0:T(8,128)(2,1)S(1)}, u32[]{:S(2)}, u32[]{:S(2)}) collective-permute-start(bf16[128,256]{1,0:T(8,128)(2,1)} %shard_map.203.h0_ref), channel_id=1, source_target_pairs={{0,1},{1,2},{2,3},{3,0},{4,5},{5,6},{6,7},{7,4},{8,9},{9,10},{10,1... | collective-permute-start | bytes 196616 | tf_op jit(solution)/shard_map/ppermute | solution.py:439
  66.7 1.8 %copy-start.8 = (bf16[128,256]{1,0:T(8,128)(2,1)}, bf16[128,256]{1,0:T(8,128)(2,1)S(1)}, u32[]{:S(2)}) copy-start(bf16[128,256]{1,0:T(8,128)(2,1)S(1)} %collective-permute-done.5.h3_ref) | copy-start | bytes 196612
  66.7 1.8 copy-start.9
  68.6 0.6 copy-start.10
  68.6 1.2 copy-start.2
  130.7 49.1 %all-to-all-start.4 = ((bf16[256,24,128]{2,1,0:T(8,128)(2,1)}), bf16[256,24,128]{2,1,0:T(8,128)(2,1)S(1)}, u32[]{:S(2)}, u32[]{:S(2)}) async-start(bf16[256,24,128]{2,1,0:T(8,128)(2,1)} %bitcast.19), calls=%async_computation.4 | async-start | bytes 3145728 | tf_op jit(solution)/shard_map/all_to_all | solution.py:434
  140.7 6.2 %collective-permute-start.7 = (bf16[128,512]{1,0:T(8,128)(2,1)}, bf16[128,512]{1,0:T(8,128)(2,1)S(1)}, u32[]{:S(2)}, u32[]{:S(2)}) collective-permute-start(bf16[128,512]{1,0:T(8,128)(2,1)} %get-tuple-element.40), channel_id=1, source_target_pairs={{0,1},{1,2},{2,3},{3,0},{4,5},{5,6},{6,7},{7,4},{8,9},{9,10},{10,1... | collective-permute-start | bytes 393224 | tf_op jit(solution)/shard_map/ppermute | solution.py:439
  142.1 12.4 %collective-permute-start.8 = (bf16[128,512]{1,0:T(8,128)(2,1)}, bf16[128,512]{1,0:T(8,128)(2,1)S(1)}, u32[]{:S(2)}, u32[]{:S(2)}) collective-permute-start(bf16[128,512]{1,0:T(8,128)(2,1)} %get-tuple-element.41), channel_id=1, source_target_pairs={{0,2},{1,3},{2,0},{3,1},{4,6},{5,7},{6,4},{7,5},{8,10},{9,11},{10,... | collective-permute-start | bytes 393224 | tf_op jit(solution)/shard_map/ppermute | solution.py:439
  144.5 9.9 %collective-permute-start.9 = (bf16[128,512]{1,0:T(8,128)(2,1)}, bf16[128,512]{1,0:T(8,128)(2,1)S(1)}, u32[]{:S(2)}, u32[]{:S(2)}) collective-permute-start(bf16[128,512]{1,0:T(8,128)(2,1)} %get-tuple-element.42), channel_id=1, source_target_pairs={{0,3},{1,0},{2,1},{3,2},{4,7},{5,4},{6,5},{7,6},{8,11},{9,8},{10,9... | collective-permute-start | bytes 393224 | tf_op jit(solution)/shard_map/ppermute | solution.py:439
  146.9 32.9 %copy-start.5 = (bf16[128,512]{1,0:T(8,128)(2,1)}, bf16[128,512]{1,0:T(8,128)(2,1)S(1)}, u32[]{:S(2)}) copy-start(bf16[128,512]{1,0:T(8,128)(2,1)S(1)} %collective-permute-done.7.s1_ref) | copy-start | bytes 393220
  154.4 25.4 %copy-start.6 = (bf16[128,512]{1,0:T(8,128)(2,1)}, bf16[128,512]{1,0:T(8,128)(2,1)S(1)}, u32[]{:S(2)}) copy-start(bf16[128,512]{1,0:T(8,128)(2,1)S(1)} %collective-permute-done.8.s2_ref) | copy-start | bytes 393220
  154.4 25.4 %copy-start.7 = (bf16[128,512]{1,0:T(8,128)(2,1)}, bf16[128,512]{1,0:T(8,128)(2,1)S(1)}, u32[]{:S(2)}) copy-start(bf16[128,512]{1,0:T(8,128)(2,1)S(1)} %collective-permute-done.9.s3_ref) | copy-start | bytes 393220
  179.8 1.2 copy-start.1

commit v4 on v3

--- a/solution.py
+++ b/solution.py
@@ -266,40 +266,24 @@
     bonus = jnp.concatenate([jnp.broadcast_to(b, wide) for b in bonuses], 1)
     grouped = jnp.concatenate(scaled, 1) * gain_ref[...] + bias_ref[...]
     out = (grouped + bonus * v_ref[...].astype(F32)) * f_ref[...].astype(F32)
-    out_ref[...] = out.astype(BF16)
-
-
-def fetch(sources, targets, sems):
-    copies = [
-        pltpu.make_async_copy(source, target, sems.at[i])
-        for i, (source, target) in enumerate(zip(sources, targets))
-    ]
-    for copy in copies:
-        copy.start()
-    return copies
+    out = out.astype(BF16)
+    for y in range(out_ref.shape[0]):
+        out_ref[y] = out
 
 
 def project_kernel(
-    place_ref, token_ref, h0_ref, h1_ref, h2_ref, h3_ref, gain_ref, own_hbm, near_hbm, far_hbm,
-    residual_hbm, out_ref, normed_ref, own_middle_ref, own_ref, near_ref, far_ref, residual_ref,
-    wide_ref, rows_ref, sems,
+    place_ref, token_ref, heads_ref, gain_ref, own_ref, near_ref, far_ref, residual_ref, out_ref,
+    normed_ref, own_middle_ref, wide_ref, rows_ref,
 ):
     core = place_ref[1]
     tp = place_ref[2]
-    copies = fetch(
-        (own_hbm, near_hbm, far_hbm, residual_hbm), (own_ref, near_ref, far_ref, residual_ref), sems
-    )
-    copies[0].wait()
-    acc = dot(h0_ref[...], own_ref[...])
+    acc = dot(heads_ref[tp], own_ref[...])
     half = near_ref.shape[1]
-    heads = [ref[...] for ref in (h1_ref, h2_ref, h3_ref)]
-    copies[1].wait()
-    for k, head in enumerate(heads):
-        acc = acc + dot(jnp.where(core == 0, head[:, :half], head[:, half:]), near_ref[k])
-    copies[2].wait()
-    for k, head in enumerate(heads):
-        acc = acc + dot(jnp.where(core == 0, head[:, half:], head[:, :half]), far_ref[k])
-    copies[3].wait()
+    for k in range(3):
+        head = heads_ref[lax.rem(tp + 3 - k, 4)]
+        low, high = head[:, :half], head[:, half:]
+        acc = acc + dot(jnp.where(core == 0, low, high), near_ref[k])
+        acc = acc + dot(jnp.where(core == 0, high, low), far_ref[k])
     middle = (residual_ref[...].astype(F32) + acc).astype(BF16)
     full = middle.astype(F32)
     scale = lax.rsqrt(jnp.mean(full * full, axis=1, keepdims=True) + NORM_EPS)
@@ -338,10 +322,7 @@
         ref[...] = dot(hidden, down_ref[:, pl.ds(start, cols)]).astype(ref.dtype)
 
 
-def expert_kernel(
-    rows_ref, gate_hbm, up_hbm, down_hbm, out_ref, gate_ref, up_ref, down_ref, wide_ref, x_ref, sems
-):
-    copies = fetch((gate_hbm, up_hbm, down_hbm), (gate_ref, up_ref, down_ref), sems)
+def expert_kernel(rows_ref, gate_ref, up_ref, down_ref, out_ref, wide_ref, x_ref):
     width = gate_ref.shape[0]
     tiles = width // LANES
     block = CAP * tiles
@@ -360,13 +341,10 @@
                 pl.ds(m * tiles + i, sources, stride=PAD), :
             ].astype(BF16)
     x = x_ref[...]
-    copies[0].wait()
     gate = dot(x, gate_ref[...])
-    copies[1].wait()
     up = dot(x, up_ref[...])
     hidden = (gate * sigmoid(gate) * up).astype(BF16)
     cols = width // 4
-    copies[2].wait()
     for y in range(4):
         answer = dot(hidden, down_ref[:, y * cols : (y + 1) * cols])
         for m in range(CAP):
@@ -412,21 +390,19 @@
     out_ref[...] = (total + routed).astype(BF16)
 
 
-def call(kernel, out, *args, scalars=0, fetched=0, scratch=()):
+def call(kernel, out, *args, scalars=0, scratch=(), limit=16, inside=True, kept=True):
     smem = pl.BlockSpec(memory_space=pltpu.SMEM)
     vmem = pl.BlockSpec(memory_space=pltpu.VMEM)
-    hbm = pl.BlockSpec(memory_space=pl.ANY)
-    loaded = len(args) - scalars - fetched
-    scratch = list(scratch)
-    if fetched:
-        scratch = [pltpu.VMEM(a.shape, a.dtype) for a in args[-fetched:]] + scratch
-        scratch.append(pltpu.SemaphoreType.DMA((fetched,)))
+    args = list(args)
+    space = pltpu.VMEM if inside else pltpu.HBM
+    args[scalars:] = [pltpu.with_memory_space_constraint(a, space) for a in args[scalars:]]
     return pl.pallas_call(
         kernel,
-        out_shape=out,
-        in_specs=[smem] * scalars + [vmem] * loaded + [hbm] * fetched,
+        out_shape=jax.tree.map(lambda a: pltpu.VMEM(a.shape, a.dtype), out) if kept else out,
+        in_specs=[smem] * scalars + [vmem] * (len(args) - scalars),
         out_specs=jax.tree.map(lambda _: vmem, out),
-        scratch_shapes=scratch,
+        scratch_shapes=list(scratch),
+        compiler_params=pltpu.CompilerParams(vmem_limit_bytes=limit << 20),
     )(*args)
 
 
@@ -459,7 +435,7 @@
     maps, reads = call(
         local_kernel,
         (shape((2 * heads, 3 * CH // 4, 2 * CH), F32), shape((heads, tokens, 2 * CH), F32)),
-        receptance, key, value, decay, correction, mix,
+        receptance, key, value, decay, correction, mix, inside=False,
     )
     maps, output_rows = lax.optimization_barrier((maps, output_matrix))
     half = inner // 2
@@ -488,10 +464,10 @@
     far = turned(near, "c", 1)
     states = exchange(states, PLANE)
     mixed = call(
-        finish_kernel, shape((tokens, inner), BF16), states, reads, receptance, key,
+        finish_kernel, shape((4, tokens, inner), BF16), states, reads, receptance, key,
         value, correction, factor, mix, current, gain, bias,
     )
-    others = [turned(mixed, "tp", k) for k in (1, 2, 3)]
+    mixed = exchange(mixed, "tp")
     outgoing, normed, own_middle = call(
         project_kernel,
         (
@@ -499,10 +475,8 @@
             shape((tokens, width), BF16),
             shape((tokens, cols), BF16),
         ),
-        place, slot_token, mixed, *others, norm_gain.reshape(1, -1), output_matrix, near, far,
-        residual,
+        place, slot_token, mixed, norm_gain.reshape(1, -1), output_matrix, near, far, residual,
         scalars=2,
-        fetched=4,
         scratch=(
             pltpu.VMEM((tokens, width // LANES + 8, LANES), F32),
             pltpu.VMEM((tokens, width // LANES, LANES), BF16),
@@ -518,7 +492,6 @@
     answer = call(
         expert_kernel, shape(outgoing.shape, BF16), arrived, routed_gate[0],
         routed_up[0], routed_down[0],
-        fetched=3,
         scratch=(
             pltpu.VMEM((slots // CAP * PAD, LANES), F32),
             pltpu.VMEM((slots, width), BF16),
@@ -528,7 +501,7 @@
     return call(
         combine_kernel, shape((tokens, cols), BF16), back, slot_token, slot_weight,
         own_middle, *shared,
-        scratch=(pltpu.VMEM(back.shape, F32),),
+        scratch=(pltpu.VMEM(back.shape, F32),), kept=False,
     )
 
 

time: 185 us -> 171 us (0.924)
  Pallas kernels: 36.8 us -> 22.5 us
  waiting for transfers between devices: 44.3 us -> 47.1 us
  blocking collectives: 66 us -> 64 us
    pallas_call x9, Pallas kernels: 36.8 us -> 22.5 us  [call(): pl.pallas_call(kernel, out_shape=jax.tree.map(lambda a: pltpu.VMEM(a.shap...]
    all_to_all x2 -> x3, waiting for transfers between devices: 33.7 us -> 38.8 us  [exchange(): return lax.all_to_all(array, axes, split_axis=0, concat_axis=0, tiled=True)]
    all_to_all x2 -> x3, starting transfers between devices: 15.2 us -> 18.6 us  [exchange(): return lax.all_to_all(array, axes, split_axis=0, concat_axis=0, tiled=True)]
    ppermute x10 -> x7, starting transfers between devices: 15.4 us -> 12.2 us  [turned(): lax.ppermute(array, axis, [(i, (i + shift) % peers) for i in range(peers)])]
    ppermute x10 -> x7, waiting for transfers between devices: 10.6 us -> 8.25 us  [turned(): lax.ppermute(array, axis, [(i, (i + shift) % peers) for i in range(peers)])]
    all_to_all x3, blocking collectives: 66 us -> 64 us  [exchange(): return lax.all_to_all(array, axes, split_axis=0, concat_axis=0, tiled=True)]
    unnamed x28 -> x60, local copies, waits for them, and re-layouts: 4.52 us -> 3.87 us
  transfers between devices with their start and end apart: 12 -> 10, of which waited for: 5 -> 5; matrix products, arithmetic and copies ran while one was open for 1% -> 0% of each run, Pallas kernels for 7% -> 4%
where the time goes in v4:
time: 171 us; the launch traced here: 170 us
  blocking collectives  64 us (37%)
  waiting for transfers between devices  47.1 us (28%)
  starting transfers between devices  30.8 us (18%)
  Pallas kernels  22.5 us (13%)
  local copies, waits for them, and re-layouts  4.95 us (3%)
    all_to_all x3, blocking collectives, exchange(): return lax.all_to_all(array, axes, split_axis=0, concat_axis=0, tiled=True)  64 us
    all_to_all x3, waiting for transfers between devices, exchange(): return lax.all_to_all(array, axes, split_axis=0, concat_axis=0, tiled=True)  38.8 us
    pallas_call x9, Pallas kernels, call(): pl.pallas_call(kernel, out_shape=jax.tree.map(lambda a: pltpu.VMEM(a.shap...  22.5 us
    all_to_all x3, starting transfers between devices, exchange(): return lax.all_to_all(array, axes, split_axis=0, concat_axis=0, tiled=True)  18.6 us
    ppermute x7, starting transfers between devices, turned(): lax.ppermute(array, axis, [(i, (i + shift) % peers) for i in range(peers)])  12.2 us
    ppermute x7, waiting for transfers between devices, turned(): lax.ppermute(array, axis, [(i, (i + shift) % peers) for i in range(peers)])  8.25 us
    unnamed x60, local copies, waits for them, and re-layouts  3.87 us
  transfers between devices with their start and end apart: 10, of which 5 were waited for; matrix products, arithmetic and copies ran while one was open for 0% of the time, Pallas kernels for 4%

profile of v4, /device:TPU:1, one launch (start us, length us, event | category | flops | bytes accessed | tf_op | source)
XLA Modules:
  0.0 170.1 jit_solution(17222738155694070979)
XLA Ops:
  0.0 4.5 %shard_map.200 = (f32[8,48,128]{2,1,0:T(8,128)S(1)}, f32[4,128,128]{2,1,0:T(8,128)S(1)}) custom-call(bf16[128,256]{1,0:T(8,128)(2,1)} %r_ref.3, bf16[128,256]{1,0:T(8,128)(2,1)} %k_ref.3, bf16[128,256]{1,0:T(8,128)(2,1)} %v_ref.3, bf16[128,256]{1,0:T(8,128)(2,1)} %d_ref.1, bf16[128,256]{1,0:T(8,128)(2,1)} %c_ref.3, f32[1,256]{1,0:T(1,128)} %bitcast.25), custom_call_target="tpu_custom_call" | custom-call | tf_op jit(solution)/shard_map/pallas_call | solution.py:399
  4.5 0.7 copy-done.14
  5.2 1.1 constant_dynamic-slice_fusion
  6.3 3.6 %collective-permute-start.2 = (bf16[128,2048]{1,0:T(8,128)(2,1)S(1)}, bf16[128,2048]{1,0:T(8,128)(2,1)S(1)}, u32[]{:S(2)}, u32[]{:S(2)}) collective-permute-start(bf16[128,2048]{1,0:T(8,128)(2,1)S(1)} %constant_dynamic-slice_fusion), channel_id=1, source_target_pairs={{0,3},{1,0},{2,1},{3,2},{4,7},{5,4},{6,5},{7,6},{8,11},{9,8},{10,9... | collective-permute-start | bytes 1572872 | tf_op jit(solution)/shard_map/ppermute | solution.py:415
  9.9 0.4 collective-permute-start.1
  10.3 0.7 collective-permute-start
  11.0 11.7 %all_to_all.42.map_ref = f32[8,48,128]{2,1,0:T(8,128)S(1)} all-to-all(f32[8,48,128]{2,1,0:T(8,128)S(1)} %get-tuple-element.26), channel_id=1, replica_groups=mesh['z'=8,'x'=4,'c'=2,'tp'=4] {'x','c'}, dimensions={0} | all-to-all | bytes 393216 | tf_op jit(solution)/shard_map/all_to_all | solution.py:410
  22.7 1.4 shard_map.201
  24.2 8.2 %all-to-all-start.1 = ((f32[8,48,128]{2,1,0:T(8,128)}), f32[8,48,128]{2,1,0:T(8,128)S(1)}, u32[]{:S(2)}, u32[]{:S(2)}) async-start(f32[8,48,128]{2,1,0:T(8,128)} %get-tuple-element.28), calls=%async_computation.1 | async-start | bytes 393216 | tf_op jit(solution)/shard_map/all_to_all | solution.py:410
  32.3 0.1 pad_add_fusion.place_ref
  32.4 8.9 %all-to-all-done.1.total_ref = f32[8,48,128]{2,1,0:T(8,128)S(1)} async-done(((f32[8,48,128]{2,1,0:T(8,128)}), f32[8,48,128]{2,1,0:T(8,128)S(1)}, u32[]{:S(2)}, u32[]{:S(2)}) %all-to-all-start.1) | async-done | bytes 196640 | tf_op jit(solution)/shard_map/all_to_all | solution.py:410
  41.3 1.5 shard_map.202
  42.9 0.0 copy-start.10
  42.9 0.0 copy-start.11
  42.9 0.0 copy-start.13
  43.0 0.0 copy-start.16
  43.0 0.0 copy-start.25
  43.0 0.0 copy-start.26
  43.0 0.2 pad_maximum_fusion.near_ref
  43.2 0.0 copy-start.28
  43.2 0.0 copy-start
  43.3 0.0 copy-start.17
  43.3 2.5 %collective-permute-start.3 = (bf16[3,128,2048]{2,1,0:T(8,128)(2,1)S(1)}, bf16[3,128,2048]{2,1,0:T(8,128)(2,1)}, u32[]{:S(2)}, u32[]{:S(2)}) collective-permute-start(bf16[3,128,2048]{2,1,0:T(8,128)(2,1)S(1)} %pad_maximum_fusion.near_ref), channel_id=1, source_target_pairs={{0,4},{4,0},{1,5},{5,1},{2,6},{6,2},{3,7},{7,3},{8,12},{12,8},{9,1... | collective-permute-start | bytes 4718600 | tf_op jit(solution)/shard_map/ppermute | solution.py:415
  45.8 7.4 %all_to_all.43.state_ref = f32[8,16,128]{2,1,0:T(8,128)S(1)} all-to-all(f32[8,16,128]{2,1,0:T(8,128)S(1)} %shard_map.202), channel_id=1, replica_groups=mesh['z'=8,'x'=4,'c'=2,'tp'=4] {'x','c'}, dimensions={0} | all-to-all | bytes 131072 | tf_op jit(solution)/shard_map/all_to_all | solution.py:410
  53.2 1.9 %shard_map.203 = bf16[4,128,256]{2,1,0:T(8,128)(2,1)} custom-call(f32[8,16,128]{2,1,0:T(8,128)S(1)} %all_to_all.43.state_ref, f32[4,128,128]{2,1,0:T(8,128)S(1)} %copy-done.15, bf16[128,256]{1,0:T(8,128)(2,1)S(1)} %copy-done.10, bf16[128,256]{1,0:T(8,128)(2,1)S(1)} %copy-done.11, bf16[128,256]{1,0:T(8,128)(2,1)S(1)} %copy-done.12, ...), custom_call_target="tpu_custom_call" | custom-call | tf_op jit(solution)/shard_map/pallas_call | solution.py:399
  55.2 3.4 %all-to-all-start.3 = ((bf16[4,128,256]{2,1,0:T(8,128)(2,1)}), bf16[4,128,256]{2,1,0:T(8,128)(2,1)S(1)}, u32[]{:S(2)}, u32[]{:S(2)}) async-start(bf16[4,128,256]{2,1,0:T(8,128)(2,1)} %shard_map.203), calls=%async_computation.3 | async-start | bytes 524288 | tf_op jit(solution)/shard_map/all_to_all | solution.py:410
  58.6 0.1 copy.22.routes_ref
  58.7 0.1 copy.23.weight_ref
  58.8 0.7 shard_map.199
  59.5 0.0 copy-start.18
  59.5 0.6 copy-done.18
  60.1 4.0 %all-to-all-done.3.heads_ref = bf16[4,128,256]{2,1,0:T(8,128)(2,1)S(1)} async-done(((bf16[4,128,256]{2,1,0:T(8,128)(2,1)}), bf16[4,128,256]{2,1,0:T(8,128)(2,1)S(1)}, u32[]{:S(2)}, u32[]{:S(2)}) %all-to-all-start.3) | async-done | bytes 262176 | tf_op jit(solution)/shard_map/all_to_all | solution.py:410
  64.1 0.6 copy-done.21
  64.7 5.1 %shard_map.204 = (bf16[6144,128]{1,0:T(8,128)(2,1)S(1)}, bf16[128,2048]{1,0:T(8,128)(2,1)S(1)}, bf16[128,512]{1,0:T(8,128)(2,1)S(1)}) custom-call(s32[3]{0:T(128)S(1)} %copy-done.21, s32[6,256]{1,0:T(8,128)S(1)} %get-tuple-element.24.token_ref, bf16[4,128,256]{2,1,0:T(8,128)(2,1)S(1)} %all-to-all-done.3.heads_ref, f32[1,2048]{1,0:T(1,128)S(1)} %bitcast.24, ...), custom_call_target="tpu_custom_call" | custom-call | tf_op jit(solution)/shard_map/pallas_call | solution.py:399
  69.9 0.0 copy-start.1
  69.9 44.9 %all_to_all.44 = bf16[64,96,128]{2,1,0:T(8,128)(2,1)S(1)} all-to-all(bf16[64,96,128]{2,1,0:T(8,128)(2,1)S(1)} %bitcast.23), channel_id=1, replica_groups=mesh['z'=8,'x'=4,'c'=2,'tp'=4] {'z','x','c'}, dimensions={0} | all-to-all | bytes 3145728 | tf_op jit(solution)/shard_map/all_to_all | solution.py:410
  114.8 4.6 %shard_map.205 = bf16[6144,128]{1,0:T(8,128)(2,1)} custom-call(bf16[6144,128]{1,0:T(8,128)(2,1)S(1)} %bitcast.19, bf16[2048,512]{1,0:T(8,128)(2,1)S(1)} %bitcast.20, bf16[2048,512]{1,0:T(8,128)(2,1)S(1)} %bitcast.21, bf16[512,2048]{1,0:T(8,128)(2,1)S(1)} %bitcast.22), custom_call_target="tpu_custom_call" | custom-call | tf_op jit(solution)/shard_map/pallas_call | solution.py:399
  119.4 7.1 %all-to-all-start.5 = ((bf16[256,24,128]{2,1,0:T(8,128)(2,1)}), bf16[256,24,128]{2,1,0:T(8,128)(2,1)S(1)}, u32[]{:S(2)}, u32[]{:S(2)}) async-start(bf16[256,24,128]{2,1,0:T(8,128)(2,1)} %bitcast.16), calls=%async_computation.5 | async-start | bytes 3145728 | tf_op jit(solution)/shard_map/all_to_all | solution.py:410
  126.5 1.0 copy-done.9
  127.5 0.6 copy-done.22
  128.1 1.2 shard_map.206
  129.4 1.4 collective-permute-start.4
  130.8 2.5 %collective-permute-start.5 = (bf16[128,512]{1,0:T(8,128)(2,1)S(1)}, bf16[128,512]{1,0:T(8,128)(2,1)S(1)}, u32[]{:S(2)}, u32[]{:S(2)}) collective-permute-start(bf16[128,512]{1,0:T(8,128)(2,1)S(1)} %get-tuple-element.41), channel_id=1, source_target_pairs={{0,2},{1,3},{2,0},{3,1},{4,6},{5,7},{6,4},{7,5},{8,10},{9,11},{10,... | collective-permute-start | bytes 393224 | tf_op jit(solution)/shard_map/ppermute | solution.py:415
  133.2 1.1 collective-permute-start.6
  134.4 1.2 collective-permute-done.4.s1_ref
  135.6 7.0 %collective-permute-done.5.s2_ref = bf16[128,512]{1,0:T(8,128)(2,1)S(1)} collective-permute-done((bf16[128,512]{1,0:T(8,128)(2,1)S(1)}, bf16[128,512]{1,0:T(8,128)(2,1)S(1)}, u32[]{:S(2)}, u32[]{:S(2)}) %collective-permute-start.5) | collective-permute-done | bytes 131104 | tf_op jit(solution)/shard_map/ppermute | solution.py:415
  142.6 25.9 %all-to-all-done.5 = bf16[256,24,128]{2,1,0:T(8,128)(2,1)S(1)} async-done(((bf16[256,24,128]{2,1,0:T(8,128)(2,1)}), bf16[256,24,128]{2,1,0:T(8,128)(2,1)S(1)}, u32[]{:S(2)}, u32[]{:S(2)}) %all-to-all-start.5) | async-done | bytes 1572896 | tf_op jit(solution)/shard_map/all_to_all | solution.py:410
  168.5 1.6 shard_map.207
  (47 shorter events, 0.1 us)
Async XLA Ops:
  4.5 0.7 copy-start.14
  6.3 36.6 %collective-permute-start.2 = (bf16[128,2048]{1,0:T(8,128)(2,1)S(1)}, bf16[128,2048]{1,0:T(8,128)(2,1)S(1)}, u32[]{:S(2)}, u32[]{:S(2)}) collective-permute-start(bf16[128,2048]{1,0:T(8,128)(2,1)S(1)} %constant_dynamic-slice_fusion), channel_id=1, source_target_pairs={{0,3},{1,0},{2,1},{3,2},{4,7},{5,4},{6,5},{7,6},{8,11},{9,8},{10,9... | collective-permute-start | bytes 1572872 | tf_op jit(solution)/shard_map/ppermute | solution.py:415
  9.9 33.0 %collective-permute-start.1 = (bf16[128,2048]{1,0:T(8,128)(2,1)S(1)}, bf16[128,2048]{1,0:T(8,128)(2,1)S(1)}, u32[]{:S(2)}, u32[]{:S(2)}) collective-permute-start(bf16[128,2048]{1,0:T(8,128)(2,1)S(1)} %constant_dynamic-slice_fusion), channel_id=1, source_target_pairs={{0,2},{1,3},{2,0},{3,1},{4,6},{5,7},{6,4},{7,5},{8,10},{9,11},{10,... | collective-permute-start | bytes 1572872 | tf_op jit(solution)/shard_map/ppermute | solution.py:415
  10.3 32.6 %collective-permute-start = (bf16[128,2048]{1,0:T(8,128)(2,1)S(1)}, bf16[128,2048]{1,0:T(8,128)(2,1)S(1)}, u32[]{:S(2)}, u32[]{:S(2)}) collective-permute-start(bf16[128,2048]{1,0:T(8,128)(2,1)S(1)} %constant_dynamic-slice_fusion), channel_id=1, source_target_pairs={{0,1},{1,2},{2,3},{3,0},{4,5},{5,6},{6,7},{7,4},{8,9},{9,10},{10,1... | collective-permute-start | bytes 1572872 | tf_op jit(solution)/shard_map/ppermute | solution.py:415
  24.2 17.2 %all-to-all-start.1 = ((f32[8,48,128]{2,1,0:T(8,128)}), f32[8,48,128]{2,1,0:T(8,128)S(1)}, u32[]{:S(2)}, u32[]{:S(2)}) async-start(f32[8,48,128]{2,1,0:T(8,128)} %get-tuple-element.28), calls=%async_computation.1 | async-start | bytes 393216 | tf_op jit(solution)/shard_map/all_to_all | solution.py:410
  32.4 10.5 %copy-start.20 = (s32[3]{0:T(128)}, s32[3]{0:T(128)S(1)}, u32[]{:S(2)}) copy-start(s32[3]{0:T(128)S(1)} %pad_add_fusion.place_ref) | copy-start | bytes 40
  42.9 10.2 %copy-start.10 = (bf16[128,256]{1,0:T(8,128)(2,1)S(1)}, bf16[128,256]{1,0:T(8,128)(2,1)}, u32[]{:S(2)}) copy-start(bf16[128,256]{1,0:T(8,128)(2,1)} %r_ref.3) | copy-start | bytes 196612
  42.9 10.2 %copy-start.11 = (bf16[128,256]{1,0:T(8,128)(2,1)S(1)}, bf16[128,256]{1,0:T(8,128)(2,1)}, u32[]{:S(2)}) copy-start(bf16[128,256]{1,0:T(8,128)(2,1)} %k_ref.3) | copy-start | bytes 196612
  42.9 10.2 %copy-start.12 = (bf16[128,256]{1,0:T(8,128)(2,1)S(1)}, bf16[128,256]{1,0:T(8,128)(2,1)}, u32[]{:S(2)}) copy-start(bf16[128,256]{1,0:T(8,128)(2,1)} %v_ref.3) | copy-start | bytes 196612
  42.9 10.2 %copy-start.13 = (bf16[128,256]{1,0:T(8,128)(2,1)S(1)}, bf16[128,256]{1,0:T(8,128)(2,1)}, u32[]{:S(2)}) copy-start(bf16[128,256]{1,0:T(8,128)(2,1)} %c_ref.3) | copy-start | bytes 196612
  43.0 10.2 %copy-start.15 = (f32[4,128,128]{2,1,0:T(8,128)S(1)}, f32[4,128,128]{2,1,0:T(8,128)}, u32[]{:S(2)}) copy-start(f32[4,128,128]{2,1,0:T(8,128)} %copy-done.14) | copy-start | bytes 786436
  43.0 10.2 %copy-start.16 = (bf16[128,256]{1,0:T(8,128)(2,1)S(1)}, bf16[128,256]{1,0:T(8,128)(2,1)}, u32[]{:S(2)}) copy-start(bf16[128,256]{1,0:T(8,128)(2,1)} %f_ref.1) | copy-start | bytes 196612
  43.0 10.2 %copy-start.23 = (f32[256]{0:T(256)S(1)}, f32[256]{0:T(256)}, u32[]{:S(2)}) copy-start(f32[256]{0:T(256)} %param.27) | copy-start | bytes 3076
  43.0 10.2 %copy-start.24 = (f32[256]{0:T(256)S(1)}, f32[256]{0:T(256)}, u32[]{:S(2)}) copy-start(f32[256]{0:T(256)} %param.28) | copy-start | bytes 3076
  43.0 10.2 %copy-start.25 = (f32[256]{0:T(256)S(1)}, f32[256]{0:T(256)}, u32[]{:S(2)}) copy-start(f32[256]{0:T(256)} %param.29) | copy-start | bytes 3076
  43.0 10.2 %copy-start.26 = (f32[256]{0:T(256)S(1)}, f32[256]{0:T(256)}, u32[]{:S(2)}) copy-start(f32[256]{0:T(256)} %param.30) | copy-start | bytes 3076
  43.0 15.5 %copy-start.27 = (s32[128,8]{0,1:T(8,128)S(1)}, s32[128,8]{0,1:T(8,128)}, u32[]{:S(2)}) copy-start(s32[128,8]{0,1:T(8,128)} %param.34) | copy-start | bytes 12292
  43.2 15.5 %copy-start.28 = (f32[128,8]{0,1:T(8,128)S(1)}, f32[128,8]{0,1:T(8,128)}, u32[]{:S(2)}) copy-start(f32[128,8]{0,1:T(8,128)} %param.35) | copy-start | bytes 12292
  43.2 20.9 %copy-start = (bf16[256,2048]{1,0:T(8,128)(2,1)S(1)}, bf16[256,2048]{1,0:T(8,128)(2,1)}, u32[]{:S(2)}) copy-start(bf16[256,2048]{1,0:T(8,128)(2,1)} %own_ref.1) | copy-start | bytes 3145732
  43.2 20.9 %copy-start.4 = (bf16[128,2048]{1,0:T(8,128)(2,1)S(1)}, bf16[128,2048]{1,0:T(8,128)(2,1)}, u32[]{:S(2)}) copy-start(bf16[128,2048]{1,0:T(8,128)(2,1)} %residual_ref.1) | copy-start | bytes 1572868
  43.3 20.9 %copy-start.17 = (f32[2048]{0:T(1024)S(1)}, f32[2048]{0:T(1024)}, u32[]{:S(2)}) copy-start(f32[2048]{0:T(1024)} %param.33) | copy-start | bytes 24580
  43.3 20.8 %collective-permute-start.3 = (bf16[3,128,2048]{2,1,0:T(8,128)(2,1)S(1)}, bf16[3,128,2048]{2,1,0:T(8,128)(2,1)}, u32[]{:S(2)}, u32[]{:S(2)}) collective-permute-start(bf16[3,128,2048]{2,1,0:T(8,128)(2,1)S(1)} %pad_maximum_fusion.near_ref), channel_id=1, source_target_pairs={{0,4},{4,0},{1,5},{5,1},{2,6},{6,2},{3,7},{7,3},{8,12},{12,8},{9,1... | collective-permute-start | bytes 4718600 | tf_op jit(solution)/shard_map/ppermute | solution.py:415
  55.2 8.9 %all-to-all-start.3 = ((bf16[4,128,256]{2,1,0:T(8,128)(2,1)}), bf16[4,128,256]{2,1,0:T(8,128)(2,1)S(1)}, u32[]{:S(2)}, u32[]{:S(2)}) async-start(bf16[4,128,256]{2,1,0:T(8,128)(2,1)} %shard_map.203), calls=%async_computation.3 | async-start | bytes 524288 | tf_op jit(solution)/shard_map/all_to_all | solution.py:410
  59.5 0.6 copy-start.18
  64.1 0.6 copy-start.21
  64.7 50.1 %copy-start.2 = (bf16[1,2048,512]{2,1,0:T(8,128)(2,1)S(1)}, bf16[1,2048,512]{2,1,0:T(8,128)(2,1)}, u32[]{:S(2)}) copy-start(bf16[1,2048,512]{2,1,0:T(8,128)(2,1)} %param.37) | copy-start | bytes 6291460
  64.7 50.1 %copy-start.3 = (bf16[1,512,2048]{2,1,0:T(8,128)(2,1)S(1)}, bf16[1,512,2048]{2,1,0:T(8,128)(2,1)}, u32[]{:S(2)}) copy-start(bf16[1,512,2048]{2,1,0:T(8,128)(2,1)} %param.38) | copy-start | bytes 6291460
  69.9 44.9 %copy-start.8 = (bf16[128,2048]{1,0:T(8,128)(2,1)}, bf16[128,2048]{1,0:T(8,128)(2,1)S(1)}, u32[]{:S(2)}) copy-start(bf16[128,2048]{1,0:T(8,128)(2,1)S(1)} %get-tuple-element.38.normed_ref) | copy-start | bytes 1572868
  69.9 44.9 %copy-start.1 = (bf16[1,2048,512]{2,1,0:T(8,128)(2,1)S(1)}, bf16[1,2048,512]{2,1,0:T(8,128)(2,1)}, u32[]{:S(2)}) copy-start(bf16[1,2048,512]{2,1,0:T(8,128)(2,1)} %param.36) | copy-start | bytes 6291460
  119.4 7.1 %copy-start.5 = (bf16[2048,128]{1,0:T(8,128)(2,1)S(1)}, bf16[2048,128]{1,0:T(8,128)(2,1)}, u32[]{:S(2)}) copy-start(bf16[2048,128]{1,0:T(8,128)(2,1)} %gate_ref.1) | copy-start | bytes 1572868
  119.4 7.1 %copy-start.6 = (bf16[2048,128]{1,0:T(8,128)(2,1)S(1)}, bf16[2048,128]{1,0:T(8,128)(2,1)}, u32[]{:S(2)}) copy-start(bf16[2048,128]{1,0:T(8,128)(2,1)} %up_ref.1) | copy-start | bytes 1572868
  119.4 7.1 %copy-start.7 = (bf16[128,2048]{1,0:T(8,128)(2,1)S(1)}, bf16[128,2048]{1,0:T(8,128)(2,1)}, u32[]{:S(2)}) copy-start(bf16[128,2048]{1,0:T(8,128)(2,1)} %down_ref.1) | copy-start | bytes 1572868
  119.4 49.1 %all-to-all-start.5 = ((bf16[256,24,128]{2,1,0:T(8,128)(2,1)}), bf16[256,24,128]{2,1,0:T(8,128)(2,1)S(1)}, u32[]{:S(2)}, u32[]{:S(2)}) async-start(bf16[256,24,128]{2,1,0:T(8,128)(2,1)} %bitcast.16), calls=%async_computation.5 | async-start | bytes 3145728 | tf_op jit(solution)/shard_map/all_to_all | solution.py:410
  126.5 1.0 copy-start.9
  127.5 0.6 copy-start.22
  128.1 40.3 %copy-start.19 = (f32[6,256]{1,0:T(8,128)S(1)}, f32[6,256]{1,0:T(8,128)}, u32[]{:S(2)}) copy-start(f32[6,256]{1,0:T(8,128)} %copy-done.18) | copy-start | bytes 18436
  129.4 6.2 %collective-permute-start.4 = (bf16[128,512]{1,0:T(8,128)(2,1)S(1)}, bf16[128,512]{1,0:T(8,128)(2,1)S(1)}, u32[]{:S(2)}, u32[]{:S(2)}) collective-permute-start(bf16[128,512]{1,0:T(8,128)(2,1)S(1)} %get-tuple-element.40), channel_id=1, source_target_pairs={{0,1},{1,2},{2,3},{3,0},{4,5},{5,6},{6,7},{7,4},{8,9},{9,10},{10,1... | collective-permute-start | bytes 393224 | tf_op jit(solution)/shard_map/ppermute | solution.py:415
  130.8 11.8 %collective-permute-start.5 = (bf16[128,512]{1,0:T(8,128)(2,1)S(1)}, bf16[128,512]{1,0:T(8,128)(2,1)S(1)}, u32[]{:S(2)}, u32[]{:S(2)}) collective-permute-start(bf16[128,512]{1,0:T(8,128)(2,1)S(1)} %get-tuple-element.41), channel_id=1, source_target_pairs={{0,2},{1,3},{2,0},{3,1},{4,6},{5,7},{6,4},{7,5},{8,10},{9,11},{10,... | collective-permute-start | bytes 393224 | tf_op jit(solution)/shard_map/ppermute | solution.py:415
  133.2 9.4 %collective-permute-start.6 = (bf16[128,512]{1,0:T(8,128)(2,1)S(1)}, bf16[128,512]{1,0:T(8,128)(2,1)S(1)}, u32[]{:S(2)}, u32[]{:S(2)}) collective-permute-start(bf16[128,512]{1,0:T(8,128)(2,1)S(1)} %get-tuple-element.42), channel_id=1, source_target_pairs={{0,3},{1,0},{2,1},{3,2},{4,7},{5,4},{6,5},{7,6},{8,11},{9,8},{10,9... | collective-permute-start | bytes 393224 | tf_op jit(solution)/shard_map/ppermute | solution.py:415

commit v5 on v4

--- a/solution.py
+++ b/solution.py
@@ -161,29 +161,32 @@
         read_ref[h] = reads[h] + jnp.concatenate([asked[h], on_values[h][t:]], 1)
 
 
-def packed(state):
-    half = CH // 2
-    left = jnp.concatenate([state[:half, :CH], state[half:, :CH]], 1)
-    quarter = half // 2
-    pieces = []
-    for c in range(2):
-        cols = state[:, CH + c * half : CH + (c + 1) * half]
-        rows = [cols[i * quarter : (i + 1) * quarter] for i in range(4)]
-        pieces.append(jnp.concatenate([left, jnp.concatenate(rows, 1)], 0))
-    return pieces
-
-
-def repacked(state):
+def eye_of(width):
+    row, col = iotas(CH, width)
+    return jnp.where(row == col, 1.0, 0.0)
+
+
+def folded(state, cols):
     half = CH // 2
     quarter = half // 2
-    left = jnp.concatenate([state[:half, :CH], state[half:, :CH]], 1)
-    rows = [state[i * quarter : (i + 1) * quarter, CH:] for i in range(4)]
-    return jnp.concatenate([left, jnp.concatenate(rows, 1)], 0)
+    moved = state[:, :CH] - eye_of(CH)
+    left = jnp.concatenate([moved[:half], moved[half:]], 1)
+    rows = [state[i * quarter : (i + 1) * quarter, cols] for i in range(4)]
+    return jnp.concatenate([left, jnp.concatenate(rows, 1)], 0).astype(BF16)
+
+
+def packed(state):
+    return [folded(state, slice(CH + c * CH // 2, CH + (c + 1) * CH // 2)) for c in range(2)]
+
+
+def repacked(state):
+    return folded(state, slice(CH, None))
 
 
 def unpacked(block):
     half = CH // 2
-    left = jnp.concatenate([block[:half, :CH], block[:half, CH:]], 0)
+    block = block.astype(F32)
+    left = jnp.concatenate([block[:half, :CH], block[:half, CH:]], 0) + eye_of(CH)
     right = jnp.concatenate([block[half:, i * half : (i + 1) * half] for i in range(4)], 0)
     return jnp.concatenate([left, right], 1)
 
@@ -277,16 +280,29 @@
 ):
     core = place_ref[1]
     tp = place_ref[2]
-    acc = dot(heads_ref[tp], own_ref[...])
     half = near_ref.shape[1]
+    width = residual_ref.shape[1]
+    heads = [heads_ref[tp]]
     for k in range(3):
         head = heads_ref[lax.rem(tp + 3 - k, 4)]
         low, high = head[:, :half], head[:, half:]
-        acc = acc + dot(jnp.where(core == 0, low, high), near_ref[k])
-        acc = acc + dot(jnp.where(core == 0, high, low), far_ref[k])
-    middle = (residual_ref[...].astype(F32) + acc).astype(BF16)
+        heads += [jnp.where(core == 0, low, high), jnp.where(core == 0, high, low)]
+    pieces = []
+    squares = jnp.zeros((heads[0].shape[0], LANES), F32)
+    step = 2 * LANES
+    for start in range(0, width, step):
+        s = slice(start, start + step)
+        acc = residual_ref[:, s].astype(F32) + dot(heads[0], own_ref[:, s])
+        for k in range(3):
+            acc = acc + dot(heads[2 * k + 1], near_ref[k, :, s])
+            acc = acc + dot(heads[2 * k + 2], far_ref[k, :, s])
+        piece = acc.astype(BF16)
+        full = piece.astype(F32)
+        squares = squares + full[:, :LANES] * full[:, :LANES] + full[:, LANES:] * full[:, LANES:]
+        pieces.append(piece)
+    middle = jnp.concatenate(pieces, 1)
     full = middle.astype(F32)
-    scale = lax.rsqrt(jnp.mean(full * full, axis=1, keepdims=True) + NORM_EPS)
+    scale = lax.rsqrt(jnp.sum(squares, axis=1, keepdims=True) / width + NORM_EPS)
     normed = (full * scale * gain_ref[...]).astype(BF16)
     normed_ref[...] = normed
     cols = own_middle_ref.shape[1]
@@ -434,7 +450,7 @@
 
     maps, reads = call(
         local_kernel,
-        (shape((2 * heads, 3 * CH // 4, 2 * CH), F32), shape((heads, tokens, 2 * CH), F32)),
+        (shape((2 * heads, 3 * CH // 4, 2 * CH), BF16), shape((heads, tokens, 2 * CH), F32)),
         receptance, key, value, decay, correction, mix, inside=False,
     )
     maps, output_rows = lax.optimization_barrier((maps, output_matrix))
@@ -446,7 +462,7 @@
         plane_kernel,
         (
             shape((plane, CH, 3 * CH // 2), F32),
-            shape((z_count, 3 * CH // 4, 2 * CH), F32),
+            shape((z_count, 3 * CH // 4, 2 * CH), BF16),
         ),
         maps,
     )
@@ -459,10 +475,10 @@
         entering_kernel, shape((plane, CH // 4, 2 * CH), F32), place, before, totals,
         scalars=1,
     )
+    states = exchange(states, PLANE)
     states, *near = lax.optimization_barrier((states, *near))
     near = jnp.stack(near)
     far = turned(near, "c", 1)
-    states = exchange(states, PLANE)
     mixed = call(
         finish_kernel, shape((4, tokens, inner), BF16), states, reads, receptance, key,
         value, correction, factor, mix, current, gain, bias,

time: 171 us -> 169 us (0.988)
  no operation moved by 1% of the time
where the time goes in v5:
time: 169 us; the launch traced here: 168 us
  blocking collectives  64.9 us (38%)
  waiting for transfers between devices  45.7 us (27%)
  starting transfers between devices  29.3 us (17%)
  Pallas kernels  22.5 us (13%)
  local copies, waits for them, and re-layouts  4.95 us (3%)
    all_to_all x3, blocking collectives, exchange(): return lax.all_to_all(array, axes, split_axis=0, concat_axis=0, tiled=True)  64.9 us
    all_to_all x3, waiting for transfers between devices, exchange(): return lax.all_to_all(array, axes, split_axis=0, concat_axis=0, tiled=True)  37.4 us
    pallas_call x9, Pallas kernels, call(): pl.pallas_call(kernel, out_shape=jax.tree.map(lambda a: pltpu.VMEM(a.shap...  22.5 us
    all_to_all x3, starting transfers between devices, exchange(): return lax.all_to_all(array, axes, split_axis=0, concat_axis=0, tiled=True)  18.8 us
    ppermute x7, starting transfers between devices, turned(): lax.ppermute(array, axis, [(i, (i + shift) % peers) for i in range(peers)])  10.5 us
    ppermute x7, waiting for transfers between devices, turned(): lax.ppermute(array, axis, [(i, (i + shift) % peers) for i in range(peers)])  8.25 us
    unnamed x60, local copies, waits for them, and re-layouts  3.87 us
  transfers between devices with their start and end apart: 10, of which 5 were waited for; matrix products, arithmetic and copies ran while one was open for 0% of the time, Pallas kernels for 4%

profile of v5, /device:TPU:1, one launch (start us, length us, event | category | flops | bytes accessed | tf_op | source)
XLA Modules:
  0.0 168.1 jit_solution(5984102549275249096)
XLA Ops:
  0.0 4.5 %shard_map.200 = (bf16[8,48,128]{2,1,0:T(8,128)(2,1)S(1)}, f32[4,128,128]{2,1,0:T(8,128)S(1)}) custom-call(bf16[128,256]{1,0:T(8,128)(2,1)} %r_ref.3, bf16[128,256]{1,0:T(8,128)(2,1)} %k_ref.3, bf16[128,256]{1,0:T(8,128)(2,1)} %v_ref.3, bf16[128,256]{1,0:T(8,128)(2,1)} %d_ref.1, bf16[128,256]{1,0:T(8,128)(2,1)} %c_ref.3, f32[1,256]{1,0:T(1,128)} %bitcast.25), custom_call_target="tpu_custom_call" | custom-call | tf_op jit(solution)/shard_map/pallas_call | solution.py:415
  4.5 0.7 copy-done.14
  5.2 1.1 constant_dynamic-slice_fusion
  6.3 3.6 %collective-permute-start.2 = (bf16[128,2048]{1,0:T(8,128)(2,1)S(1)}, bf16[128,2048]{1,0:T(8,128)(2,1)S(1)}, u32[]{:S(2)}, u32[]{:S(2)}) collective-permute-start(bf16[128,2048]{1,0:T(8,128)(2,1)S(1)} %constant_dynamic-slice_fusion), channel_id=1, source_target_pairs={{0,3},{1,0},{2,1},{3,2},{4,7},{5,4},{6,5},{7,6},{8,11},{9,8},{10,9... | collective-permute-start | bytes 1572872 | tf_op jit(solution)/shard_map/ppermute | solution.py:431
  9.9 0.3 collective-permute-start.1
  10.3 0.7 collective-permute-start
  11.0 10.9 %all_to_all.42.map_ref = bf16[8,48,128]{2,1,0:T(8,128)(2,1)S(1)} all-to-all(bf16[8,48,128]{2,1,0:T(8,128)(2,1)S(1)} %get-tuple-element.26), channel_id=1, replica_groups=mesh['z'=8,'x'=4,'c'=2,'tp'=4] {'x','c'}, dimensions={0} | all-to-all | bytes 196608 | tf_op jit(solution)/shard_map/all_to_all | solution.py:426
  21.8 1.4 shard_map.201
  23.3 8.2 %all-to-all-start.1 = ((bf16[8,48,128]{2,1,0:T(8,128)(2,1)}), bf16[8,48,128]{2,1,0:T(8,128)(2,1)S(1)}, u32[]{:S(2)}, u32[]{:S(2)}) async-start(bf16[8,48,128]{2,1,0:T(8,128)(2,1)} %get-tuple-element.28), calls=%async_computation.1 | async-start | bytes 196608 | tf_op jit(solution)/shard_map/all_to_all | solution.py:426
  31.5 0.1 pad_add_fusion.place_ref
  31.5 7.4 %all-to-all-done.1.total_ref = bf16[8,48,128]{2,1,0:T(8,128)(2,1)S(1)} async-done(((bf16[8,48,128]{2,1,0:T(8,128)(2,1)}), bf16[8,48,128]{2,1,0:T(8,128)(2,1)S(1)}, u32[]{:S(2)}, u32[]{:S(2)}) %all-to-all-start.1) | async-done | bytes 98336 | tf_op jit(solution)/shard_map/all_to_all | solution.py:426
  38.9 1.5 shard_map.202
  40.5 9.3 %all_to_all.43.state_ref = f32[8,16,128]{2,1,0:T(8,128)S(1)} all-to-all(f32[8,16,128]{2,1,0:T(8,128)S(1)} %shard_map.202), channel_id=1, replica_groups=mesh['z'=8,'x'=4,'c'=2,'tp'=4] {'x','c'}, dimensions={0} | all-to-all | bytes 131072 | tf_op jit(solution)/shard_map/all_to_all | solution.py:426
  49.8 0.0 copy-start.10
  49.8 0.0 copy-start.11
  49.8 0.0 copy-start.12
  49.8 0.0 copy-start.13
  49.8 0.0 copy-start.16
  49.9 0.0 copy-start.23
  49.9 0.0 copy-start.24
  49.9 0.0 copy-start.25
  49.9 0.0 copy-start.28
  49.9 0.2 pad_maximum_fusion.near_ref
  50.1 0.0 copy-start.17
  50.1 0.9 collective-permute-start.3
  51.1 1.9 %shard_map.203 = bf16[4,128,256]{2,1,0:T(8,128)(2,1)} custom-call(f32[8,16,128]{2,1,0:T(8,128)S(1)} %all_to_all.43.state_ref, f32[4,128,128]{2,1,0:T(8,128)S(1)} %copy-done.15, bf16[128,256]{1,0:T(8,128)(2,1)S(1)} %copy-done.10, bf16[128,256]{1,0:T(8,128)(2,1)S(1)} %copy-done.11, bf16[128,256]{1,0:T(8,128)(2,1)S(1)} %copy-done.12, ...), custom_call_target="tpu_custom_call" | custom-call | tf_op jit(solution)/shard_map/pallas_call | solution.py:415
  53.0 3.4 %all-to-all-start.3 = ((bf16[4,128,256]{2,1,0:T(8,128)(2,1)}), bf16[4,128,256]{2,1,0:T(8,128)(2,1)S(1)}, u32[]{:S(2)}, u32[]{:S(2)}) async-start(bf16[4,128,256]{2,1,0:T(8,128)(2,1)} %shard_map.203), calls=%async_computation.3 | async-start | bytes 524288 | tf_op jit(solution)/shard_map/all_to_all | solution.py:426
  56.4 0.1 copy.22.routes_ref
  56.5 0.1 copy.23.weight_ref
  56.6 0.7 shard_map.199
  57.3 0.6 copy-done.18
  57.9 4.2 %all-to-all-done.3.heads_ref = bf16[4,128,256]{2,1,0:T(8,128)(2,1)S(1)} async-done(((bf16[4,128,256]{2,1,0:T(8,128)(2,1)}), bf16[4,128,256]{2,1,0:T(8,128)(2,1)S(1)}, u32[]{:S(2)}, u32[]{:S(2)}) %all-to-all-start.3) | async-done | bytes 262176 | tf_op jit(solution)/shard_map/all_to_all | solution.py:426
  62.1 0.6 copy-done.21
  62.7 5.1 %shard_map.204 = (bf16[6144,128]{1,0:T(8,128)(2,1)S(1)}, bf16[128,2048]{1,0:T(8,128)(2,1)S(1)}, bf16[128,512]{1,0:T(8,128)(2,1)S(1)}) custom-call(s32[3]{0:T(128)S(1)} %copy-done.21, s32[6,256]{1,0:T(8,128)S(1)} %get-tuple-element.24.token_ref, bf16[4,128,256]{2,1,0:T(8,128)(2,1)S(1)} %all-to-all-done.3.heads_ref, f32[1,2048]{1,0:T(1,128)S(1)} %bitcast.24, ...), custom_call_target="tpu_custom_call" | custom-call | tf_op jit(solution)/shard_map/pallas_call | solution.py:415
  67.9 0.0 copy-start.1
  67.9 44.8 %all_to_all.44 = bf16[64,96,128]{2,1,0:T(8,128)(2,1)S(1)} all-to-all(bf16[64,96,128]{2,1,0:T(8,128)(2,1)S(1)} %bitcast.23), channel_id=1, replica_groups=mesh['z'=8,'x'=4,'c'=2,'tp'=4] {'z','x','c'}, dimensions={0} | all-to-all | bytes 3145728 | tf_op jit(solution)/shard_map/all_to_all | solution.py:426
  112.7 4.6 %shard_map.205 = bf16[6144,128]{1,0:T(8,128)(2,1)} custom-call(bf16[6144,128]{1,0:T(8,128)(2,1)S(1)} %bitcast.19, bf16[2048,512]{1,0:T(8,128)(2,1)S(1)} %bitcast.20, bf16[2048,512]{1,0:T(8,128)(2,1)S(1)} %bitcast.21, bf16[512,2048]{1,0:T(8,128)(2,1)S(1)} %bitcast.22), custom_call_target="tpu_custom_call" | custom-call | tf_op jit(solution)/shard_map/pallas_call | solution.py:415
  117.2 7.2 %all-to-all-start.5 = ((bf16[256,24,128]{2,1,0:T(8,128)(2,1)}), bf16[256,24,128]{2,1,0:T(8,128)(2,1)S(1)}, u32[]{:S(2)}, u32[]{:S(2)}) async-start(bf16[256,24,128]{2,1,0:T(8,128)(2,1)} %bitcast.16), calls=%async_computation.5 | async-start | bytes 3145728 | tf_op jit(solution)/shard_map/all_to_all | solution.py:426
  124.5 1.0 copy-done.9
  125.5 0.6 copy-done.22
  126.1 1.2 shard_map.206
  127.4 1.4 collective-permute-start.4
  128.8 2.5 %collective-permute-start.5 = (bf16[128,512]{1,0:T(8,128)(2,1)S(1)}, bf16[128,512]{1,0:T(8,128)(2,1)S(1)}, u32[]{:S(2)}, u32[]{:S(2)}) collective-permute-start(bf16[128,512]{1,0:T(8,128)(2,1)S(1)} %get-tuple-element.41), channel_id=1, source_target_pairs={{0,2},{1,3},{2,0},{3,1},{4,6},{5,7},{6,4},{7,5},{8,10},{9,11},{10,... | collective-permute-start | bytes 393224 | tf_op jit(solution)/shard_map/ppermute | solution.py:431
  131.2 1.1 collective-permute-start.6
  132.4 1.2 collective-permute-done.4.s1_ref
  133.6 7.0 %collective-permute-done.5.s2_ref = bf16[128,512]{1,0:T(8,128)(2,1)S(1)} collective-permute-done((bf16[128,512]{1,0:T(8,128)(2,1)S(1)}, bf16[128,512]{1,0:T(8,128)(2,1)S(1)}, u32[]{:S(2)}, u32[]{:S(2)}) %collective-permute-start.5) | collective-permute-done | bytes 131104 | tf_op jit(solution)/shard_map/ppermute | solution.py:431
  140.6 25.9 %all-to-all-done.5 = bf16[256,24,128]{2,1,0:T(8,128)(2,1)S(1)} async-done(((bf16[256,24,128]{2,1,0:T(8,128)(2,1)}), bf16[256,24,128]{2,1,0:T(8,128)(2,1)S(1)}, u32[]{:S(2)}, u32[]{:S(2)}) %all-to-all-start.5) | async-done | bytes 1572896 | tf_op jit(solution)/shard_map/all_to_all | solution.py:426
  166.5 1.6 shard_map.207
  (47 shorter events, 0.1 us)
Async XLA Ops:
  4.5 0.7 copy-start.14
  6.3 43.5 %collective-permute-start.2 = (bf16[128,2048]{1,0:T(8,128)(2,1)S(1)}, bf16[128,2048]{1,0:T(8,128)(2,1)S(1)}, u32[]{:S(2)}, u32[]{:S(2)}) collective-permute-start(bf16[128,2048]{1,0:T(8,128)(2,1)S(1)} %constant_dynamic-slice_fusion), channel_id=1, source_target_pairs={{0,3},{1,0},{2,1},{3,2},{4,7},{5,4},{6,5},{7,6},{8,11},{9,8},{10,9... | collective-permute-start | bytes 1572872 | tf_op jit(solution)/shard_map/ppermute | solution.py:431
  9.9 39.8 %collective-permute-start.1 = (bf16[128,2048]{1,0:T(8,128)(2,1)S(1)}, bf16[128,2048]{1,0:T(8,128)(2,1)S(1)}, u32[]{:S(2)}, u32[]{:S(2)}) collective-permute-start(bf16[128,2048]{1,0:T(8,128)(2,1)S(1)} %constant_dynamic-slice_fusion), channel_id=1, source_target_pairs={{0,2},{1,3},{2,0},{3,1},{4,6},{5,7},{6,4},{7,5},{8,10},{9,11},{10,... | collective-permute-start | bytes 1572872 | tf_op jit(solution)/shard_map/ppermute | solution.py:431
  10.3 39.5 %collective-permute-start = (bf16[128,2048]{1,0:T(8,128)(2,1)S(1)}, bf16[128,2048]{1,0:T(8,128)(2,1)S(1)}, u32[]{:S(2)}, u32[]{:S(2)}) collective-permute-start(bf16[128,2048]{1,0:T(8,128)(2,1)S(1)} %constant_dynamic-slice_fusion), channel_id=1, source_target_pairs={{0,1},{1,2},{2,3},{3,0},{4,5},{5,6},{6,7},{7,4},{8,9},{9,10},{10,1... | collective-permute-start | bytes 1572872 | tf_op jit(solution)/shard_map/ppermute | solution.py:431
  23.3 15.6 %all-to-all-start.1 = ((bf16[8,48,128]{2,1,0:T(8,128)(2,1)}), bf16[8,48,128]{2,1,0:T(8,128)(2,1)S(1)}, u32[]{:S(2)}, u32[]{:S(2)}) async-start(bf16[8,48,128]{2,1,0:T(8,128)(2,1)} %get-tuple-element.28), calls=%async_computation.1 | async-start | bytes 196608 | tf_op jit(solution)/shard_map/all_to_all | solution.py:426
  31.5 18.2 %copy-start.20 = (s32[3]{0:T(128)}, s32[3]{0:T(128)S(1)}, u32[]{:S(2)}) copy-start(s32[3]{0:T(128)S(1)} %pad_add_fusion.place_ref) | copy-start | bytes 40
  49.8 1.2 copy-start.10
  49.8 1.2 copy-start.11
  49.8 1.2 copy-start.12
  49.8 1.2 copy-start.13
  49.8 1.2 copy-start.15
  49.8 1.2 copy-start.16
  49.9 1.2 copy-start.23
  49.9 1.2 copy-start.24
  49.9 1.2 copy-start.25
  49.9 1.2 copy-start.26
  49.9 6.5 %copy-start.27 = (s32[128,8]{0,1:T(8,128)S(1)}, s32[128,8]{0,1:T(8,128)}, u32[]{:S(2)}) copy-start(s32[128,8]{0,1:T(8,128)} %param.34) | copy-start | bytes 12292
  49.9 6.6 %copy-start.28 = (f32[128,8]{0,1:T(8,128)S(1)}, f32[128,8]{0,1:T(8,128)}, u32[]{:S(2)}) copy-start(f32[128,8]{0,1:T(8,128)} %param.35) | copy-start | bytes 12292
  50.1 12.0 %copy-start = (bf16[256,2048]{1,0:T(8,128)(2,1)S(1)}, bf16[256,2048]{1,0:T(8,128)(2,1)}, u32[]{:S(2)}) copy-start(bf16[256,2048]{1,0:T(8,128)(2,1)} %own_ref.1) | copy-start | bytes 3145732
  50.1 12.0 %copy-start.4 = (bf16[128,2048]{1,0:T(8,128)(2,1)S(1)}, bf16[128,2048]{1,0:T(8,128)(2,1)}, u32[]{:S(2)}) copy-start(bf16[128,2048]{1,0:T(8,128)(2,1)} %residual_ref.1) | copy-start | bytes 1572868
  50.1 12.0 %copy-start.17 = (f32[2048]{0:T(1024)S(1)}, f32[2048]{0:T(1024)}, u32[]{:S(2)}) copy-start(f32[2048]{0:T(1024)} %param.33) | copy-start | bytes 24580
  50.1 12.0 %collective-permute-start.3 = (bf16[3,128,2048]{2,1,0:T(8,128)(2,1)S(1)}, bf16[3,128,2048]{2,1,0:T(8,128)(2,1)}, u32[]{:S(2)}, u32[]{:S(2)}) collective-permute-start(bf16[3,128,2048]{2,1,0:T(8,128)(2,1)S(1)} %pad_maximum_fusion.near_ref), channel_id=1, source_target_pairs={{0,4},{4,0},{1,5},{5,1},{2,6},{6,2},{3,7},{7,3},{8,12},{12,8},{9,1... | collective-permute-start | bytes 4718600 | tf_op jit(solution)/shard_map/ppermute | solution.py:431
  53.0 9.1 %all-to-all-start.3 = ((bf16[4,128,256]{2,1,0:T(8,128)(2,1)}), bf16[4,128,256]{2,1,0:T(8,128)(2,1)S(1)}, u32[]{:S(2)}, u32[]{:S(2)}) async-start(bf16[4,128,256]{2,1,0:T(8,128)(2,1)} %shard_map.203), calls=%async_computation.3 | async-start | bytes 524288 | tf_op jit(solution)/shard_map/all_to_all | solution.py:426
  57.3 0.6 copy-start.18
  62.1 0.6 copy-start.21
  62.7 49.9 %copy-start.2 = (bf16[1,2048,512]{2,1,0:T(8,128)(2,1)S(1)}, bf16[1,2048,512]{2,1,0:T(8,128)(2,1)}, u32[]{:S(2)}) copy-start(bf16[1,2048,512]{2,1,0:T(8,128)(2,1)} %param.37) | copy-start | bytes 6291460
  62.7 49.9 %copy-start.3 = (bf16[1,512,2048]{2,1,0:T(8,128)(2,1)S(1)}, bf16[1,512,2048]{2,1,0:T(8,128)(2,1)}, u32[]{:S(2)}) copy-start(bf16[1,512,2048]{2,1,0:T(8,128)(2,1)} %param.38) | copy-start | bytes 6291460
  67.9 44.8 %copy-start.8 = (bf16[128,2048]{1,0:T(8,128)(2,1)}, bf16[128,2048]{1,0:T(8,128)(2,1)S(1)}, u32[]{:S(2)}) copy-start(bf16[128,2048]{1,0:T(8,128)(2,1)S(1)} %get-tuple-element.38.normed_ref) | copy-start | bytes 1572868
  67.9 44.8 %copy-start.1 = (bf16[1,2048,512]{2,1,0:T(8,128)(2,1)S(1)}, bf16[1,2048,512]{2,1,0:T(8,128)(2,1)}, u32[]{:S(2)}) copy-start(bf16[1,2048,512]{2,1,0:T(8,128)(2,1)} %param.36) | copy-start | bytes 6291460
  117.2 7.2 %copy-start.5 = (bf16[2048,128]{1,0:T(8,128)(2,1)S(1)}, bf16[2048,128]{1,0:T(8,128)(2,1)}, u32[]{:S(2)}) copy-start(bf16[2048,128]{1,0:T(8,128)(2,1)} %gate_ref.1) | copy-start | bytes 1572868
  117.2 7.2 %copy-start.6 = (bf16[2048,128]{1,0:T(8,128)(2,1)S(1)}, bf16[2048,128]{1,0:T(8,128)(2,1)}, u32[]{:S(2)}) copy-start(bf16[2048,128]{1,0:T(8,128)(2,1)} %up_ref.1) | copy-start | bytes 1572868
  117.2 7.2 %copy-start.7 = (bf16[128,2048]{1,0:T(8,128)(2,1)S(1)}, bf16[128,2048]{1,0:T(8,128)(2,1)}, u32[]{:S(2)}) copy-start(bf16[128,2048]{1,0:T(8,128)(2,1)} %down_ref.1) | copy-start | bytes 1572868
  117.2 49.2 %all-to-all-start.5 = ((bf16[256,24,128]{2,1,0:T(8,128)(2,1)}), bf16[256,24,128]{2,1,0:T(8,128)(2,1)S(1)}, u32[]{:S(2)}, u32[]{:S(2)}) async-start(bf16[256,24,128]{2,1,0:T(8,128)(2,1)} %bitcast.16), calls=%async_computation.5 | async-start | bytes 3145728 | tf_op jit(solution)/shard_map/all_to_all | solution.py:426
  124.5 1.0 copy-start.9
  125.5 0.6 copy-start.22
  126.1 40.3 %copy-start.19 = (f32[6,256]{1,0:T(8,128)S(1)}, f32[6,256]{1,0:T(8,128)}, u32[]{:S(2)}) copy-start(f32[6,256]{1,0:T(8,128)} %copy-done.18) | copy-start | bytes 18436
  127.4 6.2 %collective-permute-start.4 = (bf16[128,512]{1,0:T(8,128)(2,1)S(1)}, bf16[128,512]{1,0:T(8,128)(2,1)S(1)}, u32[]{:S(2)}, u32[]{:S(2)}) collective-permute-start(bf16[128,512]{1,0:T(8,128)(2,1)S(1)} %get-tuple-element.40), channel_id=1, source_target_pairs={{0,1},{1,2},{2,3},{3,0},{4,5},{5,6},{6,7},{7,4},{8,9},{9,10},{10,1... | collective-permute-start | bytes 393224 | tf_op jit(solution)/shard_map/ppermute | solution.py:431
  128.8 11.8 %collective-permute-start.5 = (bf16[128,512]{1,0:T(8,128)(2,1)S(1)}, bf16[128,512]{1,0:T(8,128)(2,1)S(1)}, u32[]{:S(2)}, u32[]{:S(2)}) collective-permute-start(bf16[128,512]{1,0:T(8,128)(2,1)S(1)} %get-tuple-element.41), channel_id=1, source_target_pairs={{0,2},{1,3},{2,0},{3,1},{4,6},{5,7},{6,4},{7,5},{8,10},{9,11},{10,... | collective-permute-start | bytes 393224 | tf_op jit(solution)/shard_map/ppermute | solution.py:431
  131.2 9.4 %collective-permute-start.6 = (bf16[128,512]{1,0:T(8,128)(2,1)S(1)}, bf16[128,512]{1,0:T(8,128)(2,1)S(1)}, u32[]{:S(2)}, u32[]{:S(2)}) collective-permute-start(bf16[128,512]{1,0:T(8,128)(2,1)S(1)} %get-tuple-element.42), channel_id=1, source_target_pairs={{0,3},{1,0},{2,1},{3,2},{4,7},{5,4},{6,5},{7,6},{8,11},{9,8},{10,9... | collective-permute-start | bytes 393224 | tf_op jit(solution)/shard_map/ppermute | solution.py:431

commit v6 on v5

--- a/solution.py
+++ b/solution.py
@@ -236,7 +236,7 @@
     quarter = CH // 4
     for q in range(count):
         pieces = [mine[q * CH + i * quarter : q * CH + (i + 1) * quarter] for i in range(4)]
-        out_ref[q] = jnp.concatenate(pieces, 1)
+        out_ref[q] = jnp.concatenate(pieces, 1).astype(BF16)
 
 
 def finish_kernel(
@@ -249,7 +249,7 @@
     weight = r_ref[...].astype(F32) * mixed * cur_ref[...]
     readouts = []
     for h in every:
-        even, odd = state_ref[2 * h], state_ref[2 * h + 1]
+        even, odd = state_ref[2 * h].astype(F32), state_ref[2 * h + 1].astype(F32)
         half = CH // 2
         state = jnp.concatenate(
             [
@@ -269,33 +269,32 @@
     bonus = jnp.concatenate([jnp.broadcast_to(b, wide) for b in bonuses], 1)
     grouped = jnp.concatenate(scaled, 1) * gain_ref[...] + bias_ref[...]
     out = (grouped + bonus * v_ref[...].astype(F32)) * f_ref[...].astype(F32)
-    out = out.astype(BF16)
-    for y in range(out_ref.shape[0]):
-        out_ref[y] = out
+    out_ref[...] = out.astype(BF16)
 
 
 def project_kernel(
-    place_ref, token_ref, heads_ref, gain_ref, own_ref, near_ref, far_ref, residual_ref, out_ref,
+    place_ref, token_ref, h0_ref, h1_ref, h2_ref, h3_ref, gain_ref, own_ref, near_ref, far_ref, residual_ref, out_ref,
     normed_ref, own_middle_ref, wide_ref, rows_ref,
 ):
     core = place_ref[1]
     tp = place_ref[2]
     half = near_ref.shape[1]
     width = residual_ref.shape[1]
-    heads = [heads_ref[tp]]
-    for k in range(3):
-        head = heads_ref[lax.rem(tp + 3 - k, 4)]
+    heads = [h0_ref[...]]
+    for ref in (h1_ref, h2_ref, h3_ref):
+        head = ref[...]
         low, high = head[:, :half], head[:, half:]
         heads += [jnp.where(core == 0, low, high), jnp.where(core == 0, high, low)]
+    heads = jnp.concatenate(heads, 1)
     pieces = []
-    squares = jnp.zeros((heads[0].shape[0], LANES), F32)
+    squares = jnp.zeros((heads.shape[0], LANES), F32)
     step = 2 * LANES
     for start in range(0, width, step):
         s = slice(start, start + step)
-        acc = residual_ref[:, s].astype(F32) + dot(heads[0], own_ref[:, s])
+        rows = [own_ref[:, s]]
         for k in range(3):
-            acc = acc + dot(heads[2 * k + 1], near_ref[k, :, s])
-            acc = acc + dot(heads[2 * k + 2], far_ref[k, :, s])
+            rows += [near_ref[k, :, s], far_ref[k, :, s]]
+        acc = residual_ref[:, s].astype(F32) + dot(heads, jnp.concatenate(rows, 0))
         piece = acc.astype(BF16)
         full = piece.astype(F32)
         squares = squares + full[:, :LANES] * full[:, :LANES] + full[:, LANES:] * full[:, LANES:]
@@ -472,7 +471,7 @@
         (shape((CAP, experts), jnp.int32), shape((CAP, experts), F32)), routes, chosen,
     )
     states = call(
-        entering_kernel, shape((plane, CH // 4, 2 * CH), F32), place, before, totals,
+        entering_kernel, shape((plane, CH // 4, 2 * CH), BF16), place, before, totals,
         scalars=1,
     )
     states = exchange(states, PLANE)
@@ -480,10 +479,10 @@
     near = jnp.stack(near)
     far = turned(near, "c", 1)
     mixed = call(
-        finish_kernel, shape((4, tokens, inner), BF16), states, reads, receptance, key,
+        finish_kernel, shape((tokens, inner), BF16), states, reads, receptance, key,
         value, correction, factor, mix, current, gain, bias,
     )
-    mixed = exchange(mixed, "tp")
+    others = [turned(mixed, "tp", k) for k in (1, 2, 3)]
     outgoing, normed, own_middle = call(
         project_kernel,
         (
@@ -491,7 +490,7 @@
             shape((tokens, width), BF16),
             shape((tokens, cols), BF16),
         ),
-        place, slot_token, mixed, norm_gain.reshape(1, -1), output_matrix, near, far, residual,
+        place, slot_token, mixed, *others, norm_gain.reshape(1, -1), output_matrix, near, far, residual,
         scalars=2,
         scratch=(
             pltpu.VMEM((tokens, width // LANES + 8, LANES), F32),

time: 169 us -> 169 us (level)
  local copies, waits for them, and re-layouts: 4.95 us -> 7.19 us
    all_to_all x3 -> x2, waiting for transfers between devices: 37.4 us -> 33.2 us  [exchange(): return lax.all_to_all(array, axes, split_axis=0, concat_axis=0, tiled=True)]
    ppermute x7 -> x10, starting transfers between devices: 10.5 us -> 14 us  [turned(): lax.ppermute(array, axis, [(i, (i + shift) % peers) for i in range(peers)])]
    all_to_all x3 -> x2, starting transfers between devices: 18.8 us -> 15.5 us  [exchange(): return lax.all_to_all(array, axes, split_axis=0, concat_axis=0, tiled=True)]
    ppermute x7 -> x10, waiting for transfers between devices: 8.25 us -> 11.4 us  [turned(): lax.ppermute(array, axis, [(i, (i + shift) % peers) for i in range(peers)])]
    unnamed x60 -> x64, local copies, waits for them, and re-layouts: 3.87 us -> 6.11 us
  transfers between devices with their start and end apart: 10 -> 12, of which waited for: 5 -> 6; matrix products, arithmetic and copies ran while one was open for 0% -> 0% of each run, Pallas kernels for 4% -> 3%
where the time goes in v6:
time: 169 us; the launch traced here: 168 us
  blocking collectives  63.7 us (38%)
  waiting for transfers between devices  44.7 us (26%)
  starting transfers between devices  29.5 us (17%)
  Pallas kernels  21.2 us (13%)
  local copies, waits for them, and re-layouts  7.19 us (4%)
  other arithmetic  1.74 us (1%)
    all_to_all x3, blocking collectives, exchange(): return lax.all_to_all(array, axes, split_axis=0, concat_axis=0, tiled=True)  63.7 us
    all_to_all x2, waiting for transfers between devices, exchange(): return lax.all_to_all(array, axes, split_axis=0, concat_axis=0, tiled=True)  33.2 us
    pallas_call x9, Pallas kernels, call(): pl.pallas_call(kernel, out_shape=jax.tree.map(lambda a: pltpu.VMEM(a.shap...  21.2 us
    all_to_all x2, starting transfers between devices, exchange(): return lax.all_to_all(array, axes, split_axis=0, concat_axis=0, tiled=True)  15.5 us
    ppermute x10, starting transfers between devices, turned(): lax.ppermute(array, axis, [(i, (i + shift) % peers) for i in range(peers)])  14 us
    ppermute x10, waiting for transfers between devices, turned(): lax.ppermute(array, axis, [(i, (i + shift) % peers) for i in range(peers)])  11.4 us
    unnamed x64, local copies, waits for them, and re-layouts  6.11 us
  transfers between devices with their start and end apart: 12, of which 6 were waited for; matrix products, arithmetic and copies ran while one was open for 0% of the time, Pallas kernels for 3%

profile of v6, /device:TPU:1, one launch (start us, length us, event | category | flops | bytes accessed | tf_op | source)
XLA Modules:
  0.0 168.3 jit_solution(17709815294040094843)
XLA Ops:
  0.0 4.5 %shard_map.200 = (bf16[8,48,128]{2,1,0:T(8,128)(2,1)S(1)}, f32[4,128,128]{2,1,0:T(8,128)S(1)}) custom-call(bf16[128,256]{1,0:T(8,128)(2,1)} %r_ref.3, bf16[128,256]{1,0:T(8,128)(2,1)} %k_ref.3, bf16[128,256]{1,0:T(8,128)(2,1)} %v_ref.3, bf16[128,256]{1,0:T(8,128)(2,1)} %d_ref.1, bf16[128,256]{1,0:T(8,128)(2,1)} %c_ref.3, f32[1,256]{1,0:T(1,128)} %bitcast.25), custom_call_target="tpu_custom_call" | custom-call | tf_op jit(solution)/shard_map/pallas_call | solution.py:414
  4.5 1.1 constant_dynamic-slice_fusion
  5.6 3.6 %collective-permute-start.2 = (bf16[128,2048]{1,0:T(8,128)(2,1)S(1)}, bf16[128,2048]{1,0:T(8,128)(2,1)}, u32[]{:S(2)}, u32[]{:S(2)}) collective-permute-start(bf16[128,2048]{1,0:T(8,128)(2,1)S(1)} %constant_dynamic-slice_fusion), channel_id=1, source_target_pairs={{0,3},{1,0},{2,1},{3,2},{4,7},{5,4},{6,5},{7,6},{8,11},{9,8},{10,9... | collective-permute-start | bytes 1572872 | tf_op jit(solution)/shard_map/ppermute | solution.py:430
  9.2 0.3 collective-permute-start.1
  9.6 0.7 collective-permute-start
  10.3 11.0 %all_to_all.37.map_ref = bf16[8,48,128]{2,1,0:T(8,128)(2,1)S(1)} all-to-all(bf16[8,48,128]{2,1,0:T(8,128)(2,1)S(1)} %get-tuple-element.26), channel_id=1, replica_groups=mesh['z'=8,'x'=4,'c'=2,'tp'=4] {'x','c'}, dimensions={0} | all-to-all | bytes 196608 | tf_op jit(solution)/shard_map/all_to_all | solution.py:425
  21.2 1.4 shard_map.201
  22.7 8.2 %all-to-all-start.1 = ((bf16[8,48,128]{2,1,0:T(8,128)(2,1)}), bf16[8,48,128]{2,1,0:T(8,128)(2,1)S(1)}, u32[]{:S(2)}, u32[]{:S(2)}) async-start(bf16[8,48,128]{2,1,0:T(8,128)(2,1)} %get-tuple-element.28), calls=%async_computation.1 | async-start | bytes 196608 | tf_op jit(solution)/shard_map/all_to_all | solution.py:425
  30.9 0.1 pad_add_fusion.place_ref
  30.9 7.4 %all-to-all-done.1.total_ref = bf16[8,48,128]{2,1,0:T(8,128)(2,1)S(1)} async-done(((bf16[8,48,128]{2,1,0:T(8,128)(2,1)}), bf16[8,48,128]{2,1,0:T(8,128)(2,1)S(1)}, u32[]{:S(2)}, u32[]{:S(2)}) %all-to-all-start.1) | async-done | bytes 98336 | tf_op jit(solution)/shard_map/all_to_all | solution.py:425
  38.3 1.5 shard_map.202
  39.9 9.1 %all_to_all.38.state_ref = bf16[8,16,128]{2,1,0:T(8,128)(2,1)S(1)} all-to-all(bf16[8,16,128]{2,1,0:T(8,128)(2,1)S(1)} %shard_map.202), channel_id=1, replica_groups=mesh['z'=8,'x'=4,'c'=2,'tp'=4] {'x','c'}, dimensions={0} | all-to-all | bytes 65536 | tf_op jit(solution)/shard_map/all_to_all | solution.py:425
  49.0 0.0 copy-start.10
  49.0 0.0 copy-start.13
  49.0 0.0 copy-start.18
  49.0 0.0 copy-start.27
  49.1 0.0 copy-start.28
  49.1 0.0 copy-start
  49.1 1.7 pad_maximum_fusion.near_ref
  50.8 0.8 collective-permute-start.6
  51.7 1.0 shard_map.203.h0_ref
  52.7 2.0 %collective-permute-start.5 = (bf16[128,256]{1,0:T(8,128)(2,1)S(1)}, bf16[128,256]{1,0:T(8,128)(2,1)S(1)}, u32[]{:S(2)}, u32[]{:S(2)}) collective-permute-start(bf16[128,256]{1,0:T(8,128)(2,1)S(1)} %shard_map.203.h0_ref), channel_id=1, source_target_pairs={{0,3},{1,0},{2,1},{3,2},{4,7},{5,4},{6,5},{7,6},{8,11},{9,8},{10,9... | collective-permute-start | bytes 196616 | tf_op jit(solution)/shard_map/ppermute | solution.py:430
  54.7 1.4 collective-permute-start.4
  56.2 0.1 copy.22.routes_ref
  56.3 0.1 copy.23.weight_ref
  56.4 0.7 shard_map.199
  57.0 0.6 copy-done.20
  57.6 1.7 %collective-permute-done.4.h2_ref = bf16[128,256]{1,0:T(8,128)(2,1)S(1)} collective-permute-done((bf16[128,256]{1,0:T(8,128)(2,1)S(1)}, bf16[128,256]{1,0:T(8,128)(2,1)S(1)}, u32[]{:S(2)}, u32[]{:S(2)}) %collective-permute-start.4) | collective-permute-done | bytes 65568 | tf_op jit(solution)/shard_map/ppermute | solution.py:430
  59.4 0.6 copy-done.14
  60.0 1.5 collective-permute-done.3.h1_ref
  61.5 0.6 copy-done.16
  62.1 0.8 copy-done.15
  63.0 0.8 copy-done.17
  63.8 0.6 copy-done.23
  64.4 4.8 %shard_map.204 = (bf16[6144,128]{1,0:T(8,128)(2,1)S(1)}, bf16[128,2048]{1,0:T(8,128)(2,1)S(1)}, bf16[128,512]{1,0:T(8,128)(2,1)S(1)}) custom-call(s32[3]{0:T(128)S(1)} %copy-done.23, s32[6,256]{1,0:T(8,128)S(1)} %get-tuple-element.24.token_ref, bf16[128,256]{1,0:T(8,128)(2,1)S(1)} %shard_map.203.h0_ref, bf16[128,256]{1,0:T(8,128)(2,1)S(1)} %copy-done.17, ...), custom_call_target="tpu_custom_call" | custom-call | tf_op jit(solution)/shard_map/pallas_call | solution.py:414
  69.2 43.6 %all_to_all.39 = bf16[64,96,128]{2,1,0:T(8,128)(2,1)S(1)} all-to-all(bf16[64,96,128]{2,1,0:T(8,128)(2,1)S(1)} %bitcast.23), channel_id=1, replica_groups=mesh['z'=8,'x'=4,'c'=2,'tp'=4] {'z','x','c'}, dimensions={0} | all-to-all | bytes 3145728 | tf_op jit(solution)/shard_map/all_to_all | solution.py:425
  112.8 4.6 %shard_map.205 = bf16[6144,128]{1,0:T(8,128)(2,1)} custom-call(bf16[6144,128]{1,0:T(8,128)(2,1)S(1)} %bitcast.19, bf16[2048,512]{1,0:T(8,128)(2,1)S(1)} %bitcast.20, bf16[2048,512]{1,0:T(8,128)(2,1)S(1)} %bitcast.21, bf16[512,2048]{1,0:T(8,128)(2,1)S(1)} %bitcast.22), custom_call_target="tpu_custom_call" | custom-call | tf_op jit(solution)/shard_map/pallas_call | solution.py:414
  117.4 7.3 %all-to-all-start.4 = ((bf16[256,24,128]{2,1,0:T(8,128)(2,1)}), bf16[256,24,128]{2,1,0:T(8,128)(2,1)S(1)}, u32[]{:S(2)}, u32[]{:S(2)}) async-start(bf16[256,24,128]{2,1,0:T(8,128)(2,1)} %bitcast.16), calls=%async_computation.4 | async-start | bytes 3145728 | tf_op jit(solution)/shard_map/all_to_all | solution.py:425
  124.8 1.0 copy-done.9
  125.8 0.6 copy-done.24
  126.4 1.2 shard_map.206
  127.6 1.4 collective-permute-start.7
  129.1 2.5 %collective-permute-start.8 = (bf16[128,512]{1,0:T(8,128)(2,1)S(1)}, bf16[128,512]{1,0:T(8,128)(2,1)S(1)}, u32[]{:S(2)}, u32[]{:S(2)}) collective-permute-start(bf16[128,512]{1,0:T(8,128)(2,1)S(1)} %get-tuple-element.41), channel_id=1, source_target_pairs={{0,2},{1,3},{2,0},{3,1},{4,6},{5,7},{6,4},{7,5},{8,10},{9,11},{10,... | collective-permute-start | bytes 393224 | tf_op jit(solution)/shard_map/ppermute | solution.py:430
  131.5 1.1 collective-permute-start.9
  132.7 1.2 collective-permute-done.7.s1_ref
  133.9 7.0 %collective-permute-done.8.s2_ref = bf16[128,512]{1,0:T(8,128)(2,1)S(1)} collective-permute-done((bf16[128,512]{1,0:T(8,128)(2,1)S(1)}, bf16[128,512]{1,0:T(8,128)(2,1)S(1)}, u32[]{:S(2)}, u32[]{:S(2)}) %collective-permute-start.8) | collective-permute-done | bytes 131104 | tf_op jit(solution)/shard_map/ppermute | solution.py:430
  140.9 25.9 %all-to-all-done.4 = bf16[256,24,128]{2,1,0:T(8,128)(2,1)S(1)} async-done(((bf16[256,24,128]{2,1,0:T(8,128)(2,1)}), bf16[256,24,128]{2,1,0:T(8,128)(2,1)S(1)}, u32[]{:S(2)}, u32[]{:S(2)}) %all-to-all-start.4) | async-done | bytes 1572896 | tf_op jit(solution)/shard_map/all_to_all | solution.py:425
  166.8 1.6 shard_map.207
  (55 shorter events, 0.1 us)
Async XLA Ops:
  5.6 43.3 %collective-permute-start.2 = (bf16[128,2048]{1,0:T(8,128)(2,1)S(1)}, bf16[128,2048]{1,0:T(8,128)(2,1)}, u32[]{:S(2)}, u32[]{:S(2)}) collective-permute-start(bf16[128,2048]{1,0:T(8,128)(2,1)S(1)} %constant_dynamic-slice_fusion), channel_id=1, source_target_pairs={{0,3},{1,0},{2,1},{3,2},{4,7},{5,4},{6,5},{7,6},{8,11},{9,8},{10,9... | collective-permute-start | bytes 1572872 | tf_op jit(solution)/shard_map/ppermute | solution.py:430
  9.2 39.7 %collective-permute-start.1 = (bf16[128,2048]{1,0:T(8,128)(2,1)S(1)}, bf16[128,2048]{1,0:T(8,128)(2,1)}, u32[]{:S(2)}, u32[]{:S(2)}) collective-permute-start(bf16[128,2048]{1,0:T(8,128)(2,1)S(1)} %constant_dynamic-slice_fusion), channel_id=1, source_target_pairs={{0,2},{1,3},{2,0},{3,1},{4,6},{5,7},{6,4},{7,5},{8,10},{9,11},{10,... | collective-permute-start | bytes 1572872 | tf_op jit(solution)/shard_map/ppermute | solution.py:430
  9.6 39.4 %collective-permute-start = (bf16[128,2048]{1,0:T(8,128)(2,1)S(1)}, bf16[128,2048]{1,0:T(8,128)(2,1)}, u32[]{:S(2)}, u32[]{:S(2)}) collective-permute-start(bf16[128,2048]{1,0:T(8,128)(2,1)S(1)} %constant_dynamic-slice_fusion), channel_id=1, source_target_pairs={{0,1},{1,2},{2,3},{3,0},{4,5},{5,6},{6,7},{7,4},{8,9},{9,10},{10,1... | collective-permute-start | bytes 1572872 | tf_op jit(solution)/shard_map/ppermute | solution.py:430
  22.7 15.6 %all-to-all-start.1 = ((bf16[8,48,128]{2,1,0:T(8,128)(2,1)}), bf16[8,48,128]{2,1,0:T(8,128)(2,1)S(1)}, u32[]{:S(2)}, u32[]{:S(2)}) async-start(bf16[8,48,128]{2,1,0:T(8,128)(2,1)} %get-tuple-element.28), calls=%async_computation.1 | async-start | bytes 196608 | tf_op jit(solution)/shard_map/all_to_all | solution.py:425
  30.9 18.0 %copy-start.22 = (s32[3]{0:T(128)}, s32[3]{0:T(128)S(1)}, u32[]{:S(2)}) copy-start(s32[3]{0:T(128)S(1)} %pad_add_fusion.place_ref) | copy-start | bytes 40
  49.0 2.7 %copy-start.10 = (bf16[128,256]{1,0:T(8,128)(2,1)S(1)}, bf16[128,256]{1,0:T(8,128)(2,1)}, u32[]{:S(2)}) copy-start(bf16[128,256]{1,0:T(8,128)(2,1)} %r_ref.3) | copy-start | bytes 196612
  49.0 2.7 %copy-start.11 = (bf16[128,256]{1,0:T(8,128)(2,1)S(1)}, bf16[128,256]{1,0:T(8,128)(2,1)}, u32[]{:S(2)}) copy-start(bf16[128,256]{1,0:T(8,128)(2,1)} %k_ref.3) | copy-start | bytes 196612
  49.0 2.6 %copy-start.12 = (bf16[128,256]{1,0:T(8,128)(2,1)S(1)}, bf16[128,256]{1,0:T(8,128)(2,1)}, u32[]{:S(2)}) copy-start(bf16[128,256]{1,0:T(8,128)(2,1)} %v_ref.3) | copy-start | bytes 196612
  49.0 2.6 %copy-start.13 = (bf16[128,256]{1,0:T(8,128)(2,1)S(1)}, bf16[128,256]{1,0:T(8,128)(2,1)}, u32[]{:S(2)}) copy-start(bf16[128,256]{1,0:T(8,128)(2,1)} %c_ref.3) | copy-start | bytes 196612
  49.0 2.6 %copy-start.18 = (bf16[128,256]{1,0:T(8,128)(2,1)S(1)}, bf16[128,256]{1,0:T(8,128)(2,1)}, u32[]{:S(2)}) copy-start(bf16[128,256]{1,0:T(8,128)(2,1)} %f_ref.1) | copy-start | bytes 196612
  49.0 2.6 %copy-start.25 = (f32[256]{0:T(256)S(1)}, f32[256]{0:T(256)}, u32[]{:S(2)}) copy-start(f32[256]{0:T(256)} %param.27) | copy-start | bytes 3076
  49.0 2.6 %copy-start.26 = (f32[256]{0:T(256)S(1)}, f32[256]{0:T(256)}, u32[]{:S(2)}) copy-start(f32[256]{0:T(256)} %param.28) | copy-start | bytes 3076
  49.0 2.6 %copy-start.27 = (f32[256]{0:T(256)S(1)}, f32[256]{0:T(256)}, u32[]{:S(2)}) copy-start(f32[256]{0:T(256)} %param.29) | copy-start | bytes 3076
  49.1 2.6 %copy-start.28 = (f32[256]{0:T(256)S(1)}, f32[256]{0:T(256)}, u32[]{:S(2)}) copy-start(f32[256]{0:T(256)} %param.30) | copy-start | bytes 3076
  49.1 7.1 %copy-start.29 = (s32[128,8]{0,1:T(8,128)S(1)}, s32[128,8]{0,1:T(8,128)}, u32[]{:S(2)}) copy-start(s32[128,8]{0,1:T(8,128)} %param.34) | copy-start | bytes 12292
  49.1 7.2 %copy-start.30 = (f32[128,8]{0,1:T(8,128)S(1)}, f32[128,8]{0,1:T(8,128)}, u32[]{:S(2)}) copy-start(f32[128,8]{0,1:T(8,128)} %param.35) | copy-start | bytes 12292
  49.1 13.0 %copy-start = (bf16[256,2048]{1,0:T(8,128)(2,1)S(1)}, bf16[256,2048]{1,0:T(8,128)(2,1)}, u32[]{:S(2)}) copy-start(bf16[256,2048]{1,0:T(8,128)(2,1)} %own_ref.1) | copy-start | bytes 3145732
  49.1 13.0 %copy-start.4 = (bf16[128,2048]{1,0:T(8,128)(2,1)S(1)}, bf16[128,2048]{1,0:T(8,128)(2,1)}, u32[]{:S(2)}) copy-start(bf16[128,2048]{1,0:T(8,128)(2,1)} %residual_ref.1) | copy-start | bytes 1572868
  49.1 13.0 %copy-start.19 = (f32[2048]{0:T(1024)S(1)}, f32[2048]{0:T(1024)}, u32[]{:S(2)}) copy-start(f32[2048]{0:T(1024)} %param.33) | copy-start | bytes 24580
  50.8 11.3 %collective-permute-start.6 = (bf16[3,128,2048]{2,1,0:T(8,128)(2,1)S(1)}, bf16[3,128,2048]{2,1,0:T(8,128)(2,1)}, u32[]{:S(2)}, u32[]{:S(2)}) collective-permute-start(bf16[3,128,2048]{2,1,0:T(8,128)(2,1)S(1)} %pad_maximum_fusion.near_ref), channel_id=1, source_target_pairs={{0,4},{4,0},{1,5},{5,1},{2,6},{6,2},{3,7},{7,3},{8,12},{12,8},{9,1... | collective-permute-start | bytes 4718600 | tf_op jit(solution)/shard_map/ppermute | solution.py:430
  52.7 4.9 %collective-permute-start.5 = (bf16[128,256]{1,0:T(8,128)(2,1)S(1)}, bf16[128,256]{1,0:T(8,128)(2,1)S(1)}, u32[]{:S(2)}, u32[]{:S(2)}) collective-permute-start(bf16[128,256]{1,0:T(8,128)(2,1)S(1)} %shard_map.203.h0_ref), channel_id=1, source_target_pairs={{0,3},{1,0},{2,1},{3,2},{4,7},{5,4},{6,5},{7,6},{8,11},{9,8},{10,9... | collective-permute-start | bytes 196616 | tf_op jit(solution)/shard_map/ppermute | solution.py:430
  54.7 4.6 %collective-permute-start.4 = (bf16[128,256]{1,0:T(8,128)(2,1)S(1)}, bf16[128,256]{1,0:T(8,128)(2,1)S(1)}, u32[]{:S(2)}, u32[]{:S(2)}) collective-permute-start(bf16[128,256]{1,0:T(8,128)(2,1)S(1)} %shard_map.203.h0_ref), channel_id=1, source_target_pairs={{0,2},{1,3},{2,0},{3,1},{4,6},{5,7},{6,4},{7,5},{8,10},{9,11},{10,... | collective-permute-start | bytes 196616 | tf_op jit(solution)/shard_map/ppermute | solution.py:430
  56.2 5.3 %collective-permute-start.3 = (bf16[128,256]{1,0:T(8,128)(2,1)S(1)}, bf16[128,256]{1,0:T(8,128)(2,1)S(1)}, u32[]{:S(2)}, u32[]{:S(2)}) collective-permute-start(bf16[128,256]{1,0:T(8,128)(2,1)S(1)} %shard_map.203.h0_ref), channel_id=1, source_target_pairs={{0,1},{1,2},{2,3},{3,0},{4,5},{5,6},{6,7},{7,4},{8,9},{9,10},{10,1... | collective-permute-start | bytes 196616 | tf_op jit(solution)/shard_map/ppermute | solution.py:430
  57.0 0.6 copy-start.20
  59.4 0.6 copy-start.14
  61.5 0.6 copy-start.16
  62.1 0.8 copy-start.15
  63.0 0.8 copy-start.17
  63.8 0.6 copy-start.23
  64.4 48.4 %copy-start.2 = (bf16[1,2048,512]{2,1,0:T(8,128)(2,1)S(1)}, bf16[1,2048,512]{2,1,0:T(8,128)(2,1)}, u32[]{:S(2)}) copy-start(bf16[1,2048,512]{2,1,0:T(8,128)(2,1)} %param.37) | copy-start | bytes 6291460
  64.4 48.4 %copy-start.3 = (bf16[1,512,2048]{2,1,0:T(8,128)(2,1)S(1)}, bf16[1,512,2048]{2,1,0:T(8,128)(2,1)}, u32[]{:S(2)}) copy-start(bf16[1,512,2048]{2,1,0:T(8,128)(2,1)} %param.38) | copy-start | bytes 6291460
  69.2 43.6 %copy-start.8 = (bf16[128,2048]{1,0:T(8,128)(2,1)}, bf16[128,2048]{1,0:T(8,128)(2,1)S(1)}, u32[]{:S(2)}) copy-start(bf16[128,2048]{1,0:T(8,128)(2,1)S(1)} %get-tuple-element.38.normed_ref) | copy-start | bytes 1572868
  69.2 43.6 %copy-start.1 = (bf16[1,2048,512]{2,1,0:T(8,128)(2,1)S(1)}, bf16[1,2048,512]{2,1,0:T(8,128)(2,1)}, u32[]{:S(2)}) copy-start(bf16[1,2048,512]{2,1,0:T(8,128)(2,1)} %param.36) | copy-start | bytes 6291460
  117.4 7.3 %copy-start.5 = (bf16[2048,128]{1,0:T(8,128)(2,1)S(1)}, bf16[2048,128]{1,0:T(8,128)(2,1)}, u32[]{:S(2)}) copy-start(bf16[2048,128]{1,0:T(8,128)(2,1)} %gate_ref.1) | copy-start | bytes 1572868
  117.4 7.4 %copy-start.6 = (bf16[2048,128]{1,0:T(8,128)(2,1)S(1)}, bf16[2048,128]{1,0:T(8,128)(2,1)}, u32[]{:S(2)}) copy-start(bf16[2048,128]{1,0:T(8,128)(2,1)} %up_ref.1) | copy-start | bytes 1572868
  117.4 7.4 %copy-start.7 = (bf16[128,2048]{1,0:T(8,128)(2,1)S(1)}, bf16[128,2048]{1,0:T(8,128)(2,1)}, u32[]{:S(2)}) copy-start(bf16[128,2048]{1,0:T(8,128)(2,1)} %down_ref.1) | copy-start | bytes 1572868
  117.4 49.4 %all-to-all-start.4 = ((bf16[256,24,128]{2,1,0:T(8,128)(2,1)}), bf16[256,24,128]{2,1,0:T(8,128)(2,1)S(1)}, u32[]{:S(2)}, u32[]{:S(2)}) async-start(bf16[256,24,128]{2,1,0:T(8,128)(2,1)} %bitcast.16), calls=%async_computation.4 | async-start | bytes 3145728 | tf_op jit(solution)/shard_map/all_to_all | solution.py:425
  124.8 1.0 copy-start.9
  125.8 0.6 copy-start.24
  126.4 40.3 %copy-start.21 = (f32[6,256]{1,0:T(8,128)S(1)}, f32[6,256]{1,0:T(8,128)}, u32[]{:S(2)}) copy-start(f32[6,256]{1,0:T(8,128)} %copy-done.20) | copy-start | bytes 18436
  127.6 6.2 %collective-permute-start.7 = (bf16[128,512]{1,0:T(8,128)(2,1)S(1)}, bf16[128,512]{1,0:T(8,128)(2,1)S(1)}, u32[]{:S(2)}, u32[]{:S(2)}) collective-permute-start(bf16[128,512]{1,0:T(8,128)(2,1)S(1)} %get-tuple-element.40), channel_id=1, source_target_pairs={{0,1},{1,2},{2,3},{3,0},{4,5},{5,6},{6,7},{7,4},{8,9},{9,10},{10,1... | collective-permute-start | bytes 393224 | tf_op jit(solution)/shard_map/ppermute | solution.py:430
  129.1 11.8 %collective-permute-start.8 = (bf16[128,512]{1,0:T(8,128)(2,1)S(1)}, bf16[128,512]{1,0:T(8,128)(2,1)S(1)}, u32[]{:S(2)}, u32[]{:S(2)}) collective-permute-start(bf16[128,512]{1,0:T(8,128)(2,1)S(1)} %get-tuple-element.41), channel_id=1, source_target_pairs={{0,2},{1,3},{2,0},{3,1},{4,6},{5,7},{6,4},{7,5},{8,10},{9,11},{10,... | collective-permute-start | bytes 393224 | tf_op jit(solution)/shard_map/ppermute | solution.py:430
  131.5 9.4 %collective-permute-start.9 = (bf16[128,512]{1,0:T(8,128)(2,1)S(1)}, bf16[128,512]{1,0:T(8,128)(2,1)S(1)}, u32[]{:S(2)}, u32[]{:S(2)}) collective-permute-start(bf16[128,512]{1,0:T(8,128)(2,1)S(1)} %get-tuple-element.42), channel_id=1, source_target_pairs={{0,3},{1,0},{2,1},{3,2},{4,7},{5,4},{6,5},{7,6},{8,11},{9,8},{10,9... | collective-permute-start | bytes 393224 | tf_op jit(solution)/shard_map/ppermute | solution.py:430

commit v7 on v6

--- a/solution.py
+++ b/solution.py
@@ -475,14 +475,16 @@
         scalars=1,
     )
     states = exchange(states, PLANE)
-    states, *near = lax.optimization_barrier((states, *near))
-    near = jnp.stack(near)
-    far = turned(near, "c", 1)
     mixed = call(
         finish_kernel, shape((tokens, inner), BF16), states, reads, receptance, key,
         value, correction, factor, mix, current, gain, bias,
     )
-    others = [turned(mixed, "tp", k) for k in (1, 2, 3)]
+    others = []
+    for k in (1, 2, 3):
+        others.append(turned(mixed, "tp", k))
+    _, *near = lax.optimization_barrier((mixed, *near))
+    near = jnp.stack(near)
+    far = turned(near, "c", 1)
     outgoing, normed, own_middle = call(
         project_kernel,
         (

time: 169 us -> 169 us (level)
  no operation moved by 1% of the time
where the time goes in v7:
time: 169 us; the launch traced here: 168 us
  blocking collectives  63.7 us (38%)
  waiting for transfers between devices  44.7 us (26%)
  starting transfers between devices  29.4 us (17%)
  Pallas kernels  21.4 us (13%)
  local copies, waits for them, and re-layouts  7.17 us (4%)
  other arithmetic  1.72 us (1%)
    all_to_all x3, blocking collectives, exchange(): return lax.all_to_all(array, axes, split_axis=0, concat_axis=0, tiled=True)  63.7 us
    all_to_all x2, waiting for transfers between devices, exchange(): return lax.all_to_all(array, axes, split_axis=0, concat_axis=0, tiled=True)  33.2 us
    pallas_call x9, Pallas kernels, call(): pl.pallas_call(kernel, out_shape=jax.tree.map(lambda a: pltpu.VMEM(a.shap...  21.4 us
    all_to_all x2, starting transfers between devices, exchange(): return lax.all_to_all(array, axes, split_axis=0, concat_axis=0, tiled=True)  15.5 us
    ppermute x10, starting transfers between devices, turned(): lax.ppermute(array, axis, [(i, (i + shift) % peers) for i in range(peers)])  13.9 us
    ppermute x10, waiting for transfers between devices, turned(): lax.ppermute(array, axis, [(i, (i + shift) % peers) for i in range(peers)])  11.5 us
    unnamed x64, local copies, waits for them, and re-layouts  6.09 us
  transfers between devices with their start and end apart: 12, of which 6 were waited for; matrix products, arithmetic and copies ran while one was open for 0% of the time, Pallas kernels for 3%

profile of v7, /device:TPU:1, one launch (start us, length us, event | category | flops | bytes accessed | tf_op | source)
XLA Modules:
  0.0 168.4 jit_solution(9834294145115250484)
XLA Ops:
  0.1 4.6 %shard_map.200 = (bf16[8,48,128]{2,1,0:T(8,128)(2,1)S(1)}, f32[4,128,128]{2,1,0:T(8,128)S(1)}) custom-call(bf16[128,256]{1,0:T(8,128)(2,1)} %r_ref.3, bf16[128,256]{1,0:T(8,128)(2,1)} %k_ref.3, bf16[128,256]{1,0:T(8,128)(2,1)} %v_ref.3, bf16[128,256]{1,0:T(8,128)(2,1)} %d_ref.1, bf16[128,256]{1,0:T(8,128)(2,1)} %c_ref.3, f32[1,256]{1,0:T(1,128)} %bitcast.25), custom_call_target="tpu_custom_call" | custom-call | tf_op jit(solution)/shard_map/pallas_call | solution.py:414
  4.7 1.1 constant_dynamic-slice_fusion
  5.8 3.6 %collective-permute-start.5 = (bf16[128,2048]{1,0:T(8,128)(2,1)S(1)}, bf16[128,2048]{1,0:T(8,128)(2,1)}, u32[]{:S(2)}, u32[]{:S(2)}) collective-permute-start(bf16[128,2048]{1,0:T(8,128)(2,1)S(1)} %constant_dynamic-slice_fusion), channel_id=1, source_target_pairs={{0,3},{1,0},{2,1},{3,2},{4,7},{5,4},{6,5},{7,6},{8,11},{9,8},{10,9... | collective-permute-start | bytes 1572872 | tf_op jit(solution)/shard_map/ppermute | solution.py:430
  9.4 0.4 collective-permute-start.4
  9.8 0.7 collective-permute-start.3
  10.5 11.0 %all_to_all.37.map_ref = bf16[8,48,128]{2,1,0:T(8,128)(2,1)S(1)} all-to-all(bf16[8,48,128]{2,1,0:T(8,128)(2,1)S(1)} %get-tuple-element.25), channel_id=1, replica_groups=mesh['z'=8,'x'=4,'c'=2,'tp'=4] {'x','c'}, dimensions={0} | all-to-all | bytes 196608 | tf_op jit(solution)/shard_map/all_to_all | solution.py:425
  21.5 1.4 shard_map.201
  22.9 8.2 %all-to-all-start.1 = ((bf16[8,48,128]{2,1,0:T(8,128)(2,1)}), bf16[8,48,128]{2,1,0:T(8,128)(2,1)S(1)}, u32[]{:S(2)}, u32[]{:S(2)}) async-start(bf16[8,48,128]{2,1,0:T(8,128)(2,1)} %get-tuple-element.27), calls=%async_computation.1 | async-start | bytes 196608 | tf_op jit(solution)/shard_map/all_to_all | solution.py:425
  31.1 0.1 pad_add_fusion.place_ref
  31.2 7.4 %all-to-all-done.1.total_ref = bf16[8,48,128]{2,1,0:T(8,128)(2,1)S(1)} async-done(((bf16[8,48,128]{2,1,0:T(8,128)(2,1)}), bf16[8,48,128]{2,1,0:T(8,128)(2,1)S(1)}, u32[]{:S(2)}, u32[]{:S(2)}) %all-to-all-start.1) | async-done | bytes 98336 | tf_op jit(solution)/shard_map/all_to_all | solution.py:425
  38.5 1.5 shard_map.202
  40.1 9.1 %all_to_all.38.state_ref = bf16[8,16,128]{2,1,0:T(8,128)(2,1)S(1)} all-to-all(bf16[8,16,128]{2,1,0:T(8,128)(2,1)S(1)} %shard_map.202), channel_id=1, replica_groups=mesh['z'=8,'x'=4,'c'=2,'tp'=4] {'x','c'}, dimensions={0} | all-to-all | bytes 65536 | tf_op jit(solution)/shard_map/all_to_all | solution.py:425
  49.2 1.0 shard_map.203.h0_ref
  50.3 0.0 copy-start.29
  50.3 0.0 copy-start.30
  50.3 0.0 copy-start
  50.3 0.0 copy-start.4
  50.3 0.0 copy-start.19
  50.3 1.6 pad_maximum_fusion.near_ref
  52.0 0.8 collective-permute-start.6
  52.8 2.0 %collective-permute-start.2 = (bf16[128,256]{1,0:T(8,128)(2,1)S(1)}, bf16[128,256]{1,0:T(8,128)(2,1)S(1)}, u32[]{:S(2)}, u32[]{:S(2)}) collective-permute-start(bf16[128,256]{1,0:T(8,128)(2,1)S(1)} %shard_map.203.h0_ref), channel_id=1, source_target_pairs={{0,3},{1,0},{2,1},{3,2},{4,7},{5,4},{6,5},{7,6},{8,11},{9,8},{10,9... | collective-permute-start | bytes 196616 | tf_op jit(solution)/shard_map/ppermute | solution.py:430
  54.8 1.4 collective-permute-start.1
  56.2 0.1 copy.22.routes_ref
  56.3 0.1 copy.23.weight_ref
  56.4 0.7 shard_map.199
  57.1 0.6 copy-done.20
  57.7 1.7 %collective-permute-done.1.h2_ref = bf16[128,256]{1,0:T(8,128)(2,1)S(1)} collective-permute-done((bf16[128,256]{1,0:T(8,128)(2,1)S(1)}, bf16[128,256]{1,0:T(8,128)(2,1)S(1)}, u32[]{:S(2)}, u32[]{:S(2)}) %collective-permute-start.1) | collective-permute-done | bytes 65568 | tf_op jit(solution)/shard_map/ppermute | solution.py:430
  59.4 0.6 copy-done.14
  60.0 1.5 collective-permute-done.h1_ref
  61.5 0.6 copy-done.16
  62.2 0.8 copy-done.15
  63.0 0.8 copy-done.17
  63.9 0.6 copy-done.23
  64.5 4.7 %shard_map.204 = (bf16[6144,128]{1,0:T(8,128)(2,1)S(1)}, bf16[128,2048]{1,0:T(8,128)(2,1)S(1)}, bf16[128,512]{1,0:T(8,128)(2,1)S(1)}) custom-call(s32[3]{0:T(128)S(1)} %copy-done.23, s32[6,256]{1,0:T(8,128)S(1)} %get-tuple-element.23.token_ref, bf16[128,256]{1,0:T(8,128)(2,1)S(1)} %shard_map.203.h0_ref, bf16[128,256]{1,0:T(8,128)(2,1)S(1)} %copy-done.17, ...), custom_call_target="tpu_custom_call" | custom-call | tf_op jit(solution)/shard_map/pallas_call | solution.py:414
  69.2 0.0 copy-start.1
  69.2 43.6 %all_to_all.39 = bf16[64,96,128]{2,1,0:T(8,128)(2,1)S(1)} all-to-all(bf16[64,96,128]{2,1,0:T(8,128)(2,1)S(1)} %bitcast.23), channel_id=1, replica_groups=mesh['z'=8,'x'=4,'c'=2,'tp'=4] {'z','x','c'}, dimensions={0} | all-to-all | bytes 3145728 | tf_op jit(solution)/shard_map/all_to_all | solution.py:425
  112.9 4.6 %shard_map.205 = bf16[6144,128]{1,0:T(8,128)(2,1)} custom-call(bf16[6144,128]{1,0:T(8,128)(2,1)S(1)} %bitcast.19, bf16[2048,512]{1,0:T(8,128)(2,1)S(1)} %bitcast.20, bf16[2048,512]{1,0:T(8,128)(2,1)S(1)} %bitcast.21, bf16[512,2048]{1,0:T(8,128)(2,1)S(1)} %bitcast.22), custom_call_target="tpu_custom_call" | custom-call | tf_op jit(solution)/shard_map/pallas_call | solution.py:414
  117.5 7.3 %all-to-all-start.4 = ((bf16[256,24,128]{2,1,0:T(8,128)(2,1)}), bf16[256,24,128]{2,1,0:T(8,128)(2,1)S(1)}, u32[]{:S(2)}, u32[]{:S(2)}) async-start(bf16[256,24,128]{2,1,0:T(8,128)(2,1)} %bitcast.16), calls=%async_computation.4 | async-start | bytes 3145728 | tf_op jit(solution)/shard_map/all_to_all | solution.py:425
  124.8 1.0 copy-done.9
  125.9 0.6 copy-done.24
  126.5 1.2 shard_map.206
  127.7 1.4 collective-permute-start.7
  129.1 2.5 %collective-permute-start.8 = (bf16[128,512]{1,0:T(8,128)(2,1)S(1)}, bf16[128,512]{1,0:T(8,128)(2,1)S(1)}, u32[]{:S(2)}, u32[]{:S(2)}) collective-permute-start(bf16[128,512]{1,0:T(8,128)(2,1)S(1)} %get-tuple-element.39), channel_id=1, source_target_pairs={{0,2},{1,3},{2,0},{3,1},{4,6},{5,7},{6,4},{7,5},{8,10},{9,11},{10,... | collective-permute-start | bytes 393224 | tf_op jit(solution)/shard_map/ppermute | solution.py:430
  131.6 1.1 collective-permute-start.9
  132.7 1.2 collective-permute-done.7.s1_ref
  133.9 7.0 %collective-permute-done.8.s2_ref = bf16[128,512]{1,0:T(8,128)(2,1)S(1)} collective-permute-done((bf16[128,512]{1,0:T(8,128)(2,1)S(1)}, bf16[128,512]{1,0:T(8,128)(2,1)S(1)}, u32[]{:S(2)}, u32[]{:S(2)}) %collective-permute-start.8) | collective-permute-done | bytes 131104 | tf_op jit(solution)/shard_map/ppermute | solution.py:430
  140.9 25.9 %all-to-all-done.4 = bf16[256,24,128]{2,1,0:T(8,128)(2,1)S(1)} async-done(((bf16[256,24,128]{2,1,0:T(8,128)(2,1)}), bf16[256,24,128]{2,1,0:T(8,128)(2,1)S(1)}, u32[]{:S(2)}, u32[]{:S(2)}) %all-to-all-start.4) | async-done | bytes 1572896 | tf_op jit(solution)/shard_map/all_to_all | solution.py:425
  166.8 1.6 shard_map.207
  (55 shorter events, 0.1 us)
Async XLA Ops:
  0.0 49.2 %copy-start.13 = (bf16[128,256]{1,0:T(8,128)(2,1)S(1)}, bf16[128,256]{1,0:T(8,128)(2,1)}, u32[]{:S(2)}) copy-start(bf16[128,256]{1,0:T(8,128)(2,1)} %c_ref.3) | copy-start | bytes 196612
  0.0 49.2 %copy-start.12 = (bf16[128,256]{1,0:T(8,128)(2,1)S(1)}, bf16[128,256]{1,0:T(8,128)(2,1)}, u32[]{:S(2)}) copy-start(bf16[128,256]{1,0:T(8,128)(2,1)} %v_ref.3) | copy-start | bytes 196612
  0.0 49.2 %copy-start.11 = (bf16[128,256]{1,0:T(8,128)(2,1)S(1)}, bf16[128,256]{1,0:T(8,128)(2,1)}, u32[]{:S(2)}) copy-start(bf16[128,256]{1,0:T(8,128)(2,1)} %k_ref.3) | copy-start | bytes 196612
  0.0 49.2 %copy-start.10 = (bf16[128,256]{1,0:T(8,128)(2,1)S(1)}, bf16[128,256]{1,0:T(8,128)(2,1)}, u32[]{:S(2)}) copy-start(bf16[128,256]{1,0:T(8,128)(2,1)} %r_ref.3) | copy-start | bytes 196612
  0.0 49.2 %copy-start.25 = (f32[256]{0:T(256)S(1)}, f32[256]{0:T(256)}, u32[]{:S(2)}) copy-start(f32[256]{0:T(256)} %param.27) | copy-start | bytes 3076
  0.0 49.2 %copy-start.28 = (f32[256]{0:T(256)S(1)}, f32[256]{0:T(256)}, u32[]{:S(2)}) copy-start(f32[256]{0:T(256)} %param.30) | copy-start | bytes 3076
  0.0 49.2 %copy-start.27 = (f32[256]{0:T(256)S(1)}, f32[256]{0:T(256)}, u32[]{:S(2)}) copy-start(f32[256]{0:T(256)} %param.29) | copy-start | bytes 3076
  0.0 49.2 %copy-start.26 = (f32[256]{0:T(256)S(1)}, f32[256]{0:T(256)}, u32[]{:S(2)}) copy-start(f32[256]{0:T(256)} %param.28) | copy-start | bytes 3076
  0.1 49.2 %copy-start.18 = (bf16[128,256]{1,0:T(8,128)(2,1)S(1)}, bf16[128,256]{1,0:T(8,128)(2,1)}, u32[]{:S(2)}) copy-start(bf16[128,256]{1,0:T(8,128)(2,1)} %f_ref.1) | copy-start | bytes 196612
  5.8 44.4 %collective-permute-start.5 = (bf16[128,2048]{1,0:T(8,128)(2,1)S(1)}, bf16[128,2048]{1,0:T(8,128)(2,1)}, u32[]{:S(2)}, u32[]{:S(2)}) collective-permute-start(bf16[128,2048]{1,0:T(8,128)(2,1)S(1)} %constant_dynamic-slice_fusion), channel_id=1, source_target_pairs={{0,3},{1,0},{2,1},{3,2},{4,7},{5,4},{6,5},{7,6},{8,11},{9,8},{10,9... | collective-permute-start | bytes 1572872 | tf_op jit(solution)/shard_map/ppermute | solution.py:430
  9.4 40.8 %collective-permute-start.4 = (bf16[128,2048]{1,0:T(8,128)(2,1)S(1)}, bf16[128,2048]{1,0:T(8,128)(2,1)}, u32[]{:S(2)}, u32[]{:S(2)}) collective-permute-start(bf16[128,2048]{1,0:T(8,128)(2,1)S(1)} %constant_dynamic-slice_fusion), channel_id=1, source_target_pairs={{0,2},{1,3},{2,0},{3,1},{4,6},{5,7},{6,4},{7,5},{8,10},{9,11},{10,... | collective-permute-start | bytes 1572872 | tf_op jit(solution)/shard_map/ppermute | solution.py:430
  9.8 40.5 %collective-permute-start.3 = (bf16[128,2048]{1,0:T(8,128)(2,1)S(1)}, bf16[128,2048]{1,0:T(8,128)(2,1)}, u32[]{:S(2)}, u32[]{:S(2)}) collective-permute-start(bf16[128,2048]{1,0:T(8,128)(2,1)S(1)} %constant_dynamic-slice_fusion), channel_id=1, source_target_pairs={{0,1},{1,2},{2,3},{3,0},{4,5},{5,6},{6,7},{7,4},{8,9},{9,10},{10,1... | collective-permute-start | bytes 1572872 | tf_op jit(solution)/shard_map/ppermute | solution.py:430
  22.9 15.6 %all-to-all-start.1 = ((bf16[8,48,128]{2,1,0:T(8,128)(2,1)}), bf16[8,48,128]{2,1,0:T(8,128)(2,1)S(1)}, u32[]{:S(2)}, u32[]{:S(2)}) async-start(bf16[8,48,128]{2,1,0:T(8,128)(2,1)} %get-tuple-element.27), calls=%async_computation.1 | async-start | bytes 196608 | tf_op jit(solution)/shard_map/all_to_all | solution.py:425
  31.2 19.1 %copy-start.22 = (s32[3]{0:T(128)}, s32[3]{0:T(128)S(1)}, u32[]{:S(2)}) copy-start(s32[3]{0:T(128)S(1)} %pad_add_fusion.place_ref) | copy-start | bytes 40
  50.3 5.9 %copy-start.29 = (s32[128,8]{0,1:T(8,128)S(1)}, s32[128,8]{0,1:T(8,128)}, u32[]{:S(2)}) copy-start(s32[128,8]{0,1:T(8,128)} %param.34) | copy-start | bytes 12292
  50.3 6.0 %copy-start.30 = (f32[128,8]{0,1:T(8,128)S(1)}, f32[128,8]{0,1:T(8,128)}, u32[]{:S(2)}) copy-start(f32[128,8]{0,1:T(8,128)} %param.35) | copy-start | bytes 12292
  50.3 11.8 %copy-start = (bf16[256,2048]{1,0:T(8,128)(2,1)S(1)}, bf16[256,2048]{1,0:T(8,128)(2,1)}, u32[]{:S(2)}) copy-start(bf16[256,2048]{1,0:T(8,128)(2,1)} %own_ref.1) | copy-start | bytes 3145732
  50.3 11.8 %copy-start.4 = (bf16[128,2048]{1,0:T(8,128)(2,1)S(1)}, bf16[128,2048]{1,0:T(8,128)(2,1)}, u32[]{:S(2)}) copy-start(bf16[128,2048]{1,0:T(8,128)(2,1)} %residual_ref.1) | copy-start | bytes 1572868
  50.3 11.8 %copy-start.19 = (f32[2048]{0:T(1024)S(1)}, f32[2048]{0:T(1024)}, u32[]{:S(2)}) copy-start(f32[2048]{0:T(1024)} %param.33) | copy-start | bytes 24580
  52.0 10.2 %collective-permute-start.6 = (bf16[3,128,2048]{2,1,0:T(8,128)(2,1)S(1)}, bf16[3,128,2048]{2,1,0:T(8,128)(2,1)}, u32[]{:S(2)}, u32[]{:S(2)}) collective-permute-start(bf16[3,128,2048]{2,1,0:T(8,128)(2,1)S(1)} %pad_maximum_fusion.near_ref), channel_id=1, source_target_pairs={{0,4},{4,0},{1,5},{5,1},{2,6},{6,2},{3,7},{7,3},{8,12},{12,8},{9,1... | collective-permute-start | bytes 4718600 | tf_op jit(solution)/shard_map/ppermute | solution.py:430
  52.8 4.9 %collective-permute-start.2 = (bf16[128,256]{1,0:T(8,128)(2,1)S(1)}, bf16[128,256]{1,0:T(8,128)(2,1)S(1)}, u32[]{:S(2)}, u32[]{:S(2)}) collective-permute-start(bf16[128,256]{1,0:T(8,128)(2,1)S(1)} %shard_map.203.h0_ref), channel_id=1, source_target_pairs={{0,3},{1,0},{2,1},{3,2},{4,7},{5,4},{6,5},{7,6},{8,11},{9,8},{10,9... | collective-permute-start | bytes 196616 | tf_op jit(solution)/shard_map/ppermute | solution.py:430
  54.8 4.6 %collective-permute-start.1 = (bf16[128,256]{1,0:T(8,128)(2,1)S(1)}, bf16[128,256]{1,0:T(8,128)(2,1)S(1)}, u32[]{:S(2)}, u32[]{:S(2)}) collective-permute-start(bf16[128,256]{1,0:T(8,128)(2,1)S(1)} %shard_map.203.h0_ref), channel_id=1, source_target_pairs={{0,2},{1,3},{2,0},{3,1},{4,6},{5,7},{6,4},{7,5},{8,10},{9,11},{10,... | collective-permute-start | bytes 196616 | tf_op jit(solution)/shard_map/ppermute | solution.py:430
  56.2 5.3 %collective-permute-start = (bf16[128,256]{1,0:T(8,128)(2,1)S(1)}, bf16[128,256]{1,0:T(8,128)(2,1)S(1)}, u32[]{:S(2)}, u32[]{:S(2)}) collective-permute-start(bf16[128,256]{1,0:T(8,128)(2,1)S(1)} %shard_map.203.h0_ref), channel_id=1, source_target_pairs={{0,1},{1,2},{2,3},{3,0},{4,5},{5,6},{6,7},{7,4},{8,9},{9,10},{10,1... | collective-permute-start | bytes 196616 | tf_op jit(solution)/shard_map/ppermute | solution.py:430
  57.1 0.6 copy-start.20
  59.4 0.6 copy-start.14
  61.5 0.6 copy-start.16
  62.2 0.8 copy-start.15
  63.0 0.8 copy-start.17
  63.9 0.6 copy-start.23
  64.5 48.4 %copy-start.2 = (bf16[1,2048,512]{2,1,0:T(8,128)(2,1)S(1)}, bf16[1,2048,512]{2,1,0:T(8,128)(2,1)}, u32[]{:S(2)}) copy-start(bf16[1,2048,512]{2,1,0:T(8,128)(2,1)} %param.37) | copy-start | bytes 6291460
  64.5 48.4 %copy-start.3 = (bf16[1,512,2048]{2,1,0:T(8,128)(2,1)S(1)}, bf16[1,512,2048]{2,1,0:T(8,128)(2,1)}, u32[]{:S(2)}) copy-start(bf16[1,512,2048]{2,1,0:T(8,128)(2,1)} %param.38) | copy-start | bytes 6291460
  69.2 43.7 %copy-start.8 = (bf16[128,2048]{1,0:T(8,128)(2,1)}, bf16[128,2048]{1,0:T(8,128)(2,1)S(1)}, u32[]{:S(2)}) copy-start(bf16[128,2048]{1,0:T(8,128)(2,1)S(1)} %get-tuple-element.36.normed_ref) | copy-start | bytes 1572868
  69.2 43.7 %copy-start.1 = (bf16[1,2048,512]{2,1,0:T(8,128)(2,1)S(1)}, bf16[1,2048,512]{2,1,0:T(8,128)(2,1)}, u32[]{:S(2)}) copy-start(bf16[1,2048,512]{2,1,0:T(8,128)(2,1)} %param.36) | copy-start | bytes 6291460
  117.5 7.3 %copy-start.5 = (bf16[2048,128]{1,0:T(8,128)(2,1)S(1)}, bf16[2048,128]{1,0:T(8,128)(2,1)}, u32[]{:S(2)}) copy-start(bf16[2048,128]{1,0:T(8,128)(2,1)} %gate_ref.1) | copy-start | bytes 1572868
  117.5 7.3 %copy-start.6 = (bf16[2048,128]{1,0:T(8,128)(2,1)S(1)}, bf16[2048,128]{1,0:T(8,128)(2,1)}, u32[]{:S(2)}) copy-start(bf16[2048,128]{1,0:T(8,128)(2,1)} %up_ref.1) | copy-start | bytes 1572868
  117.5 7.3 %copy-start.7 = (bf16[128,2048]{1,0:T(8,128)(2,1)S(1)}, bf16[128,2048]{1,0:T(8,128)(2,1)}, u32[]{:S(2)}) copy-start(bf16[128,2048]{1,0:T(8,128)(2,1)} %down_ref.1) | copy-start | bytes 1572868
  117.5 49.3 %all-to-all-start.4 = ((bf16[256,24,128]{2,1,0:T(8,128)(2,1)}), bf16[256,24,128]{2,1,0:T(8,128)(2,1)S(1)}, u32[]{:S(2)}, u32[]{:S(2)}) async-start(bf16[256,24,128]{2,1,0:T(8,128)(2,1)} %bitcast.16), calls=%async_computation.4 | async-start | bytes 3145728 | tf_op jit(solution)/shard_map/all_to_all | solution.py:425
  124.8 1.0 copy-start.9
  125.9 0.6 copy-start.24
  126.5 40.3 %copy-start.21 = (f32[6,256]{1,0:T(8,128)S(1)}, f32[6,256]{1,0:T(8,128)}, u32[]{:S(2)}) copy-start(f32[6,256]{1,0:T(8,128)} %copy-done.20) | copy-start | bytes 18436
  127.7 6.2 %collective-permute-start.7 = (bf16[128,512]{1,0:T(8,128)(2,1)S(1)}, bf16[128,512]{1,0:T(8,128)(2,1)S(1)}, u32[]{:S(2)}, u32[]{:S(2)}) collective-permute-start(bf16[128,512]{1,0:T(8,128)(2,1)S(1)} %get-tuple-element.38), channel_id=1, source_target_pairs={{0,1},{1,2},{2,3},{3,0},{4,5},{5,6},{6,7},{7,4},{8,9},{9,10},{10,1... | collective-permute-start | bytes 393224 | tf_op jit(solution)/shard_map/ppermute | solution.py:430
  129.1 11.8 %collective-permute-start.8 = (bf16[128,512]{1,0:T(8,128)(2,1)S(1)}, bf16[128,512]{1,0:T(8,128)(2,1)S(1)}, u32[]{:S(2)}, u32[]{:S(2)}) collective-permute-start(bf16[128,512]{1,0:T(8,128)(2,1)S(1)} %get-tuple-element.39), channel_id=1, source_target_pairs={{0,2},{1,3},{2,0},{3,1},{4,6},{5,7},{6,4},{7,5},{8,10},{9,11},{10,... | collective-permute-start | bytes 393224 | tf_op jit(solution)/shard_map/ppermute | solution.py:430
  131.6 9.4 %collective-permute-start.9 = (bf16[128,512]{1,0:T(8,128)(2,1)S(1)}, bf16[128,512]{1,0:T(8,128)(2,1)S(1)}, u32[]{:S(2)}, u32[]{:S(2)}) collective-permute-start(bf16[128,512]{1,0:T(8,128)(2,1)S(1)} %get-tuple-element.40), channel_id=1, source_target_pairs={{0,3},{1,0},{2,1},{3,2},{4,7},{5,4},{6,5},{7,6},{8,11},{9,8},{10,9... | collective-permute-start | bytes 393224 | tf_op jit(solution)/shard_map/ppermute | solution.py:430
